TPU v7x, 512 devices: a whole 4x4x16 slice. The times are simulated.
512 devices in a mesh: sp: 128 (over z, x, core), tp: 4 (over y).
Axes of the slice: x: 4, y: 4, z: 16, core: 2. Of those that a mesh axis runs over, the one named last changes fastest.
Arguments:
- tokens: bfloat16 [16384, 2048], P('sp'), may hold values from -6 to 6
- pre_gain: float32 [2048], replicated, may hold values from 0.1 to 1.9
- outer_gate: bfloat16 [2048, 1024], P('sp', 'tp'), may hold values from -0.125 to 0.125
- inner_gate: bfloat16 [2048, 1024], P('sp', 'tp'), may hold values from -0.125 to 0.125
- conv_input: bfloat16 [2048, 1024], P('sp', 'tp'), may hold values from -0.125 to 0.125
- conv_taps: float32 [3, 1024], P(None, 'tp'), may hold values from -3.5 to 3.5
- query_down: bfloat16 [2048, 768], P(None, 'tp'), may hold values from -0.088388348 to 0.088388348
- latent_down: bfloat16 [2048, 512], P(None, 'tp'), may hold values from -0.088388348 to 0.088388348
- rotary_down: bfloat16 [2048, 32], replicated, may hold values from -0.125 to 0.125
- query_gain: float32 [768], replicated, may hold values from 1 to 3
- latent_gain: float32 [512], replicated, may hold values from 1 to 3
- query_up: bfloat16 [768, 512], P(None, 'tp'), may hold values from -0.14433757 to 0.14433757
- query_rotary: bfloat16 [768, 256], P(None, 'tp'), may hold values from -0.21875 to 0.21875
- key_up: bfloat16 [512, 512], P(None, 'tp'), may hold values from -4.33012702 to 4.33012702
- value_up: bfloat16 [512, 512], P(None, 'tp'), may hold values from -0.25 to 0.25
- conv_output: bfloat16 [1024, 2048], P('tp'), may hold values from -0.15625 to 0.15625
- heads_output: bfloat16 [512, 2048], P('tp'), may hold values from -0.15625 to 0.15625
- post_gain: float32 [2048], replicated, may hold values from 0.1 to 1.9
Outputs:
- mixed: bfloat16 [16384, 2048], P(('sp', 'tp'))
- row_logsum: float32 [8, 16384], P('tp', 'sp')
All inputs are finite; a program needn't handle non-finite values.
Results may differ from a plain program's by a relative error of at most 0.013.
Values may be sent and summed in bfloat16 or wider, within the bound.
No kernel may reach another device: no remote copies, remote signals or barrier semaphores. Data moves between devices by JAX's collectives and lax.ppermute only.
A program may use at most 64 MiB of HBM per device.

v0:
```python
import math

import jax
import jax.numpy as jnp
from jax import lax
from jax.sharding import Mesh
from jax.sharding import PartitionSpec as P

NOPE = 64
ROPE = 32
VDIM = 64
TAPS = 3
SP = ("sp_0", "sp_1", "sp_2")
SP_TP = ("sp_0", "sp_1", "sp_2", "tp")


eps = 1e-06
rope_theta = 500000.0


def copy_for_each(array, axis):
    copies = jnp.broadcast_to(array, (lax.axis_size(axis), *array.shape))
    return lax.all_to_all(copies, axis, split_axis=0, concat_axis=0, tiled=True)


def laid_out(pieces, dim):
    shape = list(pieces.shape[1:])
    shape[dim] *= pieces.shape[0]
    return jnp.moveaxis(pieces, 0, dim).reshape(shape)


def gathered_by_axis(array, axes, dim):
    far, near = axes
    pieces = copy_for_each(copy_for_each(array, far), near)
    return laid_out(pieces.swapaxes(0, 1).reshape(-1, *array.shape), dim)


def sent_together(arrays, axis, dim, along):
    both = jnp.concatenate(arrays, axis=along)
    whole, at, done = (gathered_by_axis(both, axis, dim), 0, [])
    for a in arrays:
        done.append(lax.slice_in_dim(whole, at, at + a.shape[along], axis=along))
        at += a.shape[along]
    return tuple(done)


def shifted(value, axis, steps):
    count = lax.axis_size(axis)
    first, last = (max(0, -steps), min(count, count - steps))
    return lax.ppermute(value, axis, [(source, source + steps) for source in range(first, last)])


def one_gather(arrays, axis, dims):
    vector = jnp.concatenate([a.reshape(-1) for a in arrays])
    lines, at, done = (lax.all_gather(vector, axis), 0, [])
    for a, dim in zip(arrays, dims):
        pieces = lines[:, at : at + a.size].reshape(-1, *a.shape)
        done.append(laid_out(pieces, dim))
        at += a.size
    return tuple(done)


def side_by_side(arrays, axis, dim, along):
    both = jnp.concatenate(arrays, axis=along)
    whole, at, done = (lax.all_gather(both, axis, axis=dim, tiled=True), 0, [])
    for a in arrays:
        done.append(lax.slice_in_dim(whole, at, at + a.shape[along], axis=along))
        at += a.shape[along]
    return tuple(done)


def in_blocks(array, dim, count):
    shape = array.shape
    pieces = array.reshape(*shape[:dim], count, shape[dim] // count, *shape[dim + 1 :])
    return jnp.moveaxis(pieces, dim, 0)


def sum_at_owner(array, axis, dim):
    pieces = in_blocks(array, dim, lax.axis_size(axis))
    arrived = lax.all_to_all(pieces, axis, split_axis=0, concat_axis=0, tiled=True)
    return arrived.astype(jnp.float32).sum(axis=0)


def rms_scale(values, scale_row):
    widened = values.astype(jnp.float32)
    return (
        widened * lax.rsqrt(jnp.mean(widened * widened, axis=-1, keepdims=True) + eps) * scale_row
    )


def rotate(values, positions):
    half_width = values.shape[-1] // 2
    frequency = rope_theta ** (-jnp.arange(half_width, dtype=jnp.float32) / half_width)
    angles = positions.astype(jnp.float32)[:, None] * frequency
    cosine = jnp.cos(angles)[:, None, :]
    sine_part = jnp.sin(angles)[:, None, :]
    leading = values[..., :half_width]
    trailing = values[..., half_width:]
    return jnp.concatenate(
        [leading * cosine - trailing * sine_part, trailing * cosine + leading * sine_part], axis=-1
    )


def attend(
    state_now, query_nope, query_turned, key_nope, key_rotary, value_rows, key_first, query_position
):
    row_best, weight_sum, weighted = state_now
    heads_here = query_nope.shape[1]
    key_count = key_nope.shape[0]
    key_heads = key_nope.reshape(key_count, heads_here, NOPE)
    value_heads = value_rows.reshape(key_count, heads_here, VDIM)
    scores = jnp.einsum("qhd,khd->hqk", query_nope, key_heads, preferred_element_type=jnp.float32)
    scores = scores + jnp.einsum(
        "qhd,kd->hqk", query_turned, key_rotary, preferred_element_type=jnp.float32
    )
    scores = scores * (NOPE + ROPE) ** (-0.5)
    key_position = key_first + jnp.arange(key_count, dtype=jnp.int32)
    causal = key_position[None, :] <= query_position[:, None]
    scores = jnp.where(causal[None], scores, -1e30)
    new_best = jnp.maximum(row_best, jnp.max(scores, axis=-1))
    weights = jnp.where(causal[None], jnp.exp(scores - new_best[..., None]), 0.0)
    shrink = jnp.exp(row_best - new_best)
    weight_sum = weight_sum * shrink + jnp.sum(weights, axis=-1)
    weighted = weighted * shrink[..., None] + jnp.einsum(
        "hqk,khd->hqd",
        weights.astype(jnp.bfloat16),
        value_heads,
        preferred_element_type=jnp.float32,
    )
    return (new_best, weight_sum, weighted)


def fold_blocks(state_now, pieces, step_rule):
    total_rows = pieces[0].shape[0]
    block_width = math.gcd(total_rows, 1024)
    block_count = total_rows // block_width
    stacked = tuple(
        (member.reshape(block_count, block_width, member.shape[1]) for member in pieces)
    )

    def one_block(state_in, inputs):
        block_index, block_pieces = inputs
        return (step_rule(state_in, block_pieces, block_index * block_width), None)

    state_out, unused = lax.scan(
        one_block, state_now, (jnp.arange(block_count, dtype=jnp.int32), stacked)
    )
    return state_out


def local(
    tokens,
    pre_gain,
    outer_gate,
    inner_gate,
    conv_input,
    conv_taps,
    query_down,
    latent_down,
    rotary_down,
    query_gain,
    latent_gain,
    query_up,
    query_rotary,
    key_up,
    value_up,
    conv_output,
    heads_output,
    post_gain,
):
    row_count = tokens.shape[0]
    normed = rms_scale(tokens, pre_gain).astype(jnp.bfloat16)
    sp_index = lax.axis_index(SP)
    positions = sp_index * row_count + jnp.arange(row_count, dtype=jnp.int32)
    pieces = sent_together((outer_gate, inner_gate, conv_input), (("sp_0", "sp_1"), "sp_2"), 0, 1)
    outer_part, inner_part, signal = tuple(
        (jnp.dot(normed, member, preferred_element_type=jnp.float32) for member in pieces)
    )
    product = (inner_part * signal).astype(jnp.bfloat16)
    edge_rows = shifted(product[row_count - (TAPS - 1) :], SP, 1)
    extended = jnp.concatenate([edge_rows, product], axis=0).astype(jnp.float32)
    convolved = extended[0:row_count] * conv_taps[0]
    for offset in range(1, TAPS):
        convolved = convolved + extended[offset : offset + row_count] * conv_taps[offset]
    conv_mixed = (outer_part * convolved).astype(jnp.bfloat16)
    query_latent = jnp.dot(normed, query_down, preferred_element_type=jnp.float32).astype(
        jnp.bfloat16
    )
    key_latent = jnp.dot(normed, latent_down, preferred_element_type=jnp.float32).astype(
        jnp.bfloat16
    )
    query_latent, key_latent = one_gather((query_latent, key_latent), "tp", (1, 1))
    query_normed = rms_scale(query_latent, query_gain).astype(jnp.bfloat16)
    latent_normed = rms_scale(key_latent, latent_gain).astype(jnp.bfloat16)
    rotary_raw = jnp.dot(normed, rotary_down, preferred_element_type=jnp.float32)
    key_rotary = rotate(rotary_raw[:, None, :], positions)[:, 0, :].astype(jnp.bfloat16)
    heads_here = query_up.shape[1] // NOPE
    query_nope = jnp.dot(query_normed, query_up, preferred_element_type=jnp.float32).astype(
        jnp.bfloat16
    )
    query_nope = query_nope.reshape(row_count, heads_here, NOPE)
    turned_raw = jnp.dot(query_normed, query_rotary, preferred_element_type=jnp.float32)
    query_turned = rotate(turned_raw.reshape(row_count, heads_here, ROPE), positions).astype(
        jnp.bfloat16
    )
    key_nope = jnp.dot(latent_normed, key_up, preferred_element_type=jnp.float32).astype(
        jnp.bfloat16
    )
    value_rows = jnp.dot(latent_normed, value_up, preferred_element_type=jnp.float32).astype(
        jnp.bfloat16
    )
    initial = (
        jnp.full((heads_here, row_count), -1e30, jnp.float32),
        jnp.zeros((heads_here, row_count), jnp.float32),
        jnp.zeros((heads_here, row_count, VDIM), jnp.float32),
    )

    def heads_step(state_now, block_pieces, key_first):
        return attend(
            state_now,
            query_nope,
            query_turned,
            block_pieces[0],
            block_pieces[1],
            block_pieces[2],
            key_first,
            positions,
        )

    row_best, weight_sum, weighted = fold_blocks(
        initial, side_by_side((key_nope, key_rotary, value_rows), SP, 0, 1), heads_step
    )
    heads_mixed = (weighted / weight_sum[..., None]).astype(jnp.bfloat16)
    heads_mixed = heads_mixed.transpose(1, 0, 2).reshape(row_count, heads_here * VDIM)
    row_logsum = row_best + jnp.log(weight_sum)
    projected = sum_at_owner(
        (
            jnp.dot(conv_mixed, conv_output, preferred_element_type=jnp.float32)
            + jnp.dot(heads_mixed, heads_output, preferred_element_type=jnp.float32)
        ).astype(jnp.bfloat16),
        "tp",
        0,
    )
    mixed = rms_scale(projected, post_gain).astype(jnp.bfloat16)
    return (mixed, row_logsum)


def solution(mesh):
    split = Mesh(mesh.devices.reshape(16, 4, 2, mesh.shape["tp"]), ("sp_0", "sp_1", "sp_2", "tp"))
    return jax.shard_map(
        local,
        mesh=split,
        in_specs=(
            P(SP, None),
            P(),
            P(SP, "tp"),
            P(SP, "tp"),
            P(SP, "tp"),
            P(None, "tp"),
            P(None, "tp"),
            P(None, "tp"),
            P(),
            P(),
            P(),
            P(None, "tp"),
            P(None, "tp"),
            P(None, "tp"),
            P(None, "tp"),
            P("tp", None),
            P("tp", None),
            P(),
        ),
        out_specs=(P(SP_TP, None), P("tp", SP)),
        check_vma=False,
    )
```

profile of v0, /device:TPU:1, one launch (start us, length us, event | category | flops | bytes accessed | tf_op | source)
XLA Modules:
  0.0 311.4 jit_solution(3868678448744605362)
XLA Ops:
  7.3 1.3 fusion.22
  8.7 1.6 fusion.21
  10.3 1.8 convolution_convert_fusion
  12.4 10.8 %all-gather = bf16[163840]{0:T(1024)(128)(2,1)S(1)} all-gather(bf16[40960]{0:T(1024)(128)(2,1)S(1)} %pad_maximum_fusion), channel_id=2, replica_groups=mesh['sp_0'=16,'sp_1'=4,'sp_2'=2,'tp'=4] {'tp'}, dimensions={0}, use_global_device_ids=true | all-gather | bytes 409600 | tf_op jit(solution)/shard_map/all_gather | solution.py:55
  25.8 1.3 broadcast_in_dim.26
  27.0 19.1 %all-to-all-start = ((bf16[64,16,768]{2,1,0:T(8,128)(2,1)}), bf16[64,16,768]{2,1,0:T(8,128)(2,1)S(1)}, u32[]{:S(2)}, u32[]{:S(2)}) async-start(bf16[64,16,768]{2,1,0:T(8,128)(2,1)} %broadcast_in_dim.26), calls=%async_computation | async-start | bytes 3145728 | tf_op jit(solution)/shard_map/all_to_all | solution.py:23
  49.4 1.2 fusion.61
  51.4 1.2 convolution_convert_fusion.4
  52.6 69.6 %all-to-all-done = bf16[64,16,768]{2,1,0:T(8,128)(2,1)S(1)} async-done(((bf16[64,16,768]{2,1,0:T(8,128)(2,1)}), bf16[64,16,768]{2,1,0:T(8,128)(2,1)S(1)}, u32[]{:S(2)}, u32[]{:S(2)}) %all-to-all-start) | async-done | bytes 1572896 | tf_op jit(solution)/shard_map/all_to_all | solution.py:23
  122.5 12.5 %all_to_all.15 = bf16[2,64,16,768]{3,2,1,0:T(8,128)(2,1)S(1)} all-to-all(bf16[2,64,16,768]{3,2,1,0:T(8,128)(2,1)S(1)} %broadcast_in_dim.31), channel_id=1, replica_groups=mesh['sp_0'=16,'sp_1'=4,'sp_2'=2,'tp'=4] {'sp_2'}, dimensions={0} | all-to-all | bytes 6291456 | tf_op jit(solution)/shard_map/all_to_all | solution.py:23
  137.5 4.4 %collective-permute-start = (bf16[2,256]{1,0:T(2,128)(2,1)S(1)}, bf16[2,256]{1,0:T(2,128)(2,1)S(1)}, u32[]{:S(2)}, u32[]{:S(2)}) collective-permute-start(bf16[2,256]{1,0:T(2,128)(2,1)S(1)} %slice.79), channel_id=1, source_target_pairs={{0,4},{4,8},{8,12},{12,16},{16,20},{20,24},{24,28},{28,32},{32,36}... | collective-permute-start | bytes 3080 | tf_op jit(solution)/shard_map/ppermute | solution.py:50
  142.6 2.0 fusion.20
  144.6 70.6 %all-gather.3.cloned.1.call-done = bf16[16384,288]{0,1:T(8,128)(2,1)} async-done(((bf16[128,288]{0,1:T(8,128)(2,1)}), bf16[16384,288]{0,1:T(8,128)(2,1)}) %all-gather.3.cloned.1.call-update) | async-done | bytes 9437200 | tf_op jit(solution)/shard_map/all_gather | solution.py:65
  215.2 1.3 slice.88
  216.6 3.9 %fusion.59 = (bf16[16384,128]{0,1:T(8,128)(2,1)S(1)}, bf16[16384,128]{0,1:T(8,128)(2,1)S(1)}) fusion(bf16[16384,288]{0,1:T(8,128)(2,1)} %all-gather.3.cloned.1.call-done), kind=kLoop, calls=%fused_computation.109 | loop fusion | bytes 16777216 | tf_op jit(solution)/shard_map/slice | solution.py:67
  220.5 4.3 %copy_bitcast_fusion = (bf16[16,1024,128]{1,2,0:T(8,128)(2,1)}, bf16[16,1024,128]{1,2,0:T(8,128)(2,1)}) fusion(bf16[16,16,8,1024]{3,2,1,0:T(8,128)(2,1)S(1)} %bitcast.114, bf16[16,16,8,1024]{3,2,1,0:T(8,128)(2,1)S(1)} %bitcast.115), kind=kLoop, calls=%fused_computation.28 | loop fusion | bytes 16777216
  224.8 63.5 %while.15 = (s32[]{:T(128)}, f32[2,128]{1,0:T(2,128)S(1)}, f32[2,128]{1,0:T(2,128)S(1)}, f32[2,128,64]{1,2,0:T(8,128)S(1)}, s32[16]{0:T(128)S(1)}, /*index=5*/bf...) while((s32[]{:T(128)}, f32[2,128]{1,0:T(2,128)S(1)}, ...), condition=%wide.region_7.8_spmd.clone, body=%wide.region_4.7_spmd.clone.sunk | while | flops 86690176 | bytes 7611585 | solution.py:145
  226.3 1.1 constant_dynamic-slice_fusion.3
  230.2 1.1 constant_dynamic-slice_fusion.3
  234.2 1.1 constant_dynamic-slice_fusion.3
  238.2 1.1 constant_dynamic-slice_fusion.3
  242.2 1.1 constant_dynamic-slice_fusion.3
  246.1 1.1 constant_dynamic-slice_fusion.3
  254.1 1.1 constant_dynamic-slice_fusion.3
  258.0 1.1 constant_dynamic-slice_fusion.3
  262.0 1.1 constant_dynamic-slice_fusion.3
  266.0 1.1 constant_dynamic-slice_fusion.3
  281.8 1.1 constant_dynamic-slice_fusion.3
  285.8 1.1 constant_dynamic-slice_fusion.3
  288.3 2.2 fusion.17
  290.5 4.0 %all-to-all-start.2 = ((bf16[4,32,2048]{2,1,0:T(8,128)(2,1)}), bf16[4,32,2048]{2,1,0:T(8,128)(2,1)S(1)}, u32[]{:S(2)}, u32[]{:S(2)}) async-start(bf16[4,32,2048]{2,1,0:T(8,128)(2,1)} %bitcast.22), calls=%async_computation.2 | async-start | bytes 1048576 | tf_op jit(solution)/shard_map/all_to_all | solution.py:80
  295.1 8.5 %all-to-all-done.2 = bf16[4,32,2048]{2,1,0:T(8,128)(2,1)S(1)} async-done(((bf16[4,32,2048]{2,1,0:T(8,128)(2,1)}), bf16[4,32,2048]{2,1,0:T(8,128)(2,1)S(1)}, u32[]{:S(2)}, u32[]{:S(2)}) %all-to-all-start.2) | async-done | bytes 524320 | tf_op jit(solution)/shard_map/all_to_all | solution.py:80
  (272 shorter events, 50.8 us)
Async XLA Ops:
  7.2 135.4 %copy-start = (bf16[256,2048]{1,0:T(8,128)(2,1)S(1)}, bf16[256,2048]{1,0:T(8,128)(2,1)}, u32[]{:S(2)}) copy-start(bf16[256,2048]{1,0:T(8,128)(2,1)} %param.35) | copy-start | bytes 3145732
  7.2 16.4 %copy-start.2 = (bf16[128,2048]{1,0:T(8,128)(2,1)S(1)}, bf16[128,2048]{1,0:T(8,128)(2,1)}, u32[]{:S(2)}) copy-start(bf16[128,2048]{1,0:T(8,128)(2,1)} %param.20) | copy-start | bytes 1572868
  7.2 16.4 %copy-start.7 = (f32[2048]{0:T(1024)S(1)}, f32[2048]{0:T(1024)}, u32[]{:S(2)}) copy-start(f32[2048]{0:T(1024)} %param.21) | copy-start | bytes 24580
  7.2 16.4 %copy-start.18 = (bf16[2048,32]{0,1:T(8,128)(2,1)S(1)}, bf16[2048,32]{0,1:T(8,128)(2,1)}, u32[]{:S(2)}) copy-start(bf16[2048,32]{0,1:T(8,128)(2,1)} %param.28) | copy-start | bytes 393220
  7.2 17.0 %copy-start.12 = (f32[512]{0:T(512)S(1)}, f32[512]{0:T(512)}, u32[]{:S(2)}) copy-start(f32[512]{0:T(512)} %param.30) | copy-start | bytes 6148
  7.2 17.2 %copy-start.4 = (bf16[512,128]{1,0:T(8,128)(2,1)S(1)}, bf16[512,128]{1,0:T(8,128)(2,1)}, u32[]{:S(2)}) copy-start(bf16[512,128]{1,0:T(8,128)(2,1)} %param.34) | copy-start | bytes 393220
  7.2 208.0 %all-gather.3.cloned.1.call-start = ((), (), s32[]{:S(2)}) async-start(), calls=%async_computation.3 | async-start | bytes 9510912 | tf_op jit(solution)/shard_map/all_gather | solution.py:65
  7.3 17.6 %copy-start.13 = (f32[16]{0:T(128)}, f32[16]{0:T(128)S(1)}, u32[]{:S(2)}) copy-start(f32[16]{0:T(128)S(1)} %multiply_power_fusion) | copy-start | bytes 196
  7.3 17.4 %copy-start.5 = (bf16[512,128]{1,0:T(8,128)(2,1)S(1)}, bf16[512,128]{1,0:T(8,128)(2,1)}, u32[]{:S(2)}) copy-start(bf16[512,128]{1,0:T(8,128)(2,1)} %param.33) | copy-start | bytes 393220
  8.7 16.0 %copy-start.16 = (f32[128]{0:T(128)}, f32[128]{0:T(128)S(1)}, u32[]{:S(2)}) copy-start(f32[128]{0:T(128)S(1)} %add_rsqrt_fusion.3) | copy-start | bytes 1540
  8.7 17.0 %copy-start.9 = (bf16[16,256]{1,0:T(8,128)(2,1)S(1)}, bf16[16,256]{1,0:T(8,128)(2,1)}, u32[]{:S(2)}) copy-start(bf16[16,256]{1,0:T(8,128)(2,1)} %param.24) | copy-start | bytes 24580
  8.7 17.0 %copy-start.10 = (bf16[16,256]{1,0:T(8,128)(2,1)S(1)}, bf16[16,256]{1,0:T(8,128)(2,1)}, u32[]{:S(2)}) copy-start(bf16[16,256]{1,0:T(8,128)(2,1)} %param.23) | copy-start | bytes 24580
  8.7 17.0 %copy-start.11 = (bf16[16,256]{1,0:T(8,128)(2,1)S(1)}, bf16[16,256]{1,0:T(8,128)(2,1)}, u32[]{:S(2)}) copy-start(bf16[16,256]{1,0:T(8,128)(2,1)} %param.22) | copy-start | bytes 24580
  23.5 22.6 %copy-start.6 = (f32[768]{0:T(1024)S(1)}, f32[768]{0:T(1024)}, u32[]{:S(2)}) copy-start(f32[768]{0:T(1024)} %param.29) | copy-start | bytes 9220
  23.6 3.4 %copy-start.14 = (f32[128]{0:T(128)}, f32[128]{0:T(128)S(1)}, u32[]{:S(2)}) copy-start(f32[128]{0:T(128)S(1)} %add_convert_fusion.1) | copy-start | bytes 1540
  27.0 95.2 %all-to-all-start = ((bf16[64,16,768]{2,1,0:T(8,128)(2,1)}), bf16[64,16,768]{2,1,0:T(8,128)(2,1)S(1)}, u32[]{:S(2)}, u32[]{:S(2)}) async-start(bf16[64,16,768]{2,1,0:T(8,128)(2,1)} %broadcast_in_dim.26), calls=%async_computation | async-start | bytes 3145728 | tf_op jit(solution)/shard_map/all_to_all | solution.py:23
  46.7 0.9 copy-start.15
  135.0 1.0 copy-start.3
  135.0 1.0 copy-start.17
  135.4 1.7 copy-start.1
  137.5 5.1 %collective-permute-start = (bf16[2,256]{1,0:T(2,128)(2,1)S(1)}, bf16[2,256]{1,0:T(2,128)(2,1)S(1)}, u32[]{:S(2)}, u32[]{:S(2)}) collective-permute-start(bf16[2,256]{1,0:T(2,128)(2,1)S(1)} %slice.79), channel_id=1, source_target_pairs={{0,4},{4,8},{8,12},{12,16},{16,20},{20,24},{24,28},{28,32},{32,36}... | collective-permute-start | bytes 3080 | tf_op jit(solution)/shard_map/ppermute | solution.py:50
  288.3 15.5 %copy-start.8 = (f32[2048]{0:T(1024)S(1)}, f32[2048]{0:T(1024)}, u32[]{:S(2)}) copy-start(f32[2048]{0:T(1024)} %param.37) | copy-start | bytes 24580
  290.5 13.1 %all-to-all-start.2 = ((bf16[4,32,2048]{2,1,0:T(8,128)(2,1)}), bf16[4,32,2048]{2,1,0:T(8,128)(2,1)S(1)}, u32[]{:S(2)}, u32[]{:S(2)}) async-start(bf16[4,32,2048]{2,1,0:T(8,128)(2,1)} %bitcast.22), calls=%async_computation.2 | async-start | bytes 1048576 | tf_op jit(solution)/shard_map/all_to_all | solution.py:80
Sparse Core Ops, SparseCore 0:
  25.8 189.3 all-gather.2
where the time goes:
time: 312 us; the launch traced here: 311 us
  waiting for transfers between devices  149 us (48%)
  local copies, waits for them, and re-layouts  42.1 us (13%)
  matrix products  29.3 us (9%)
  starting transfers between devices  27.5 us (9%)
  blocking collectives  23.3 us (7%)
  between operations  14.6 us (5%)
  other arithmetic  13.5 us (4%)
  loops' own time  11.6 us (4%)
    all_gather x1, waiting for transfers between devices, side_by_side(): whole, at, done = (lax.all_gather(both, axis, axis=dim, tiled=True), 0, [])  70.6 us
    all_to_all x1, waiting for transfers between devices, copy_for_each(): return lax.all_to_all(copies, axis, split_axis=0, concat_axis=0, tiled=True)  69.6 us
    dynamic_slice x32, local copies, waits for them, and re-layouts, fold_blocks(): lax.scan(one_block, state_now, (jnp.arange(block_count, dtype=jnp.int32),...  26.5 us
    all_to_all x1, starting transfers between devices, copy_for_each(): return lax.all_to_all(copies, axis, split_axis=0, concat_axis=0, tiled=True)  19.1 us
    all_to_all x1, blocking collectives, copy_for_each(): return lax.all_to_all(copies, axis, split_axis=0, concat_axis=0, tiled=True)  12.5 us
    another operation x1, loops' own time, fold_blocks(): lax.scan(one_block, state_now, (jnp.arange(block_count, dtype=jnp.int32),...  11.6 us
    all_gather x1, blocking collectives, one_gather(): lines, at, done = (lax.all_gather(vector, axis), 0, [])  10.8 us
    all_to_all x1, waiting for transfers between devices, sum_at_owner(): lax.all_to_all(pieces, axis, split_axis=0, concat_axis=0, tiled=True)  8.47 us
  transfers between devices with their start and end apart: 4, of which 4 were waited for; matrix products, arithmetic and copies ran while one was open for 4% of the time, Pallas kernels for 0%

commit v1 on v0

v1 whole, which is shorter than its diff:
```python
import functools
import math

import jax
import jax.numpy as jnp
from jax import lax
from jax.experimental import pallas as pl
from jax.experimental.pallas import tpu as pltpu
from jax.sharding import Mesh
from jax.sharding import PartitionSpec as P

NOPE = 64
ROPE = 32
VDIM = 64
TAPS = 3
SP = ("sp_0", "sp_1", "sp_2")
SP_TP = ("sp_0", "sp_1", "sp_2", "tp")
GROUP = ("sp_1", "sp_2")

eps = 1e-06
rope_theta = 500000.0
SCALE = (NOPE + ROPE) ** (-0.5)
LOG2E = math.log2(math.e)
LOW = -1e30
BF16 = jnp.bfloat16
F32 = jnp.float32


def copy_for_each(array, axis):
    copies = jnp.broadcast_to(array, (lax.axis_size(axis), *array.shape))
    return lax.all_to_all(copies, axis, split_axis=0, concat_axis=0, tiled=True)


def exchange(array, axis):
    return lax.all_to_all(array, axis, split_axis=0, concat_axis=0, tiled=True)


def shifted(value, axis, steps):
    count = lax.axis_size(axis)
    first, last = (max(0, -steps), min(count, count - steps))
    return lax.ppermute(value, axis, [(source, source + steps) for source in range(first, last)])


def rms_scale(values, scale_row):
    widened = values.astype(F32)
    return (
        widened * lax.rsqrt(jnp.mean(widened * widened, axis=-1, keepdims=True) + eps) * scale_row
    )


def dot_t(values, weights):
    return lax.dot_general(weights, values, (((0,), (1,)), ((), ())), preferred_element_type=F32)


def rotate_rows(values, cosine, sine):
    half = values.shape[-2] // 2
    leading = values[..., :half, :]
    trailing = values[..., half:, :]
    return jnp.concatenate(
        [leading * cosine - trailing * sine, trailing * cosine + leading * sine], axis=-2
    )


KEYS = 256
COLS = 512


def attention_kernel(
    place, key_ref, value_ref, query_ref, out_ref, key_rows, value_cols, query_full, best, total, acc
):
    z = place[0]
    j = place[1]
    blocks = key_ref.shape[0]
    groups = query_ref.shape[0]
    queries = groups * 128
    width = 2 * queries
    for b in range(blocks):
        key_rows[b * 128 : (b + 1) * 128, :] = key_ref[b].T
        value_cols[:, b * 128 : (b + 1) * 128] = value_ref[b]
    for h in range(2):
        for g in range(groups):
            at = slice(h * queries + g * 128, h * queries + (g + 1) * 128)
            query_full[h * 64 : (h + 1) * 64, at] = query_ref[g, h * 64 : (h + 1) * 64, :]
            query_full[(1 - h) * 64 : (2 - h) * 64, at] = jnp.zeros((64, 128), BF16)
            query_full[128:160, at] = query_ref[g, 128 + h * 32 : 160 + h * 32, :]
    best[...] = jnp.full(best.shape, LOW, F32)
    total[...] = jnp.zeros(total.shape, F32)
    acc[...] = jnp.zeros(acc.shape, F32)
    factor = SCALE * LOG2E

    def step(kb, masked):
        keys = key_rows[pl.ds(pl.multiple_of(kb * KEYS, KEYS), KEYS), :]

        def column(n, carry):
            first = pl.multiple_of(n * COLS, COLS)
            cols = pl.ds(first, COLS)
            scores = jnp.dot(keys, query_full[:, cols], preferred_element_type=F32)
            if masked:
                row = lax.broadcasted_iota(jnp.int32, (KEYS, 1), 0)
                key_at = (kb * (KEYS // 128) + row // 128) * queries + j * 128 + row % 128
                col = lax.broadcasted_iota(jnp.int32, (1, COLS), 1) + first
                query_at = z * queries + col % queries
                keep = key_at <= query_at
                scores = jnp.where(keep, scores, LOW)
            old = best[:, cols]
            new = jnp.maximum(old, jnp.max(scores, axis=0, keepdims=True))
            weights = jnp.exp2(scores * factor - new * factor)
            if masked:
                weights = jnp.where(keep, weights, 0.0)
            shrink = jnp.exp2((old - new) * factor)
            best[:, cols] = new
            total[:, cols] = total[:, cols] * shrink + jnp.sum(weights, axis=0, keepdims=True)
            head = first // queries
            values = value_cols[
                pl.ds(pl.multiple_of(head * 64, 64), 64),
                pl.ds(pl.multiple_of(kb * KEYS, KEYS), KEYS),
            ]
            acc[:, cols] = acc[:, cols] * shrink + jnp.dot(
                values, weights.astype(BF16), preferred_element_type=F32
            )
            return carry

        lax.fori_loop(0, width // COLS, column, 0)

    whole = z * 128 // KEYS

    def loop_body(kb, carry):
        step(kb, False)
        return carry

    lax.fori_loop(0, whole, loop_body, 0)
    step(whole, True)

    for h in range(2):
        span = slice(h * queries, (h + 1) * queries)
        sums = jnp.maximum(total[:, span], 1e-30)
        logsum = best[:, span] * SCALE + jnp.log(sums)
        part = logsum.astype(BF16)
        rest = logsum - part.astype(F32)
        middle = rest.astype(BF16)
        last = (rest - middle.astype(F32)).astype(BF16)
        mixed = (acc[:, span] / sums).astype(BF16)
        for g in range(groups):
            at = slice(g * 128, (g + 1) * 128)
            out_ref[g, h * 64 : (h + 1) * 64, :] = mixed[:, at]
            for i, piece in enumerate((part, middle, last)):
                out_ref[g, 128 + 16 * (2 * i + h) : 144 + 16 * (2 * i + h), :] = jnp.broadcast_to(
                    piece[:, at], (16, 128)
                )


OUT_ROWS = 224


def attend(place, keys, values, queries):
    blocks, groups = keys.shape[0], queries.shape[0]
    width = 2 * groups * 128
    vmem = pl.BlockSpec(memory_space=pltpu.VMEM)
    flops = 2 * blocks * 128 * width * (160 + 64)
    return pl.pallas_call(
        attention_kernel,
        out_shape=jax.ShapeDtypeStruct((groups, OUT_ROWS, 128), BF16),
        in_specs=[pl.BlockSpec(memory_space=pltpu.SMEM), vmem, vmem, vmem],
        out_specs=vmem,
        scratch_shapes=[
            pltpu.VMEM((blocks * 128, 160), BF16),
            pltpu.VMEM((128, blocks * 128), BF16),
            pltpu.VMEM((160, width), BF16),
            pltpu.VMEM((1, width), F32),
            pltpu.VMEM((1, width), F32),
            pltpu.VMEM((64, width), F32),
        ],
        cost_estimate=pl.CostEstimate(
            flops=flops, bytes_accessed=4_000_000, transcendentals=blocks * 128 * width
        ),
        name="attend",
    )(place, keys, values, queries)


def local(
    tokens,
    pre_gain,
    outer_gate,
    inner_gate,
    conv_input,
    conv_taps,
    query_down,
    latent_down,
    rotary_down,
    query_gain,
    latent_gain,
    query_up,
    query_rotary,
    key_up,
    value_up,
    conv_output,
    heads_output,
    post_gain,
):
    rows = tokens.shape[0]
    sp_index = lax.axis_index(SP)
    z = lax.axis_index("sp_0")
    j = lax.axis_index(GROUP)
    place = jnp.stack([z, j]).astype(jnp.int32)
    depth, channels = outer_gate.shape
    half = channels // 2

    gates = jnp.stack([outer_gate, inner_gate, conv_input], axis=1)
    gates = gates.reshape(depth, 3, 2, half).transpose(2, 0, 1, 3).reshape(2, depth, 3 * half)
    gates = exchange(gates, "sp_2").reshape(2 * depth, 3 * half)
    gates = copy_for_each(gates, "sp_0")
    gates = copy_for_each(gates, "sp_1")
    gates = gates.transpose(1, 0, 2, 3).reshape(-1, 3 * half)

    normed = rms_scale(tokens, pre_gain).astype(BF16)
    positions = sp_index * rows + jnp.arange(rows, dtype=jnp.int32)
    frequency = rope_theta ** (-jnp.arange(ROPE // 2, dtype=F32) / (ROPE // 2))
    angles = positions.astype(F32)[None, :] * frequency[:, None]
    cosine, sine = jnp.cos(angles), jnp.sin(angles)

    down = jnp.concatenate([latent_down, query_down], axis=1)
    latents = jnp.dot(normed, down, preferred_element_type=F32).astype(BF16)
    latents = copy_for_each(latents, "tp")
    n_latent = latent_down.shape[1]
    key_latent = jnp.moveaxis(latents[:, :, :n_latent], 0, 1).reshape(rows, -1)
    query_latent = jnp.moveaxis(latents[:, :, n_latent:], 0, 1).reshape(rows, -1)
    latent_normed = rms_scale(key_latent, latent_gain).astype(BF16)
    key_turned = rotate_rows(dot_t(normed, rotary_down), cosine, sine).astype(BF16)
    keys = jnp.concatenate([dot_t(latent_normed, key_up).astype(BF16), key_turned], axis=0)
    values = dot_t(latent_normed, value_up).astype(BF16)
    values = copy_for_each(values, "sp_0")
    query_normed = rms_scale(query_latent, query_gain).astype(BF16)
    query_nope = dot_t(query_normed, query_up).astype(BF16)
    turned = dot_t(query_normed, query_rotary).reshape(-1, ROPE, rows)
    turned = rotate_rows(turned, cosine, sine).astype(BF16).reshape(-1, rows)
    queries = copy_for_each(jnp.concatenate([query_nope, turned], axis=0), GROUP)
    keys = lax.all_gather(keys, "sp_0", axis=0, tiled=True).reshape(-1, *keys.shape)

    parts = attend(place, keys, values, queries)
    parts = exchange(parts, GROUP)

    other = lax.ppermute(gates, "sp_2", [(0, 1), (1, 0)])
    mine = jnp.dot(normed, gates, preferred_element_type=F32)
    other = jnp.dot(normed, other, preferred_element_type=F32)
    first_core = lax.axis_index("sp_2") == 0
    spread = [jnp.where(first_core, mine, other), jnp.where(first_core, other, mine)]
    outer_part, inner_part, signal = (
        jnp.concatenate([s[:, i * half : (i + 1) * half] for s in spread], axis=1) for i in range(3)
    )
    product = (inner_part * signal).astype(BF16)
    edge_rows = shifted(product[rows - (TAPS - 1) :], SP, 1)
    extended = jnp.concatenate([edge_rows, product], axis=0).astype(F32)
    convolved = extended[0:rows] * conv_taps[0]
    for offset in range(1, TAPS):
        convolved = convolved + extended[offset : offset + rows] * conv_taps[offset]
    conv_mixed = (outer_part * convolved).astype(BF16)
    conv_projected = jnp.dot(conv_mixed, conv_output, preferred_element_type=F32)

    groups = parts.shape[0]
    logs = parts[:, 128:].reshape(groups, 3, 2, 16, 128)[:, :, :, 0, :].astype(F32)
    logs = logs[:, 0] + (logs[:, 1] + logs[:, 2])
    top = jnp.max(logs, axis=0)
    share = jnp.exp(logs - top)
    share_sum = jnp.sum(share, axis=0)
    row_logsum = top + jnp.log(share_sum)
    share = share / share_sum
    mixed_parts = parts[:, :128].reshape(groups, 2, VDIM, 128).astype(F32)
    heads = jnp.sum(mixed_parts * share[:, :, None, :], axis=0).astype(BF16).reshape(-1, rows)
    heads_projected = lax.dot_general(
        heads, heads_output, (((0,), (0,)), ((), ())), preferred_element_type=F32
    )
    projected = (conv_projected + heads_projected).astype(BF16)
    tp = lax.axis_size("tp")
    arrived = exchange(projected.reshape(tp, rows // tp, -1), "tp")
    projected = arrived.astype(F32).sum(axis=0)
    mixed = rms_scale(projected, post_gain).astype(BF16)
    return (mixed, row_logsum)


def solution(mesh):
    split = Mesh(mesh.devices.reshape(16, 4, 2, mesh.shape["tp"]), ("sp_0", "sp_1", "sp_2", "tp"))
    return jax.shard_map(
        local,
        mesh=split,
        in_specs=(
            P(SP, None),
            P(),
            P(SP, "tp"),
            P(SP, "tp"),
            P(SP, "tp"),
            P(None, "tp"),
            P(None, "tp"),
            P(None, "tp"),
            P(),
            P(),
            P(),
            P(None, "tp"),
            P(None, "tp"),
            P(None, "tp"),
            P(None, "tp"),
            P("tp", None),
            P("tp", None),
            P(),
        ),
        out_specs=(P(SP_TP, None), P("tp", SP)),
        check_vma=False,
    )
```

time: 312 us -> 211 us (0.68)
  the two profiles are of different devices: /device:TPU:1 before, /device:TPU:384 now
where the time goes in v1:
time: 211 us; the launch traced here: 210 us
  blocking collectives  93.1 us (44%)
  waiting for transfers between devices  45 us (21%)
  starting transfers between devices  34.5 us (16%)
  Pallas kernels  17 us (8%)
  matrix products  7.98 us (4%)
  local copies, waits for them, and re-layouts  6.73 us (3%)
  other arithmetic  4.49 us (2%)
    all_gather x1, blocking collectives, local(): lax.all_gather(keys, 'sp_0', axis=0, tiled=True).reshape(-1, *keys.shape)  48.5 us
    all_to_all x2, blocking collectives, copy_for_each(): return lax.all_to_all(copies, axis, split_axis=0, concat_axis=0, tiled=True)  44.7 us
    all_to_all x3, waiting for transfers between devices, copy_for_each(): return lax.all_to_all(copies, axis, split_axis=0, concat_axis=0, tiled=True)  21.3 us
    all_to_all x3, starting transfers between devices, copy_for_each(): return lax.all_to_all(copies, axis, split_axis=0, concat_axis=0, tiled=True)  20.2 us
    all_to_all x3, waiting for transfers between devices, exchange(): return lax.all_to_all(array, axis, split_axis=0, concat_axis=0, tiled=True)  17.5 us
    pallas_call x1, Pallas kernels, attend(): pl.pallas_call(attention_kernel, out_shape=jax.ShapeDtypeStruct((groups,...  17 us
    all_to_all x3, starting transfers between devices, exchange(): return lax.all_to_all(array, axis, split_axis=0, concat_axis=0, tiled=True)  10.3 us
    ppermute x1, waiting for transfers between devices, shifted(): lax.ppermute(value, axis, [(source, source + steps) for source in range(f...  6.2 us
  transfers between devices with their start and end apart: 8, of which 6 were waited for; matrix products, arithmetic and copies ran while one was open for 4% of the time, Pallas kernels for 8%

profile of v1, /device:TPU:384, one launch (start us, length us, event | category | flops | bytes accessed | tf_op | source)
XLA Modules:
  0.0 210.1 jit_solution(2697964091488213512)
XLA Ops:
  0.7 1.4 fusion.11
  2.1 1.3 copy.32
  3.4 0.6 fusion.5
  4.0 0.8 broadcast_in_dim.12
  4.8 4.6 %all-to-all-start.3 = ((bf16[4,128,320]{1,2,0:T(8,128)(2,1)}), bf16[4,128,320]{1,2,0:T(8,128)(2,1)S(1)}, u32[]{:S(2)}, u32[]{:S(2)}) async-start(bf16[4,128,320]{1,2,0:T(8,128)(2,1)} %broadcast_in_dim.12), calls=%async_computation.3 | async-start | bytes 655360 | tf_op jit(solution)/shard_map/all_to_all | solution.py:31
  10.0 0.6 reshape.172
  10.7 6.0 %all-to-all-done.3 = bf16[4,128,320]{1,2,0:T(8,128)(2,1)S(1)} async-done(((bf16[4,128,320]{1,2,0:T(8,128)(2,1)}), bf16[4,128,320]{1,2,0:T(8,128)(2,1)S(1)}, u32[]{:S(2)}, u32[]{:S(2)}) %all-to-all-start.3) | async-done | bytes 327712 | tf_op jit(solution)/shard_map/all_to_all | solution.py:31
  16.7 3.2 %all-to-all-start = ((bf16[2,16,384]{2,1,0:T(8,128)(2,1)}), bf16[2,16,384]{2,1,0:T(8,128)(2,1)S(1)}, u32[]{:S(2)}, u32[]{:S(2)}) async-start(bf16[2,16,384]{2,1,0:T(8,128)(2,1)} %reshape.172), calls=%async_computation | async-start | bytes 49152 | tf_op jit(solution)/shard_map/all_to_all | solution.py:35
  21.4 13.1 %all_to_all.40.query_ref = bf16[8,192,128]{2,1,0:T(8,128)(2,1)} all-to-all(bf16[8,192,128]{2,1,0:T(8,128)(2,1)S(1)} %broadcast_in_dim.14), channel_id=1, replica_groups=mesh['sp_0'=16,'sp_1'=4,'sp_2'=2,'tp'=4] {'sp_1','sp_2'}, dimensions={0} | all-to-all | bytes 786432 | tf_op jit(solution)/shard_map/all_to_all | solution.py:31
  34.6 31.6 %all_to_all.41 = bf16[16,32,384]{2,1,0:T(8,128)(2,1)S(1)} all-to-all(bf16[16,32,384]{2,1,0:T(8,128)(2,1)S(1)} %broadcast_in_dim.10), channel_id=1, replica_groups=mesh['sp_0'=16,'sp_1'=4,'sp_2'=2,'tp'=4] {'sp_0'}, dimensions={0} | all-to-all | bytes 786432 | tf_op jit(solution)/shard_map/all_to_all | solution.py:31
  66.1 1.3 broadcast_in_dim.11
  67.5 3.7 %all-to-all-start.2 = ((bf16[4,16,32,384]{3,2,1,0:T(8,128)(2,1)}), bf16[4,16,32,384]{3,2,1,0:T(8,128)(2,1)S(1)}, u32[]{:S(2)}, u32[]{:S(2)}) async-start(bf16[4,16,32,384]{3,2,1,0:T(8,128)(2,1)} %broadcast_in_dim.11), calls=%async_computation.2 | async-start | bytes 3145728 | tf_op jit(solution)/shard_map/all_to_all | solution.py:31
  71.4 1.1 fusion.9
  72.7 15.3 %all-to-all-done.2 = bf16[4,16,32,384]{3,2,1,0:T(8,128)(2,1)S(1)} async-done(((bf16[4,16,32,384]{3,2,1,0:T(8,128)(2,1)}), bf16[4,16,32,384]{3,2,1,0:T(8,128)(2,1)S(1)}, u32[]{:S(2)}, u32[]{:S(2)}) %all-to-all-start.2) | async-done | bytes 1572896 | tf_op jit(solution)/shard_map/all_to_all | solution.py:31
  88.0 0.9 broadcast_in_dim.13
  88.9 11.9 %all-to-all-start.4 = ((bf16[16,128,128]{2,1,0:T(8,128)(2,1)}), bf16[16,128,128]{2,1,0:T(8,128)(2,1)}, u32[]{:S(2)}, u32[]{:S(2)}) async-start(bf16[16,128,128]{2,1,0:T(8,128)(2,1)} %broadcast_in_dim.13), calls=%async_computation.4 | async-start | bytes 1048576 | tf_op jit(solution)/shard_map/all_to_all | solution.py:31
  100.9 0.6 pad_add_fusion.place
  101.7 1.4 copy.31
  103.1 1.9 collective-permute-start
  105.0 48.5 %all_gather.3 = bf16[2560,128]{1,0:T(8,128)(2,1)} all-gather(bf16[160,128]{1,0:T(8,128)(2,1)S(1)} %pad_maximum_fusion.1), channel_id=1, replica_groups=mesh['sp_0'=16,'sp_1'=4,'sp_2'=2,'tp'=4] {'sp_0'}, dimensions={0}, use_global_device_ids=true | all-gather | bytes 696320 | tf_op jit(solution)/shard_map/all_gather | solution.py:237
  153.5 17.0 %attend.1 = bf16[8,224,128]{2,1,0:T(8,128)(2,1)} custom-call(s32[2]{0:T(128)} %pad_add_fusion.place, bf16[16,160,128]{2,1,0:T(8,128)(2,1)} %bitcast.69, bf16[16,128,128]{2,1,0:T(8,128)(2,1)} %all-to-all-done.4.value_ref, bf16[8,192,128]{2,1,0:T(8,128)(2,1)} %all_to_all.40.query_ref), custom_call_target="tpu_custom_call" | custom-call | flops 1879048192 | bytes 4000000 | tf_op jit(solution)/shard_map/attend/pallas_call | solution.py:160
  170.6 3.5 %all-to-all-start.6 = ((bf16[8,224,128]{2,1,0:T(8,128)(2,1)}), bf16[8,224,128]{2,1,0:T(8,128)(2,1)S(1)}, u32[]{:S(2)}, u32[]{:S(2)}) async-start(bf16[8,224,128]{2,1,0:T(8,128)(2,1)} %attend.1), calls=%async_computation.6 | async-start | bytes 917504 | tf_op jit(solution)/shard_map/all_to_all | solution.py:35
  174.1 9.5 %all-to-all-done.6 = bf16[8,224,128]{2,1,0:T(8,128)(2,1)S(1)} async-done(((bf16[8,224,128]{2,1,0:T(8,128)(2,1)}), bf16[8,224,128]{2,1,0:T(8,128)(2,1)S(1)}, u32[]{:S(2)}, u32[]{:S(2)}) %all-to-all-start.6) | async-done | bytes 458784 | tf_op jit(solution)/shard_map/all_to_all | solution.py:35
  183.7 1.9 fusion.40
  185.6 1.9 broadcast_select_fusion.1
  187.6 2.1 collective-permute-start.1
  189.7 6.2 %collective-permute-done.1 = bf16[2,256]{1,0:T(2,128)(2,1)S(1)} collective-permute-done((bf16[2,256]{1,0:T(2,128)(2,1)S(1)}, bf16[2,256]{1,0:T(2,128)(2,1)S(1)}, u32[]{:S(2)}, u32[]{:S(2)}) %collective-permute-start.1) | collective-permute-done | bytes 1056 | tf_op jit(solution)/shard_map/ppermute | solution.py:41
  196.3 1.1 fusion
  197.4 3.6 %all-to-all-start.7 = ((bf16[4,32,2048]{2,1,0:T(8,128)(2,1)}), bf16[4,32,2048]{2,1,0:T(8,128)(2,1)S(1)}, u32[]{:S(2)}, u32[]{:S(2)}) async-start(bf16[4,32,2048]{2,1,0:T(8,128)(2,1)} %bitcast.27), calls=%async_computation.7 | async-start | bytes 1048576 | tf_op jit(solution)/shard_map/all_to_all | solution.py:35
  201.0 0.6 log_add_fusion
  201.6 7.5 %all-to-all-done.7 = bf16[4,32,2048]{2,1,0:T(8,128)(2,1)S(1)} async-done(((bf16[4,32,2048]{2,1,0:T(8,128)(2,1)}), bf16[4,32,2048]{2,1,0:T(8,128)(2,1)S(1)}, u32[]{:S(2)}, u32[]{:S(2)}) %all-to-all-start.7) | async-done | bytes 524320 | tf_op jit(solution)/shard_map/all_to_all | solution.py:35
  209.3 0.8 multiply_convert_fusion
  (80 shorter events, 3.5 us)
Async XLA Ops:
  0.6 195.3 %copy-start = (bf16[256,2048]{1,0:T(8,128)(2,1)S(1)}, bf16[256,2048]{1,0:T(8,128)(2,1)}, u32[]{:S(2)}) copy-start(bf16[256,2048]{1,0:T(8,128)(2,1)} %param.33) | copy-start | bytes 3145732
  0.6 2.7 %copy-start.1 = (bf16[128,2048]{1,0:T(8,128)(2,1)S(1)}, bf16[128,2048]{1,0:T(8,128)(2,1)}, u32[]{:S(2)}) copy-start(bf16[128,2048]{1,0:T(8,128)(2,1)} %param.18) | copy-start | bytes 1572868
  0.7 2.7 %copy-start.6 = (f32[2048]{0:T(1024)S(1)}, f32[2048]{0:T(1024)}, u32[]{:S(2)}) copy-start(f32[2048]{0:T(1024)} %param.19) | copy-start | bytes 24580
  0.7 2.7 %copy-start.14 = (bf16[2048,192]{0,1:T(8,128)(2,1)S(1)}, bf16[2048,192]{0,1:T(8,128)(2,1)}, u32[]{:S(2)}) copy-start(bf16[2048,192]{0,1:T(8,128)(2,1)} %param.24) | copy-start | bytes 2359300
  3.4 6.0 %copy-start.8 = (bf16[16,256]{1,0:T(8,128)(2,1)S(1)}, bf16[16,256]{1,0:T(8,128)(2,1)}, u32[]{:S(2)}) copy-start(bf16[16,256]{1,0:T(8,128)(2,1)} %param.22) | copy-start | bytes 24580
  3.4 6.1 %copy-start.9 = (bf16[16,256]{1,0:T(8,128)(2,1)S(1)}, bf16[16,256]{1,0:T(8,128)(2,1)}, u32[]{:S(2)}) copy-start(bf16[16,256]{1,0:T(8,128)(2,1)} %param.21) | copy-start | bytes 24580
  3.4 6.1 %copy-start.10 = (bf16[16,256]{1,0:T(8,128)(2,1)S(1)}, bf16[16,256]{1,0:T(8,128)(2,1)}, u32[]{:S(2)}) copy-start(bf16[16,256]{1,0:T(8,128)(2,1)} %param.20) | copy-start | bytes 24580
  3.4 6.1 %copy-start.15 = (bf16[2048,32]{0,1:T(8,128)(2,1)S(1)}, bf16[2048,32]{0,1:T(8,128)(2,1)}, u32[]{:S(2)}) copy-start(bf16[2048,32]{0,1:T(8,128)(2,1)} %param.26) | copy-start | bytes 393220
  4.0 16.2 %copy-start.11 = (f32[768]{0:T(1024)S(1)}, f32[768]{0:T(1024)}, u32[]{:S(2)}) copy-start(f32[768]{0:T(1024)} %param.27) | copy-start | bytes 9220
  4.8 15.6 %copy-start.5 = (bf16[768,64]{0,1:T(8,128)(2,1)S(1)}, bf16[768,64]{0,1:T(8,128)(2,1)}, u32[]{:S(2)}) copy-start(bf16[768,64]{0,1:T(8,128)(2,1)} %param.30) | copy-start | bytes 294916
  4.8 12.0 %all-to-all-start.3 = ((bf16[4,128,320]{1,2,0:T(8,128)(2,1)}), bf16[4,128,320]{1,2,0:T(8,128)(2,1)S(1)}, u32[]{:S(2)}, u32[]{:S(2)}) async-start(bf16[4,128,320]{1,2,0:T(8,128)(2,1)} %broadcast_in_dim.12), calls=%async_computation.3 | async-start | bytes 655360 | tf_op jit(solution)/shard_map/all_to_all | solution.py:31
  9.4 11.2 %copy-start.3 = (bf16[768,128]{1,0:T(8,128)(2,1)S(1)}, bf16[768,128]{1,0:T(8,128)(2,1)}, u32[]{:S(2)}) copy-start(bf16[768,128]{1,0:T(8,128)(2,1)} %param.29) | copy-start | bytes 589828
  16.7 4.6 %all-to-all-start = ((bf16[2,16,384]{2,1,0:T(8,128)(2,1)}), bf16[2,16,384]{2,1,0:T(8,128)(2,1)S(1)}, u32[]{:S(2)}, u32[]{:S(2)}) async-start(bf16[2,16,384]{2,1,0:T(8,128)(2,1)} %reshape.172), calls=%async_computation | async-start | bytes 49152 | tf_op jit(solution)/shard_map/all_to_all | solution.py:35
  67.5 3.8 %copy-start.13 = (f32[512]{0:T(512)S(1)}, f32[512]{0:T(512)}, u32[]{:S(2)}) copy-start(f32[512]{0:T(512)} %param.28) | copy-start | bytes 6148
  67.5 20.6 %all-to-all-start.2 = ((bf16[4,16,32,384]{3,2,1,0:T(8,128)(2,1)}), bf16[4,16,32,384]{3,2,1,0:T(8,128)(2,1)S(1)}, u32[]{:S(2)}, u32[]{:S(2)}) async-start(bf16[4,16,32,384]{3,2,1,0:T(8,128)(2,1)} %broadcast_in_dim.11), calls=%async_computation.2 | async-start | bytes 3145728 | tf_op jit(solution)/shard_map/all_to_all | solution.py:31
  71.3 30.2 %copy-start.4 = (bf16[512,128]{1,0:T(8,128)(2,1)S(1)}, bf16[512,128]{1,0:T(8,128)(2,1)}, u32[]{:S(2)}) copy-start(bf16[512,128]{1,0:T(8,128)(2,1)} %param.31) | copy-start | bytes 393220
  88.9 64.6 %all-to-all-start.4 = ((bf16[16,128,128]{2,1,0:T(8,128)(2,1)}), bf16[16,128,128]{2,1,0:T(8,128)(2,1)}, u32[]{:S(2)}, u32[]{:S(2)}) async-start(bf16[16,128,128]{2,1,0:T(8,128)(2,1)} %broadcast_in_dim.13), calls=%async_computation.4 | async-start | bytes 1048576 | tf_op jit(solution)/shard_map/all_to_all | solution.py:31
  103.1 82.4 %collective-permute-start = (bf16[2048,384]{1,0:T(8,128)(2,1)}, bf16[2048,384]{1,0:T(8,128)(2,1)}, u32[]{:S(2)}, u32[]{:S(2)}) collective-permute-start(bf16[2048,384]{1,0:T(8,128)(2,1)} %bitcast.3), channel_id=1, source_target_pairs={{0,4},{4,0},{1,5},{5,1},{2,6},{6,2},{3,7},{7,3},{8,12},{12,8},{9,1... | collective-permute-start | bytes 4718600 | tf_op jit(solution)/shard_map/ppermute | solution.py:242
  153.5 20.5 %copy-start.12 = (f32[3,256]{1,0:T(4,128)S(1)}, f32[3,256]{1,0:T(4,128)}, u32[]{:S(2)}) copy-start(f32[3,256]{1,0:T(4,128)} %param.23) | copy-start | bytes 9220
  170.6 13.0 %all-to-all-start.6 = ((bf16[8,224,128]{2,1,0:T(8,128)(2,1)}), bf16[8,224,128]{2,1,0:T(8,128)(2,1)S(1)}, u32[]{:S(2)}, u32[]{:S(2)}) async-start(bf16[8,224,128]{2,1,0:T(8,128)(2,1)} %attend.1), calls=%async_computation.6 | async-start | bytes 917504 | tf_op jit(solution)/shard_map/all_to_all | solution.py:35
  187.5 8.8 %copy-start.2 = (bf16[128,2048]{1,0:T(8,128)(2,1)S(1)}, bf16[128,2048]{1,0:T(8,128)(2,1)}, u32[]{:S(2)}) copy-start(bf16[128,2048]{1,0:T(8,128)(2,1)} %param.34) | copy-start | bytes 1572868
  187.6 8.3 %collective-permute-start.1 = (bf16[2,256]{1,0:T(2,128)(2,1)S(1)}, bf16[2,256]{1,0:T(2,128)(2,1)S(1)}, u32[]{:S(2)}, u32[]{:S(2)}) collective-permute-start(bf16[2,256]{1,0:T(2,128)(2,1)S(1)} %slice.106), channel_id=1, source_target_pairs={{0,4},{4,8},{8,12},{12,16},{16,20},{20,24},{24,28},{28,32},{32,36}... | collective-permute-start | bytes 3080 | tf_op jit(solution)/shard_map/ppermute | solution.py:41
  197.4 11.9 %copy-start.7 = (f32[2048]{0:T(1024)S(1)}, f32[2048]{0:T(1024)}, u32[]{:S(2)}) copy-start(f32[2048]{0:T(1024)} %param.35) | copy-start | bytes 24580
  197.4 11.7 %all-to-all-start.7 = ((bf16[4,32,2048]{2,1,0:T(8,128)(2,1)}), bf16[4,32,2048]{2,1,0:T(8,128)(2,1)S(1)}, u32[]{:S(2)}, u32[]{:S(2)}) async-start(bf16[4,32,2048]{2,1,0:T(8,128)(2,1)} %bitcast.27), calls=%async_computation.7 | async-start | bytes 1048576 | tf_op jit(solution)/shard_map/all_to_all | solution.py:35

commit v2 on v1

--- a/solution.py
+++ b/solution.py
@@ -1,4 +1,3 @@
-import functools
 import math
 
 import jax
@@ -13,9 +12,10 @@
 ROPE = 32
 VDIM = 64
 TAPS = 3
-SP = ("sp_0", "sp_1", "sp_2")
-SP_TP = ("sp_0", "sp_1", "sp_2", "tp")
-GROUP = ("sp_1", "sp_2")
+SP = ("far", "pair", "x", "core")
+SP_TP = ("far", "pair", "x", "core", "tp")
+Z = ("far", "pair")
+GROUP = ("pair", "x", "core")
 
 eps = 1e-06
 rope_theta = 500000.0
@@ -31,6 +31,18 @@
     return lax.all_to_all(copies, axis, split_axis=0, concat_axis=0, tiled=True)
 
 
+def ring_gather(array, axis):
+    count, here = lax.axis_size(axis), lax.axis_index(axis)
+    whole = jnp.zeros((array.shape[0], count, *array.shape[1:]), array.dtype)
+    for k in range(count):
+        block = array
+        if k:
+            block = lax.ppermute(array, axis, [(i, (i + k) % count) for i in range(count)])
+        at = (0, (here + count - k) % count) + (0,) * (array.ndim - 1)
+        whole = lax.dynamic_update_slice(whole, block[:, None], at)
+    return whole
+
+
 def exchange(array, axis):
     return lax.all_to_all(array, axis, split_axis=0, concat_axis=0, tiled=True)
 
@@ -66,17 +78,17 @@
 
 
 def attention_kernel(
-    place, key_ref, value_ref, query_ref, out_ref, key_rows, value_cols, query_full, best, total, acc
+    place, held_ref, query_ref, out_ref, key_rows, value_cols, query_full, best, total, acc
 ):
     z = place[0]
     j = place[1]
-    blocks = key_ref.shape[0]
+    blocks = held_ref.shape[0]
     groups = query_ref.shape[0]
     queries = groups * 128
     width = 2 * queries
     for b in range(blocks):
-        key_rows[b * 128 : (b + 1) * 128, :] = key_ref[b].T
-        value_cols[:, b * 128 : (b + 1) * 128] = value_ref[b]
+        key_rows[b * 128 : (b + 1) * 128, :] = held_ref[b, 0:160, :].T
+        value_cols[:, b * 128 : (b + 1) * 128] = held_ref[b, 160:288, :]
     for h in range(2):
         for g in range(groups):
             at = slice(h * queries + g * 128, h * queries + (g + 1) * 128)
@@ -91,16 +103,15 @@
     def step(kb, masked):
         keys = key_rows[pl.ds(pl.multiple_of(kb * KEYS, KEYS), KEYS), :]
 
-        def column(n, carry):
-            first = pl.multiple_of(n * COLS, COLS)
-            cols = pl.ds(first, COLS)
+        for n in range(width // COLS):
+            first = n * COLS
+            cols = slice(first, first + COLS)
             scores = jnp.dot(keys, query_full[:, cols], preferred_element_type=F32)
             if masked:
                 row = lax.broadcasted_iota(jnp.int32, (KEYS, 1), 0)
                 key_at = (kb * (KEYS // 128) + row // 128) * queries + j * 128 + row % 128
-                col = lax.broadcasted_iota(jnp.int32, (1, COLS), 1) + first
-                query_at = z * queries + col % queries
-                keep = key_at <= query_at
+                col = lax.broadcasted_iota(jnp.int32, (1, COLS), 1) + first % queries
+                keep = key_at <= z * queries + col
                 scores = jnp.where(keep, scores, LOW)
             old = best[:, cols]
             new = jnp.maximum(old, jnp.max(scores, axis=0, keepdims=True))
@@ -112,15 +123,11 @@
             total[:, cols] = total[:, cols] * shrink + jnp.sum(weights, axis=0, keepdims=True)
             head = first // queries
             values = value_cols[
-                pl.ds(pl.multiple_of(head * 64, 64), 64),
-                pl.ds(pl.multiple_of(kb * KEYS, KEYS), KEYS),
+                head * 64 : (head + 1) * 64, pl.ds(pl.multiple_of(kb * KEYS, KEYS), KEYS)
             ]
             acc[:, cols] = acc[:, cols] * shrink + jnp.dot(
                 values, weights.astype(BF16), preferred_element_type=F32
             )
-            return carry
-
-        lax.fori_loop(0, width // COLS, column, 0)
 
     whole = z * 128 // KEYS
 
@@ -152,15 +159,15 @@
 OUT_ROWS = 224
 
 
-def attend(place, keys, values, queries):
-    blocks, groups = keys.shape[0], queries.shape[0]
+def attend(place, held, queries):
+    blocks, groups = held.shape[0], queries.shape[0]
     width = 2 * groups * 128
     vmem = pl.BlockSpec(memory_space=pltpu.VMEM)
     flops = 2 * blocks * 128 * width * (160 + 64)
     return pl.pallas_call(
         attention_kernel,
         out_shape=jax.ShapeDtypeStruct((groups, OUT_ROWS, 128), BF16),
-        in_specs=[pl.BlockSpec(memory_space=pltpu.SMEM), vmem, vmem, vmem],
+        in_specs=[pl.BlockSpec(memory_space=pltpu.SMEM), vmem, vmem],
         out_specs=vmem,
         scratch_shapes=[
             pltpu.VMEM((blocks * 128, 160), BF16),
@@ -174,10 +181,10 @@
             flops=flops, bytes_accessed=4_000_000, transcendentals=blocks * 128 * width
         ),
         name="attend",
-    )(place, keys, values, queries)
-
-
-def local(
+    )(place, held, queries)
+
+
+def layer(
     tokens,
     pre_gain,
     outer_gate,
@@ -199,54 +206,55 @@
 ):
     rows = tokens.shape[0]
     sp_index = lax.axis_index(SP)
-    z = lax.axis_index("sp_0")
-    j = lax.axis_index(GROUP)
-    place = jnp.stack([z, j]).astype(jnp.int32)
-    depth, channels = outer_gate.shape
-    half = channels // 2
-
-    gates = jnp.stack([outer_gate, inner_gate, conv_input], axis=1)
-    gates = gates.reshape(depth, 3, 2, half).transpose(2, 0, 1, 3).reshape(2, depth, 3 * half)
-    gates = exchange(gates, "sp_2").reshape(2 * depth, 3 * half)
-    gates = copy_for_each(gates, "sp_0")
-    gates = copy_for_each(gates, "sp_1")
-    gates = gates.transpose(1, 0, 2, 3).reshape(-1, 3 * half)
+    place = jnp.stack([lax.axis_index("far"), lax.axis_index(GROUP)]).astype(jnp.int32)
+    core = lax.axis_index("core")
+
+    gates = jnp.concatenate([outer_gate, inner_gate, conv_input], axis=1)
+    half = gates.shape[1] // 2
+    gates = lax.all_gather(gates, "core", axis=0, tiled=True)
+    gates = jnp.where(core == 0, gates[:, :half], gates[:, half:])
+    gates = copy_for_each(gates, Z)
+    gates = ring_gather(gates, "x").reshape(-1, half)
+    gates_other = lax.ppermute(gates, "core", [(0, 1), (1, 0)])
 
     normed = rms_scale(tokens, pre_gain).astype(BF16)
+    down = jnp.concatenate([latent_down, query_down], axis=1)
+    latents = jnp.dot(normed, down, preferred_element_type=F32).astype(BF16)
+    latents = lax.all_gather(latents, "tp", axis=0)
+
     positions = sp_index * rows + jnp.arange(rows, dtype=jnp.int32)
     frequency = rope_theta ** (-jnp.arange(ROPE // 2, dtype=F32) / (ROPE // 2))
     angles = positions.astype(F32)[None, :] * frequency[:, None]
     cosine, sine = jnp.cos(angles), jnp.sin(angles)
-
-    down = jnp.concatenate([latent_down, query_down], axis=1)
-    latents = jnp.dot(normed, down, preferred_element_type=F32).astype(BF16)
-    latents = copy_for_each(latents, "tp")
+    key_turned = rotate_rows(dot_t(normed, rotary_down), cosine, sine).astype(BF16)
+
     n_latent = latent_down.shape[1]
     key_latent = jnp.moveaxis(latents[:, :, :n_latent], 0, 1).reshape(rows, -1)
     query_latent = jnp.moveaxis(latents[:, :, n_latent:], 0, 1).reshape(rows, -1)
     latent_normed = rms_scale(key_latent, latent_gain).astype(BF16)
-    key_turned = rotate_rows(dot_t(normed, rotary_down), cosine, sine).astype(BF16)
-    keys = jnp.concatenate([dot_t(latent_normed, key_up).astype(BF16), key_turned], axis=0)
-    values = dot_t(latent_normed, value_up).astype(BF16)
-    values = copy_for_each(values, "sp_0")
     query_normed = rms_scale(query_latent, query_gain).astype(BF16)
     query_nope = dot_t(query_normed, query_up).astype(BF16)
     turned = dot_t(query_normed, query_rotary).reshape(-1, ROPE, rows)
     turned = rotate_rows(turned, cosine, sine).astype(BF16).reshape(-1, rows)
-    queries = copy_for_each(jnp.concatenate([query_nope, turned], axis=0), GROUP)
-    keys = lax.all_gather(keys, "sp_0", axis=0, tiled=True).reshape(-1, *keys.shape)
-
-    parts = attend(place, keys, values, queries)
+    queries = jnp.concatenate([query_nope, turned], axis=0)
+    queries = copy_for_each(queries, GROUP)
+    held = jnp.concatenate(
+        [
+            dot_t(latent_normed, key_up).astype(BF16),
+            key_turned,
+            dot_t(latent_normed, value_up).astype(BF16),
+        ],
+        axis=0,
+    )
+    held = lax.all_gather(held, "far", axis=0, tiled=True).reshape(-1, *held.shape)
+
+    parts = attend(place, held, queries)
     parts = exchange(parts, GROUP)
 
-    other = lax.ppermute(gates, "sp_2", [(0, 1), (1, 0)])
     mine = jnp.dot(normed, gates, preferred_element_type=F32)
-    other = jnp.dot(normed, other, preferred_element_type=F32)
-    first_core = lax.axis_index("sp_2") == 0
-    spread = [jnp.where(first_core, mine, other), jnp.where(first_core, other, mine)]
-    outer_part, inner_part, signal = (
-        jnp.concatenate([s[:, i * half : (i + 1) * half] for s in spread], axis=1) for i in range(3)
-    )
+    other = jnp.dot(normed, gates_other, preferred_element_type=F32)
+    spread = [jnp.where(core == 0, mine, other), jnp.where(core == 0, other, mine)]
+    outer_part, inner_part, signal = jnp.split(jnp.concatenate(spread, axis=1), 3, axis=1)
     product = (inner_part * signal).astype(BF16)
     edge_rows = shifted(product[rows - (TAPS - 1) :], SP, 1)
     extended = jnp.concatenate([edge_rows, product], axis=0).astype(F32)
@@ -278,9 +286,9 @@
 
 
 def solution(mesh):
-    split = Mesh(mesh.devices.reshape(16, 4, 2, mesh.shape["tp"]), ("sp_0", "sp_1", "sp_2", "tp"))
+    split = Mesh(mesh.devices.reshape(8, 2, 4, 2, mesh.shape["tp"]), SP_TP)
     return jax.shard_map(
-        local,
+        layer,
         mesh=split,
         in_specs=(
             P(SP, None),

time: 211 us -> 145 us (0.69)
  blocking collectives: 93.1 us -> 49.1 us
  waiting for transfers between devices: 45 us -> 23.6 us
  starting transfers between devices: 34.5 us -> 40.6 us
  matrix products: 7.98 us -> 4.28 us
    all_to_all x2 -> x0, blocking collectives: 44.7 us -> none  [copy_for_each(): return lax.all_to_all(copies, axis, split_axis=0, concat_axis=0, tiled=True)]
    all_to_all x3 -> x2, waiting for transfers between devices: 21.3 us -> 7.03 us  [copy_for_each(): return lax.all_to_all(copies, axis, split_axis=0, concat_axis=0, tiled=True)]
    ppermute x1 -> x4, starting transfers between devices: 1.91 us -> 14.1 us  [the longest x3 11.9 us: ring_gather(): lax.ppermute(array, axis, [(i, (i + k) % count) for i in range(count)])]
    all_to_all x3 -> x2, waiting for transfers between devices: 17.5 us -> 7.51 us  [exchange(): return lax.all_to_all(array, axis, split_axis=0, concat_axis=0, tiled=True)]
    all_to_all x3 -> x2, starting transfers between devices: 20.2 us -> 16 us  [copy_for_each(): return lax.all_to_all(copies, axis, split_axis=0, concat_axis=0, tiled=True)]
    dynamic_update_slice x0 -> x4, local copies, waits for them, and re-layouts: none -> 3.34 us  [ring_gather(): whole = lax.dynamic_update_slice(whole, block[:, None], at)]
    ppermute x1 -> x4, waiting for transfers between devices: 0.01 us -> 3.11 us  [the longest x1 3.1 us: layer(): gates_other = lax.ppermute(gates, 'core', [(0, 1), (1, 0)])]
    dot_general x5, matrix products: 5.85 us -> 3.03 us  [the longest x1 1.12 us: layer(): lax.dot_general(heads, heads_output, (((0,), (0,)), ((), ())), preferred_...]
  transfers between devices with their start and end apart: 8 -> 9, of which waited for: 6 -> 4; matrix products, arithmetic and copies ran while one was open for 4% -> 6% of each run, Pallas kernels for 8% -> 10%
where the time goes in v2:
time: 145 us; the launch traced here: 144 us
  blocking collectives  49.1 us (34%)
  starting transfers between devices  40.6 us (28%)
  waiting for transfers between devices  23.6 us (16%)
  Pallas kernels  15.1 us (10%)
  local copies, waits for them, and re-layouts  6.33 us (4%)
  other arithmetic  4.29 us (3%)
  matrix products  4.28 us (3%)
    all_gather x1, blocking collectives, layer(): lax.all_gather(held, 'far', axis=0, tiled=True).reshape(-1, *held.shape)  34.9 us
    all_to_all x2, starting transfers between devices, copy_for_each(): return lax.all_to_all(copies, axis, split_axis=0, concat_axis=0, tiled=True)  16 us
    pallas_call x1, Pallas kernels, attend(): pl.pallas_call(attention_kernel, out_shape=jax.ShapeDtypeStruct((groups,...  15.1 us
    all_gather x1, blocking collectives, layer(): latents = lax.all_gather(latents, 'tp', axis=0)  12.4 us
    ppermute x3, starting transfers between devices, ring_gather(): lax.ppermute(array, axis, [(i, (i + k) % count) for i in range(count)])  11.9 us
    all_to_all x2, starting transfers between devices, exchange(): return lax.all_to_all(array, axis, split_axis=0, concat_axis=0, tiled=True)  8.22 us
    all_to_all x2, waiting for transfers between devices, exchange(): return lax.all_to_all(array, axis, split_axis=0, concat_axis=0, tiled=True)  7.51 us
    all_to_all x2, waiting for transfers between devices, copy_for_each(): return lax.all_to_all(copies, axis, split_axis=0, concat_axis=0, tiled=True)  7.03 us
  transfers between devices with their start and end apart: 9, of which 4 were waited for; matrix products, arithmetic and copies ran while one was open for 6% of the time, Pallas kernels for 10%

profile of v2, /device:TPU:384, one launch (start us, length us, event | category | flops | bytes accessed | tf_op | source)
XLA Modules:
  0.0 144.5 jit_solution(10435333380263313223)
XLA Ops:
  0.7 0.9 pad_maximum_fusion.3
  1.6 1.8 %all_gather.12 = bf16[32,768]{1,0:T(8,128)(2,1)S(1)} all-gather(bf16[16,768]{1,0:T(8,128)(2,1)S(1)} %pad_maximum_fusion.3), channel_id=1, replica_groups=mesh['far'=8,'pair'=2,'x'=4,'core'=2,'tp'=4] {'core'}, dimensions={0}, use_global_device_ids=true | all-gather | bytes 73728 | tf_op jit(solution)/shard_map/all_gather | solution.py:214
  3.4 0.8 broadcast_in_dim.15
  4.2 10.2 %all-to-all-start = ((bf16[16,32,384]{2,1,0:T(8,128)(2,1)}), bf16[16,32,384]{2,1,0:T(8,128)(2,1)}, u32[]{:S(2)}, u32[]{:S(2)}) async-start(bf16[16,32,384]{2,1,0:T(8,128)(2,1)} %broadcast_in_dim.15), calls=%async_computation | async-start | bytes 786432 | tf_op jit(solution)/shard_map/all_to_all | solution.py:31
  14.9 0.6 fusion.5
  15.5 12.4 %all-gather = bf16[512,320]{0,1:T(8,128)(2,1)S(1)} all-gather(bf16[128,320]{0,1:T(8,128)(2,1)S(1)} %fusion.5), channel_id=2, replica_groups=mesh['far'=8,'pair'=2,'x'=4,'core'=2,'tp'=4] {'tp'}, dimensions={0}, use_global_device_ids=true | all-gather | bytes 409600 | tf_op jit(solution)/shard_map/all_gather | solution.py:223
  28.1 0.4 convolution_bitcast_fusion
  29.5 7.0 %all-to-all-done = bf16[16,32,384]{2,1,0:T(8,128)(2,1)} async-done(((bf16[16,32,384]{2,1,0:T(8,128)(2,1)}), bf16[16,32,384]{2,1,0:T(8,128)(2,1)}, u32[]{:S(2)}, u32[]{:S(2)}) %all-to-all-start) | async-done | bytes 393248 | tf_op jit(solution)/shard_map/all_to_all | solution.py:31
  36.5 1.0 broadcast_in_dim.20
  37.6 5.8 %all-to-all-start.1 = ((bf16[16,192,128]{2,1,0:T(8,128)(2,1)}), bf16[16,192,128]{2,1,0:T(8,128)(2,1)}, u32[]{:S(2)}, u32[]{:S(2)}) async-start(bf16[16,192,128]{2,1,0:T(8,128)(2,1)} %broadcast_in_dim.20), calls=%async_computation.1 | async-start | bytes 1572864 | tf_op jit(solution)/shard_map/all_to_all | solution.py:31
  44.2 3.8 %collective-permute-start = (bf16[16,32,384]{2,1,0:T(8,128)(2,1)}, bf16[16,32,384]{2,1,0:T(8,128)(2,1)S(1)}, u32[]{:S(2)}, u32[]{:S(2)}) collective-permute-start(bf16[16,32,384]{2,1,0:T(8,128)(2,1)} %all-to-all-done), channel_id=1, source_target_pairs={{0,8},{8,16},{16,24},{24,0},{1,9},{9,17},{17,25},{25,1},{2,10},{10... | collective-permute-start | bytes 1179656 | tf_op jit(solution)/shard_map/ppermute | solution.py:40
  48.0 34.9 %all_gather.15 = bf16[2304,128]{1,0:T(8,128)(2,1)} all-gather(bf16[288,128]{1,0:T(8,128)(2,1)S(1)} %pad_maximum_fusion.1), channel_id=1, replica_groups=mesh['far'=8,'pair'=2,'x'=4,'core'=2,'tp'=4] {'far'}, dimensions={0}, use_global_device_ids=true | all-gather | bytes 663552 | tf_op jit(solution)/shard_map/all_gather | solution.py:249
  82.9 0.7 pad_add_fusion.place
  83.6 4.9 %collective-permute-start.1 = (bf16[16,32,384]{2,1,0:T(8,128)(2,1)}, bf16[16,32,384]{2,1,0:T(8,128)(2,1)}, u32[]{:S(2)}, u32[]{:S(2)}) collective-permute-start(bf16[16,32,384]{2,1,0:T(8,128)(2,1)} %all-to-all-done), channel_id=1, source_target_pairs={{0,16},{8,24},{16,0},{24,8},{1,17},{9,25},{17,1},{25,9},{2,18},{10... | collective-permute-start | bytes 1179656 | tf_op jit(solution)/shard_map/ppermute | solution.py:40
  88.5 3.2 %collective-permute-start.2 = (bf16[16,32,384]{2,1,0:T(8,128)(2,1)}, bf16[16,32,384]{2,1,0:T(8,128)(2,1)}, u32[]{:S(2)}, u32[]{:S(2)}) collective-permute-start(bf16[16,32,384]{2,1,0:T(8,128)(2,1)} %all-to-all-done), channel_id=1, source_target_pairs={{0,24},{8,0},{16,8},{24,16},{1,25},{9,1},{17,9},{25,17},{2,26},{10... | collective-permute-start | bytes 1179656 | tf_op jit(solution)/shard_map/ppermute | solution.py:40
  91.9 1.1 bitcast_dynamic-update-slice_fusion.2
  93.1 15.1 %attend.1 = bf16[16,224,128]{2,1,0:T(8,128)(2,1)} custom-call(s32[2]{0:T(128)} %pad_add_fusion.place, bf16[8,288,128]{2,1,0:T(8,128)(2,1)} %bitcast.82, bf16[16,192,128]{2,1,0:T(8,128)(2,1)} %all-to-all-done.1.query_ref), custom_call_target="tpu_custom_call" | custom-call | flops 1879048192 | bytes 4000000 | tf_op jit(solution)/shard_map/attend/pallas_call | solution.py:167
  108.2 3.6 %all-to-all-start.2 = ((bf16[16,224,128]{2,1,0:T(8,128)(2,1)}), bf16[16,224,128]{2,1,0:T(8,128)(2,1)S(1)}, u32[]{:S(2)}, u32[]{:S(2)}) async-start(bf16[16,224,128]{2,1,0:T(8,128)(2,1)} %attend.1), calls=%async_computation.2 | async-start | bytes 1835008 | tf_op jit(solution)/shard_map/all_to_all | solution.py:47
  111.8 1.1 bitcast_dynamic-update-slice_fusion
  113.0 1.1 bitcast_dynamic-update-slice_fusion.3
  114.1 2.2 %collective-permute-start.3 = (bf16[2048,384]{1,0:T(8,128)(2,1)S(1)}, bf16[2048,384]{1,0:T(8,128)(2,1)S(1)}, u32[]{:S(2)}, u32[]{:S(2)}) collective-permute-start(bf16[2048,384]{1,0:T(8,128)(2,1)S(1)} %bitcast.80), channel_id=1, source_target_pairs={{0,4},{4,0},{1,5},{5,1},{2,6},{6,2},{3,7},{7,3},{8,12},{12,8},{9,1... | collective-permute-start | bytes 4718600 | tf_op jit(solution)/shard_map/ppermute | solution.py:218
  116.3 3.1 %collective-permute-done.3 = bf16[2048,384]{1,0:T(8,128)(2,1)S(1)} collective-permute-done((bf16[2048,384]{1,0:T(8,128)(2,1)S(1)}, bf16[2048,384]{1,0:T(8,128)(2,1)S(1)}, u32[]{:S(2)}, u32[]{:S(2)}) %collective-permute-start.3) | collective-permute-done | bytes 1572896 | tf_op jit(solution)/shard_map/ppermute | solution.py:218
  119.4 0.5 fusion.37
  119.9 0.5 broadcast_select_fusion.1
  120.4 2.2 %collective-permute-start.4 = (bf16[2,256]{1,0:T(2,128)(2,1)S(1)}, bf16[2,256]{1,0:T(2,128)(2,1)S(1)}, u32[]{:S(2)}, u32[]{:S(2)}) collective-permute-start(bf16[2,256]{1,0:T(2,128)(2,1)S(1)} %slice.86), channel_id=1, source_target_pairs={{0,4},{4,8},{8,12},{12,16},{16,20},{20,24},{24,28},{28,32},{32,36}... | collective-permute-start | bytes 3080 | tf_op jit(solution)/shard_map/ppermute | solution.py:53
  122.6 6.0 %collective-permute-done.4 = bf16[2,256]{1,0:T(2,128)(2,1)S(1)} collective-permute-done((bf16[2,256]{1,0:T(2,128)(2,1)S(1)}, bf16[2,256]{1,0:T(2,128)(2,1)S(1)}, u32[]{:S(2)}, u32[]{:S(2)}) %collective-permute-start.4) | collective-permute-done | bytes 1056 | tf_op jit(solution)/shard_map/ppermute | solution.py:53
  129.3 0.4 copy-done.4
  129.7 1.1 fusion
  130.8 4.6 %all-to-all-start.3 = ((bf16[4,32,2048]{2,1,0:T(8,128)(2,1)}), bf16[4,32,2048]{2,1,0:T(8,128)(2,1)S(1)}, u32[]{:S(2)}, u32[]{:S(2)}) async-start(bf16[4,32,2048]{2,1,0:T(8,128)(2,1)} %bitcast.30), calls=%async_computation.3 | async-start | bytes 1048576 | tf_op jit(solution)/shard_map/all_to_all | solution.py:47
  135.4 0.6 log_add_fusion
  136.0 7.5 %all-to-all-done.3 = bf16[4,32,2048]{2,1,0:T(8,128)(2,1)S(1)} async-done(((bf16[4,32,2048]{2,1,0:T(8,128)(2,1)}), bf16[4,32,2048]{2,1,0:T(8,128)(2,1)S(1)}, u32[]{:S(2)}, u32[]{:S(2)}) %all-to-all-start.3) | async-done | bytes 524320 | tf_op jit(solution)/shard_map/all_to_all | solution.py:47
  143.7 0.8 multiply_convert_fusion
  (78 shorter events, 3.5 us)
Async XLA Ops:
  0.6 128.0 %copy-start = (bf16[256,2048]{1,0:T(8,128)(2,1)S(1)}, bf16[256,2048]{1,0:T(8,128)(2,1)}, u32[]{:S(2)}) copy-start(bf16[256,2048]{1,0:T(8,128)(2,1)} %param.33) | copy-start | bytes 3145732
  0.6 13.8 %copy-start.1 = (bf16[128,2048]{1,0:T(8,128)(2,1)S(1)}, bf16[128,2048]{1,0:T(8,128)(2,1)}, u32[]{:S(2)}) copy-start(bf16[128,2048]{1,0:T(8,128)(2,1)} %param.18) | copy-start | bytes 1572868
  0.7 14.0 %copy-start.3 = (bf16[2048,128]{1,0:T(8,128)(2,1)S(1)}, bf16[2048,128]{1,0:T(8,128)(2,1)}, u32[]{:S(2)}) copy-start(bf16[2048,128]{1,0:T(8,128)(2,1)} %param.25) | copy-start | bytes 1572868
  0.7 14.2 %copy-start.9 = (f32[2048]{0:T(1024)S(1)}, f32[2048]{0:T(1024)}, u32[]{:S(2)}) copy-start(f32[2048]{0:T(1024)} %param.19) | copy-start | bytes 24580
  0.7 14.2 %copy-start.14 = (bf16[2048,192]{0,1:T(8,128)(2,1)S(1)}, bf16[2048,192]{0,1:T(8,128)(2,1)}, u32[]{:S(2)}) copy-start(bf16[2048,192]{0,1:T(8,128)(2,1)} %param.24) | copy-start | bytes 2359300
  4.2 32.3 %all-to-all-start = ((bf16[16,32,384]{2,1,0:T(8,128)(2,1)}), bf16[16,32,384]{2,1,0:T(8,128)(2,1)}, u32[]{:S(2)}, u32[]{:S(2)}) async-start(bf16[16,32,384]{2,1,0:T(8,128)(2,1)} %broadcast_in_dim.15), calls=%async_computation | async-start | bytes 786432 | tf_op jit(solution)/shard_map/all_to_all | solution.py:31
  14.9 13.1 %copy-start.15 = (bf16[2048,32]{0,1:T(8,128)(2,1)S(1)}, bf16[2048,32]{0,1:T(8,128)(2,1)}, u32[]{:S(2)}) copy-start(bf16[2048,32]{0,1:T(8,128)(2,1)} %param.26) | copy-start | bytes 393220
  15.5 13.3 %copy-start.11 = (f32[768]{0:T(1024)S(1)}, f32[768]{0:T(1024)}, u32[]{:S(2)}) copy-start(f32[768]{0:T(1024)} %param.27) | copy-start | bytes 9220
  28.0 1.0 copy-start.8
  28.0 1.2 copy-start.5
  29.5 14.1 %copy-start.13 = (f32[512]{0:T(512)S(1)}, f32[512]{0:T(512)}, u32[]{:S(2)}) copy-start(f32[512]{0:T(512)} %param.28) | copy-start | bytes 6148
  37.6 6.2 %copy-start.6 = (bf16[512,128]{1,0:T(8,128)(2,1)S(1)}, bf16[512,128]{1,0:T(8,128)(2,1)}, u32[]{:S(2)}) copy-start(bf16[512,128]{1,0:T(8,128)(2,1)} %param.32) | copy-start | bytes 393220
  37.6 6.4 %copy-start.7 = (bf16[512,128]{1,0:T(8,128)(2,1)S(1)}, bf16[512,128]{1,0:T(8,128)(2,1)}, u32[]{:S(2)}) copy-start(bf16[512,128]{1,0:T(8,128)(2,1)} %param.31) | copy-start | bytes 393220
  37.6 55.5 %all-to-all-start.1 = ((bf16[16,192,128]{2,1,0:T(8,128)(2,1)}), bf16[16,192,128]{2,1,0:T(8,128)(2,1)}, u32[]{:S(2)}, u32[]{:S(2)}) async-start(bf16[16,192,128]{2,1,0:T(8,128)(2,1)} %broadcast_in_dim.20), calls=%async_computation.1 | async-start | bytes 1572864 | tf_op jit(solution)/shard_map/all_to_all | solution.py:31
  44.2 48.8 %collective-permute-start = (bf16[16,32,384]{2,1,0:T(8,128)(2,1)}, bf16[16,32,384]{2,1,0:T(8,128)(2,1)S(1)}, u32[]{:S(2)}, u32[]{:S(2)}) collective-permute-start(bf16[16,32,384]{2,1,0:T(8,128)(2,1)} %all-to-all-done), channel_id=1, source_target_pairs={{0,8},{8,16},{16,24},{24,0},{1,9},{9,17},{17,25},{25,1},{2,10},{10... | collective-permute-start | bytes 1179656 | tf_op jit(solution)/shard_map/ppermute | solution.py:40
  83.6 28.3 %collective-permute-start.1 = (bf16[16,32,384]{2,1,0:T(8,128)(2,1)}, bf16[16,32,384]{2,1,0:T(8,128)(2,1)}, u32[]{:S(2)}, u32[]{:S(2)}) collective-permute-start(bf16[16,32,384]{2,1,0:T(8,128)(2,1)} %all-to-all-done), channel_id=1, source_target_pairs={{0,16},{8,24},{16,0},{24,8},{1,17},{9,25},{17,1},{25,9},{2,18},{10... | collective-permute-start | bytes 1179656 | tf_op jit(solution)/shard_map/ppermute | solution.py:40
  88.5 24.5 %collective-permute-start.2 = (bf16[16,32,384]{2,1,0:T(8,128)(2,1)}, bf16[16,32,384]{2,1,0:T(8,128)(2,1)}, u32[]{:S(2)}, u32[]{:S(2)}) collective-permute-start(bf16[16,32,384]{2,1,0:T(8,128)(2,1)} %all-to-all-done), channel_id=1, source_target_pairs={{0,24},{8,0},{16,8},{24,16},{1,25},{9,1},{17,9},{25,17},{2,26},{10... | collective-permute-start | bytes 1179656 | tf_op jit(solution)/shard_map/ppermute | solution.py:40
  108.2 20.8 %all-to-all-start.2 = ((bf16[16,224,128]{2,1,0:T(8,128)(2,1)}), bf16[16,224,128]{2,1,0:T(8,128)(2,1)S(1)}, u32[]{:S(2)}, u32[]{:S(2)}) async-start(bf16[16,224,128]{2,1,0:T(8,128)(2,1)} %attend.1), calls=%async_computation.2 | async-start | bytes 1835008 | tf_op jit(solution)/shard_map/all_to_all | solution.py:47
  111.8 7.6 %copy-start.2 = (bf16[128,2048]{1,0:T(8,128)(2,1)S(1)}, bf16[128,2048]{1,0:T(8,128)(2,1)}, u32[]{:S(2)}) copy-start(bf16[128,2048]{1,0:T(8,128)(2,1)} %param.18) | copy-start | bytes 1572868
  114.1 5.3 %collective-permute-start.3 = (bf16[2048,384]{1,0:T(8,128)(2,1)S(1)}, bf16[2048,384]{1,0:T(8,128)(2,1)S(1)}, u32[]{:S(2)}, u32[]{:S(2)}) collective-permute-start(bf16[2048,384]{1,0:T(8,128)(2,1)S(1)} %bitcast.80), channel_id=1, source_target_pairs={{0,4},{4,0},{1,5},{5,1},{2,6},{6,2},{3,7},{7,3},{8,12},{12,8},{9,1... | collective-permute-start | bytes 4718600 | tf_op jit(solution)/shard_map/ppermute | solution.py:218
  119.9 2.7 %copy-start.12 = (f32[3,256]{1,0:T(4,128)S(1)}, f32[3,256]{1,0:T(4,128)}, u32[]{:S(2)}) copy-start(f32[3,256]{1,0:T(4,128)} %param.23) | copy-start | bytes 9220
  120.4 8.2 %collective-permute-start.4 = (bf16[2,256]{1,0:T(2,128)(2,1)S(1)}, bf16[2,256]{1,0:T(2,128)(2,1)S(1)}, u32[]{:S(2)}, u32[]{:S(2)}) collective-permute-start(bf16[2,256]{1,0:T(2,128)(2,1)S(1)} %slice.86), channel_id=1, source_target_pairs={{0,4},{4,8},{8,12},{12,16},{16,20},{20,24},{24,28},{28,32},{32,36}... | collective-permute-start | bytes 3080 | tf_op jit(solution)/shard_map/ppermute | solution.py:53
  128.6 1.0 copy-start.4
  130.8 12.9 %copy-start.10 = (f32[2048]{0:T(1024)S(1)}, f32[2048]{0:T(1024)}, u32[]{:S(2)}) copy-start(f32[2048]{0:T(1024)} %param.35) | copy-start | bytes 24580
  130.8 12.7 %all-to-all-start.3 = ((bf16[4,32,2048]{2,1,0:T(8,128)(2,1)}), bf16[4,32,2048]{2,1,0:T(8,128)(2,1)S(1)}, u32[]{:S(2)}, u32[]{:S(2)}) async-start(bf16[4,32,2048]{2,1,0:T(8,128)(2,1)} %bitcast.30), calls=%async_computation.3 | async-start | bytes 1048576 | tf_op jit(solution)/shard_map/all_to_all | solution.py:47

commit v3 on v2

--- a/solution.py
+++ b/solution.py
@@ -31,16 +31,10 @@
     return lax.all_to_all(copies, axis, split_axis=0, concat_axis=0, tiled=True)
 
 
-def ring_gather(array, axis):
-    count, here = lax.axis_size(axis), lax.axis_index(axis)
-    whole = jnp.zeros((array.shape[0], count, *array.shape[1:]), array.dtype)
-    for k in range(count):
-        block = array
-        if k:
-            block = lax.ppermute(array, axis, [(i, (i + k) % count) for i in range(count)])
-        at = (0, (here + count - k) % count) + (0,) * (array.ndim - 1)
-        whole = lax.dynamic_update_slice(whole, block[:, None], at)
-    return whole
+def weight_rows(joint, depth, wide, cores):
+    rows = joint[:, 2 * QUERY_ROWS :].reshape(wide, cores, -1, 6, depth, 128)
+    rows = rows.transpose(2, 0, 1, 4, 3, 5)
+    return rows.reshape(-1, 6 * 128)
 
 
 def exchange(array, axis):
@@ -74,6 +68,7 @@
 
 
 KEYS = 256
+QUERY_ROWS = 192
 COLS = 512
 
 
@@ -83,7 +78,8 @@
     z = place[0]
     j = place[1]
     blocks = held_ref.shape[0]
-    groups = query_ref.shape[0]
+    near = query_ref.shape[0]
+    groups = 2 * near
     queries = groups * 128
     width = 2 * queries
     for b in range(blocks):
@@ -92,9 +88,14 @@
     for h in range(2):
         for g in range(groups):
             at = slice(h * queries + g * 128, h * queries + (g + 1) * 128)
-            query_full[h * 64 : (h + 1) * 64, at] = query_ref[g, h * 64 : (h + 1) * 64, :]
+            from_row = g // near * QUERY_ROWS
+            query_full[h * 64 : (h + 1) * 64, at] = query_ref[
+                g % near, from_row + h * 64 : from_row + (h + 1) * 64, :
+            ]
             query_full[(1 - h) * 64 : (2 - h) * 64, at] = jnp.zeros((64, 128), BF16)
-            query_full[128:160, at] = query_ref[g, 128 + h * 32 : 160 + h * 32, :]
+            query_full[128:160, at] = query_ref[
+                g % near, from_row + 128 + h * 32 : from_row + 160 + h * 32, :
+            ]
     best[...] = jnp.full(best.shape, LOW, F32)
     total[...] = jnp.zeros(total.shape, F32)
     acc[...] = jnp.zeros(acc.shape, F32)
@@ -159,16 +160,20 @@
 OUT_ROWS = 224
 
 
-def attend(place, held, queries):
-    blocks, groups = held.shape[0], queries.shape[0]
+def attend(place, held, joint):
+    blocks, groups = held.shape[0], 2 * joint.shape[0]
     width = 2 * groups * 128
-    vmem = pl.BlockSpec(memory_space=pltpu.VMEM)
     flops = 2 * blocks * 128 * width * (160 + 64)
     return pl.pallas_call(
         attention_kernel,
         out_shape=jax.ShapeDtypeStruct((groups, OUT_ROWS, 128), BF16),
-        in_specs=[pl.BlockSpec(memory_space=pltpu.SMEM), vmem, vmem],
-        out_specs=vmem,
+        grid=(1,),
+        in_specs=[
+            pl.BlockSpec(memory_space=pltpu.SMEM),
+            pl.BlockSpec(held.shape, lambda i: (0, 0, 0)),
+            pl.BlockSpec((groups // 2, 2 * QUERY_ROWS, 128), lambda i: (0, 0, 0)),
+        ],
+        out_specs=pl.BlockSpec((groups, OUT_ROWS, 128), lambda i: (0, 0, 0)),
         scratch_shapes=[
             pltpu.VMEM((blocks * 128, 160), BF16),
             pltpu.VMEM((128, blocks * 128), BF16),
@@ -181,7 +186,7 @@
             flops=flops, bytes_accessed=4_000_000, transcendentals=blocks * 128 * width
         ),
         name="attend",
-    )(place, held, queries)
+    )(place, held, joint)
 
 
 def layer(
@@ -209,13 +214,10 @@
     place = jnp.stack([lax.axis_index("far"), lax.axis_index(GROUP)]).astype(jnp.int32)
     core = lax.axis_index("core")
 
+    depth = outer_gate.shape[0]
     gates = jnp.concatenate([outer_gate, inner_gate, conv_input], axis=1)
-    half = gates.shape[1] // 2
-    gates = lax.all_gather(gates, "core", axis=0, tiled=True)
-    gates = jnp.where(core == 0, gates[:, :half], gates[:, half:])
+    gates = gates.reshape(depth, -1, 128).swapaxes(0, 1).reshape(-1, 128)
     gates = copy_for_each(gates, Z)
-    gates = ring_gather(gates, "x").reshape(-1, half)
-    gates_other = lax.ppermute(gates, "core", [(0, 1), (1, 0)])
 
     normed = rms_scale(tokens, pre_gain).astype(BF16)
     down = jnp.concatenate([latent_down, query_down], axis=1)
@@ -237,7 +239,19 @@
     turned = dot_t(query_normed, query_rotary).reshape(-1, ROPE, rows)
     turned = rotate_rows(turned, cosine, sine).astype(BF16).reshape(-1, rows)
     queries = jnp.concatenate([query_nope, turned], axis=0)
-    queries = copy_for_each(queries, GROUP)
+    queries_other = lax.ppermute(queries, "pair", [(0, 1), (1, 0)])
+    first_of_pair = lax.axis_index("pair") == 0
+    both = [
+        jnp.where(first_of_pair, queries, queries_other),
+        jnp.where(first_of_pair, queries_other, queries),
+    ]
+    _, wide, cores = (lax.axis_size(name) for name in GROUP)
+    halves = gates.reshape(cores, -1, 128)
+    both = jnp.broadcast_to(jnp.concatenate(both, axis=0), (wide, cores, 2 * QUERY_ROWS, 128))
+    halves = jnp.broadcast_to(halves, (wide, *halves.shape))
+    sent = jnp.concatenate([both, halves], axis=2)
+    joint = exchange(sent.reshape(-1, *sent.shape[2:]), GROUP[1:])
+    joint_other = lax.ppermute(joint, "core", [(0, 1), (1, 0)])
     held = jnp.concatenate(
         [
             dot_t(latent_normed, key_up).astype(BF16),
@@ -248,13 +262,14 @@
     )
     held = lax.all_gather(held, "far", axis=0, tiled=True).reshape(-1, *held.shape)
 
-    parts = attend(place, held, queries)
+    parts = attend(place, held, joint)
     parts = exchange(parts, GROUP)
 
-    mine = jnp.dot(normed, gates, preferred_element_type=F32)
-    other = jnp.dot(normed, gates_other, preferred_element_type=F32)
-    spread = [jnp.where(core == 0, mine, other), jnp.where(core == 0, other, mine)]
-    outer_part, inner_part, signal = jnp.split(jnp.concatenate(spread, axis=1), 3, axis=1)
+    mine, other = (weight_rows(whole, depth, wide, cores) for whole in (joint, joint_other))
+    low, high = jnp.split(normed, 2, axis=1)
+    spread = jnp.dot(jnp.where(core == 0, low, high), mine, preferred_element_type=F32)
+    spread += jnp.dot(jnp.where(core == 0, high, low), other, preferred_element_type=F32)
+    outer_part, inner_part, signal = jnp.split(spread, 3, axis=1)
     product = (inner_part * signal).astype(BF16)
     edge_rows = shifted(product[rows - (TAPS - 1) :], SP, 1)
     extended = jnp.concatenate([edge_rows, product], axis=0).astype(F32)

time: 145 us -> 137 us (0.945)
  starting transfers between devices: 40.6 us -> 30.7 us
  waiting for transfers between devices: 23.6 us -> 19 us
  other arithmetic: 4.29 us -> 8.14 us
  local copies, waits for them, and re-layouts: 6.33 us -> 8.84 us
  blocking collectives: 49.1 us -> 46.8 us
  matrix products: 4.28 us -> 6.15 us
    ppermute x4 -> x2, starting transfers between devices: 14.1 us -> 4.37 us  [the longest x1 2.46 us: layer(): queries_other = lax.ppermute(queries, 'pair', [(0, 1), (1, 0)])]
    all_to_all x2 -> x1, waiting for transfers between devices: 7.03 us -> 0.01 us  [copy_for_each(): return lax.all_to_all(copies, axis, split_axis=0, concat_axis=0, tiled=True)]
    all_to_all x2 -> x1, starting transfers between devices: 16 us -> 10.2 us  [copy_for_each(): return lax.all_to_all(copies, axis, split_axis=0, concat_axis=0, tiled=True)]
    all_to_all x2 -> x3, starting transfers between devices: 8.22 us -> 13.8 us  [exchange(): return lax.all_to_all(array, axis, split_axis=0, concat_axis=0, tiled=True)]
    dynamic_update_slice x4 -> x0, local copies, waits for them, and re-layouts: 3.34 us -> none  [ring_gather(): whole = lax.dynamic_update_slice(whole, block[:, None], at)]
    slice x0 -> x2, local copies, waits for them, and re-layouts: none -> 3.06 us  [weight_rows(): rows = joint[:, 2 * QUERY_ROWS:].reshape(wide, cores, -1, 6, depth, 128)]
    all_to_all x2 -> x3, waiting for transfers between devices: 7.51 us -> 9.55 us  [exchange(): return lax.all_to_all(array, axis, split_axis=0, concat_axis=0, tiled=True)]
    all_gather x1 -> x0, blocking collectives: 1.83 us -> none  [layer(): gates = lax.all_gather(gates, 'core', axis=0, tiled=True)]
  transfers between devices with their start and end apart: 9 -> 7, of which waited for: 4 -> 4; matrix products, arithmetic and copies ran while one was open for 6% -> 10% of each run, Pallas kernels for 10% -> 11%
where the time goes in v3:
time: 137 us; the launch traced here: 136 us
  blocking collectives  46.8 us (34%)
  starting transfers between devices  30.7 us (22%)
  waiting for transfers between devices  19 us (14%)
  Pallas kernels  15.1 us (11%)
  local copies, waits for them, and re-layouts  8.84 us (6%)
  other arithmetic  8.14 us (6%)
  matrix products  6.15 us (4%)
    all_gather x1, blocking collectives, layer(): lax.all_gather(held, 'far', axis=0, tiled=True).reshape(-1, *held.shape)  34.2 us
    pallas_call x1, Pallas kernels, attend(): pl.pallas_call(attention_kernel, out_shape=jax.ShapeDtypeStruct((groups,...  15.1 us
    all_to_all x3, starting transfers between devices, exchange(): return lax.all_to_all(array, axis, split_axis=0, concat_axis=0, tiled=True)  13.8 us
    all_gather x1, blocking collectives, layer(): latents = lax.all_gather(latents, 'tp', axis=0)  12.6 us
    all_to_all x1, starting transfers between devices, copy_for_each(): return lax.all_to_all(copies, axis, split_axis=0, concat_axis=0, tiled=True)  10.2 us
    all_to_all x3, waiting for transfers between devices, exchange(): return lax.all_to_all(array, axis, split_axis=0, concat_axis=0, tiled=True)  9.55 us
    ppermute x1, waiting for transfers between devices, shifted(): lax.ppermute(value, axis, [(source, source + steps) for source in range(f...  5.93 us
    ppermute x1, waiting for transfers between devices, layer(): queries_other = lax.ppermute(queries, 'pair', [(0, 1), (1, 0)])  3.52 us
  transfers between devices with their start and end apart: 7, of which 4 were waited for; matrix products, arithmetic and copies ran while one was open for 10% of the time, Pallas kernels for 11%

profile of v3, /device:TPU:384, one launch (start us, length us, event | category | flops | bytes accessed | tf_op | source)
XLA Modules:
  0.0 136.0 jit_solution(2132910385950690171)
XLA Ops:
  0.7 0.9 pad_maximum_fusion.4
  1.6 0.8 broadcast_in_dim.7
  2.4 10.2 %all-to-all-start = ((bf16[16,96,128]{2,1,0:T(8,128)(2,1)}), bf16[16,96,128]{2,1,0:T(8,128)(2,1)S(1)}, u32[]{:S(2)}, u32[]{:S(2)}) async-start(bf16[16,96,128]{2,1,0:T(8,128)(2,1)} %broadcast_in_dim.7), calls=%async_computation | async-start | bytes 786432 | tf_op jit(solution)/shard_map/all_to_all | solution.py:31
  12.6 1.2 fusion.20
  14.3 1.9 %fusion.14 = bf16[128,320]{0,1:T(8,128)(2,1)S(1)} fusion(bf16[128,2048]{1,0:T(8,128)(2,1)S(1)} %fusion.22, bf16[2048,192]{0,1:T(8,128)(2,1)} %param.24, bf16[2048,128]{0,1:T(8,128)(2,1)S(1)} %copy.21), kind=kOutput, calls=%fused_computation.16 | convolution fusion | flops 170434560 | bytes 1916928 | tf_op jit(solution)/shard_map/dot_general | solution.py:224
  16.2 12.6 %all-gather = bf16[512,320]{0,1:T(8,128)(2,1)S(1)} all-gather(bf16[128,320]{0,1:T(8,128)(2,1)S(1)} %fusion.14), channel_id=2, replica_groups=mesh['far'=8,'pair'=2,'x'=4,'core'=2,'tp'=4] {'tp'}, dimensions={0}, use_global_device_ids=true | all-gather | bytes 409600 | tf_op jit(solution)/shard_map/all_gather | solution.py:225
  29.0 0.6 copy-done.5
  30.9 2.5 %collective-permute-start = (bf16[192,128]{1,0:T(8,128)(2,1)S(1)}, bf16[192,128]{1,0:T(8,128)(2,1)S(1)}, u32[]{:S(2)}, u32[]{:S(2)}) collective-permute-start(bf16[192,128]{1,0:T(8,128)(2,1)S(1)} %pad_maximum_fusion.3), channel_id=1, source_target_pairs={{0,32},{32,0},{1,33},{33,1},{2,34},{34,2},{3,35},{35,3},{4,36},{36... | collective-permute-start | bytes 147464 | tf_op jit(solution)/shard_map/ppermute | solution.py:242
  33.4 3.5 %collective-permute-done = bf16[192,128]{1,0:T(8,128)(2,1)S(1)} collective-permute-done((bf16[192,128]{1,0:T(8,128)(2,1)S(1)}, bf16[192,128]{1,0:T(8,128)(2,1)S(1)}, u32[]{:S(2)}, u32[]{:S(2)}) %collective-permute-start) | collective-permute-done | bytes 49184 | tf_op jit(solution)/shard_map/ppermute | solution.py:242
  37.3 1.6 %pad_maximum_fusion = bf16[4,2,1152,128]{3,2,1,0:T(8,128)(2,1)} fusion(bf16[4,2,768,128]{3,2,1,0:T(8,128)(2,1)S(1)} %broadcast_in_dim.8, bf16[4,2,384,128]{3,2,1,0:T(8,128)(2,1)S(1)} %broadcast_in_dim.6), kind=kLoop, calls=%fused_computation.2 | loop fusion | flops 4718592 | bytes 4718592 | tf_op jit(solution)/shard_map/concatenate | solution.py:252
  38.9 4.4 %all-to-all-start.1 = ((bf16[8,1152,128]{2,1,0:T(8,128)(2,1)}), bf16[8,1152,128]{2,1,0:T(8,128)(2,1)S(1)}, u32[]{:S(2)}, u32[]{:S(2)}) async-start(bf16[8,1152,128]{2,1,0:T(8,128)(2,1)} %bitcast.10), calls=%async_computation.1 | async-start | bytes 4718592 | tf_op jit(solution)/shard_map/all_to_all | solution.py:41
  43.3 0.9 slice.93
  44.2 0.6 pad_add_fusion.place
  45.4 1.1 fusion.17
  46.6 34.2 %all_gather.11 = bf16[2304,128]{1,0:T(8,128)(2,1)} all-gather(bf16[288,128]{1,0:T(8,128)(2,1)S(1)} %pad_maximum_fusion.2), channel_id=1, replica_groups=mesh['far'=8,'pair'=2,'x'=4,'core'=2,'tp'=4] {'far'}, dimensions={0}, use_global_device_ids=true | all-gather | bytes 663552 | tf_op jit(solution)/shard_map/all_gather | solution.py:263
  80.8 1.9 %collective-permute-start.1 = (bf16[8,1152,128]{2,1,0:T(8,128)(2,1)S(1)}, bf16[8,1152,128]{2,1,0:T(8,128)(2,1)}, u32[]{:S(2)}, u32[]{:S(2)}) collective-permute-start(bf16[8,1152,128]{2,1,0:T(8,128)(2,1)S(1)} %all-to-all-done.1.query_ref), channel_id=1, source_target_pairs={{0,4},{4,0},{1,5},{5,1},{2,6},{6,2},{3,7},{7,3},{8,12},{12,8},{9,1... | collective-permute-start | bytes 7077896 | tf_op jit(solution)/shard_map/ppermute | solution.py:254
  82.7 15.1 %attend.1 = bf16[16,224,128]{2,1,0:T(8,128)(2,1)} custom-call(s32[2]{0:T(128)} %pad_add_fusion.place, bf16[8,288,128]{2,1,0:T(8,128)(2,1)} %bitcast.90, bf16[8,1152,128]{2,1,0:T(8,128)(2,1)} %copy-done.1), custom_call_target="tpu_custom_call" | custom-call | flops 1879048192 | bytes 4000000 | tf_op jit(solution)/shard_map/attend/pallas_call | solution.py:167
  97.8 5.0 %all-to-all-start.2 = ((bf16[16,224,128]{2,1,0:T(8,128)(2,1)}), bf16[16,224,128]{2,1,0:T(8,128)(2,1)}, u32[]{:S(2)}, u32[]{:S(2)}) async-start(bf16[16,224,128]{2,1,0:T(8,128)(2,1)} %attend.1), calls=%async_computation.2 | async-start | bytes 1835008 | tf_op jit(solution)/shard_map/all_to_all | solution.py:41
  102.8 1.5 %slice.87 = bf16[8,768,128]{2,1,0:T(8,128)(2,1)S(1)} slice(bf16[8,1152,128]{2,1,0:T(8,128)(2,1)} %copy-done.1), slice={[0:8], [384:1152], [0:128]} | slice | bytes 3145728 | tf_op jit(solution)/shard_map/slice | solution.py:35
  104.4 0.5 copy.24
  105.8 1.5 %slice.88 = bf16[8,768,128]{2,1,0:T(8,128)(2,1)S(1)} slice(bf16[8,1152,128]{2,1,0:T(8,128)(2,1)} %collective-permute-done.1), slice={[0:8], [384:1152], [0:128]} | slice | bytes 3145728 | tf_op jit(solution)/shard_map/slice | solution.py:35
  107.3 0.5 copy.25
  108.3 2.4 %collective-permute-start.2 = (bf16[2,256]{1,0:T(2,128)(2,1)S(1)}, bf16[2,256]{1,0:T(2,128)(2,1)S(1)}, u32[]{:S(2)}, u32[]{:S(2)}) collective-permute-start(bf16[2,256]{1,0:T(2,128)(2,1)S(1)} %slice.89), channel_id=1, source_target_pairs={{0,4},{4,8},{8,12},{12,16},{16,20},{20,24},{24,28},{28,32},{32,36}... | collective-permute-start | bytes 3080 | tf_op jit(solution)/shard_map/ppermute | solution.py:47
  110.8 5.9 %collective-permute-done.2 = bf16[2,256]{1,0:T(2,128)(2,1)S(1)} collective-permute-done((bf16[2,256]{1,0:T(2,128)(2,1)S(1)}, bf16[2,256]{1,0:T(2,128)(2,1)S(1)}, u32[]{:S(2)}, u32[]{:S(2)}) %collective-permute-start.2) | collective-permute-done | bytes 1056 | tf_op jit(solution)/shard_map/ppermute | solution.py:47
  117.1 0.9 all-to-all-done.2
  118.0 1.0 slice.97
  119.2 1.2 fusion.23
  120.3 1.1 fusion
  121.5 4.3 %all-to-all-start.3 = ((bf16[4,32,2048]{2,1,0:T(8,128)(2,1)}), bf16[4,32,2048]{2,1,0:T(8,128)(2,1)S(1)}, u32[]{:S(2)}, u32[]{:S(2)}) async-start(bf16[4,32,2048]{2,1,0:T(8,128)(2,1)} %bitcast.30), calls=%async_computation.3 | async-start | bytes 1048576 | tf_op jit(solution)/shard_map/all_to_all | solution.py:41
  125.8 0.6 log_add_fusion
  126.4 8.6 %all-to-all-done.3 = bf16[4,32,2048]{2,1,0:T(8,128)(2,1)S(1)} async-done(((bf16[4,32,2048]{2,1,0:T(8,128)(2,1)}), bf16[4,32,2048]{2,1,0:T(8,128)(2,1)S(1)}, u32[]{:S(2)}, u32[]{:S(2)}) %all-to-all-start.3) | async-done | bytes 524320 | tf_op jit(solution)/shard_map/all_to_all | solution.py:41
  135.2 0.8 multiply_convert_fusion
  (80 shorter events, 4.7 us)
Async XLA Ops:
  0.6 116.1 %copy-start = (bf16[256,2048]{1,0:T(8,128)(2,1)S(1)}, bf16[256,2048]{1,0:T(8,128)(2,1)}, u32[]{:S(2)}) copy-start(bf16[256,2048]{1,0:T(8,128)(2,1)} %param.33) | copy-start | bytes 3145732
  0.6 13.5 %copy-start.2 = (bf16[128,2048]{1,0:T(8,128)(2,1)S(1)}, bf16[128,2048]{1,0:T(8,128)(2,1)}, u32[]{:S(2)}) copy-start(bf16[128,2048]{1,0:T(8,128)(2,1)} %param.18) | copy-start | bytes 1572868
  0.7 13.2 %copy-start.6 = (bf16[2048,128]{1,0:T(8,128)(2,1)S(1)}, bf16[2048,128]{1,0:T(8,128)(2,1)}, u32[]{:S(2)}) copy-start(bf16[2048,128]{1,0:T(8,128)(2,1)} %param.25) | copy-start | bytes 1572868
  0.7 13.4 %copy-start.12 = (f32[2048]{0:T(1024)S(1)}, f32[2048]{0:T(1024)}, u32[]{:S(2)}) copy-start(f32[2048]{0:T(1024)} %param.19) | copy-start | bytes 24580
  2.4 34.5 %all-to-all-start = ((bf16[16,96,128]{2,1,0:T(8,128)(2,1)}), bf16[16,96,128]{2,1,0:T(8,128)(2,1)S(1)}, u32[]{:S(2)}, u32[]{:S(2)}) async-start(bf16[16,96,128]{2,1,0:T(8,128)(2,1)} %broadcast_in_dim.7), calls=%async_computation | async-start | bytes 786432 | tf_op jit(solution)/shard_map/all_to_all | solution.py:31
  14.3 15.5 %copy-start.3 = (bf16[128,2048]{1,0:T(8,128)(2,1)}, bf16[128,2048]{1,0:T(8,128)(2,1)S(1)}, u32[]{:S(2)}) copy-start(bf16[128,2048]{1,0:T(8,128)(2,1)S(1)} %fusion.22) | copy-start | bytes 1572868
  14.3 15.5 %copy-start.10 = (bf16[2048,32]{0,1:T(8,128)(2,1)S(1)}, bf16[2048,32]{0,1:T(8,128)(2,1)}, u32[]{:S(2)}) copy-start(bf16[2048,32]{0,1:T(8,128)(2,1)} %param.26) | copy-start | bytes 393220
  16.2 13.9 %copy-start.14 = (f32[768]{0:T(1024)S(1)}, f32[768]{0:T(1024)}, u32[]{:S(2)}) copy-start(f32[768]{0:T(1024)} %param.27) | copy-start | bytes 9220
  16.2 14.2 %copy-start.11 = (bf16[768,64]{0,1:T(8,128)(2,1)S(1)}, bf16[768,64]{0,1:T(8,128)(2,1)}, u32[]{:S(2)}) copy-start(bf16[768,64]{0,1:T(8,128)(2,1)} %param.30) | copy-start | bytes 294916
  16.2 14.4 %copy-start.8 = (bf16[768,128]{1,0:T(8,128)(2,1)S(1)}, bf16[768,128]{1,0:T(8,128)(2,1)}, u32[]{:S(2)}) copy-start(bf16[768,128]{1,0:T(8,128)(2,1)} %param.29) | copy-start | bytes 589828
  28.9 0.7 copy-start.5
  30.9 6.0 %collective-permute-start = (bf16[192,128]{1,0:T(8,128)(2,1)S(1)}, bf16[192,128]{1,0:T(8,128)(2,1)S(1)}, u32[]{:S(2)}, u32[]{:S(2)}) collective-permute-start(bf16[192,128]{1,0:T(8,128)(2,1)S(1)} %pad_maximum_fusion.3), channel_id=1, source_target_pairs={{0,32},{32,0},{1,33},{33,1},{2,34},{34,2},{3,35},{35,3},{4,36},{36... | collective-permute-start | bytes 147464 | tf_op jit(solution)/shard_map/ppermute | solution.py:242
  38.8 6.2 %copy-start.16 = (f32[512]{0:T(512)S(1)}, f32[512]{0:T(512)}, u32[]{:S(2)}) copy-start(f32[512]{0:T(512)} %param.28) | copy-start | bytes 6148
  38.8 6.3 %copy-start.9 = (bf16[512,128]{1,0:T(8,128)(2,1)S(1)}, bf16[512,128]{1,0:T(8,128)(2,1)}, u32[]{:S(2)}) copy-start(bf16[512,128]{1,0:T(8,128)(2,1)} %param.32) | copy-start | bytes 393220
  38.9 41.9 %all-to-all-start.1 = ((bf16[8,1152,128]{2,1,0:T(8,128)(2,1)}), bf16[8,1152,128]{2,1,0:T(8,128)(2,1)S(1)}, u32[]{:S(2)}, u32[]{:S(2)}) async-start(bf16[8,1152,128]{2,1,0:T(8,128)(2,1)} %bitcast.10), calls=%async_computation.1 | async-start | bytes 4718592 | tf_op jit(solution)/shard_map/all_to_all | solution.py:41
  80.8 1.9 %copy-start.1 = (bf16[8,1152,128]{2,1,0:T(8,128)(2,1)}, bf16[8,1152,128]{2,1,0:T(8,128)(2,1)S(1)}, u32[]{:S(2)}) copy-start(bf16[8,1152,128]{2,1,0:T(8,128)(2,1)S(1)} %all-to-all-done.1.query_ref) | copy-start | bytes 7077892
  80.8 25.0 %collective-permute-start.1 = (bf16[8,1152,128]{2,1,0:T(8,128)(2,1)S(1)}, bf16[8,1152,128]{2,1,0:T(8,128)(2,1)}, u32[]{:S(2)}, u32[]{:S(2)}) collective-permute-start(bf16[8,1152,128]{2,1,0:T(8,128)(2,1)S(1)} %all-to-all-done.1.query_ref), channel_id=1, source_target_pairs={{0,4},{4,0},{1,5},{5,1},{2,6},{6,2},{3,7},{7,3},{8,12},{12,8},{9,1... | collective-permute-start | bytes 7077896 | tf_op jit(solution)/shard_map/ppermute | solution.py:254
  97.8 20.2 %all-to-all-start.2 = ((bf16[16,224,128]{2,1,0:T(8,128)(2,1)}), bf16[16,224,128]{2,1,0:T(8,128)(2,1)}, u32[]{:S(2)}, u32[]{:S(2)}) async-start(bf16[16,224,128]{2,1,0:T(8,128)(2,1)} %attend.1), calls=%async_computation.2 | async-start | bytes 1835008 | tf_op jit(solution)/shard_map/all_to_all | solution.py:41
  104.3 1.0 copy-start.4
  107.9 2.9 %copy-start.15 = (f32[3,256]{1,0:T(4,128)S(1)}, f32[3,256]{1,0:T(4,128)}, u32[]{:S(2)}) copy-start(f32[3,256]{1,0:T(4,128)} %param.23) | copy-start | bytes 9220
  108.3 12.0 %copy-start.7 = (bf16[128,2048]{1,0:T(8,128)(2,1)S(1)}, bf16[128,2048]{1,0:T(8,128)(2,1)}, u32[]{:S(2)}) copy-start(bf16[128,2048]{1,0:T(8,128)(2,1)} %param.34) | copy-start | bytes 1572868
  108.3 8.4 %collective-permute-start.2 = (bf16[2,256]{1,0:T(2,128)(2,1)S(1)}, bf16[2,256]{1,0:T(2,128)(2,1)S(1)}, u32[]{:S(2)}, u32[]{:S(2)}) collective-permute-start(bf16[2,256]{1,0:T(2,128)(2,1)S(1)} %slice.89), channel_id=1, source_target_pairs={{0,4},{4,8},{8,12},{12,16},{16,20},{20,24},{24,28},{28,32},{32,36}... | collective-permute-start | bytes 3080 | tf_op jit(solution)/shard_map/ppermute | solution.py:47
  120.3 14.9 %copy-start.13 = (f32[2048]{0:T(1024)S(1)}, f32[2048]{0:T(1024)}, u32[]{:S(2)}) copy-start(f32[2048]{0:T(1024)} %param.35) | copy-start | bytes 24580
  121.5 13.5 %all-to-all-start.3 = ((bf16[4,32,2048]{2,1,0:T(8,128)(2,1)}), bf16[4,32,2048]{2,1,0:T(8,128)(2,1)S(1)}, u32[]{:S(2)}, u32[]{:S(2)}) async-start(bf16[4,32,2048]{2,1,0:T(8,128)(2,1)} %bitcast.30), calls=%async_computation.3 | async-start | bytes 1048576 | tf_op jit(solution)/shard_map/all_to_all | solution.py:41

commit v4 on v3

--- a/solution.py
+++ b/solution.py
@@ -67,123 +67,104 @@
     )
 
 
-KEYS = 256
+COLS = 256
 QUERY_ROWS = 192
-COLS = 512
-
-
-def attention_kernel(
-    place, held_ref, query_ref, out_ref, key_rows, value_cols, query_full, best, total, acc
-):
-    z = place[0]
-    j = place[1]
+PART_ROWS = 144
+FLOOR = -1e29
+
+
+def attention_kernel(place, held_ref, query_ref, out_ref, key_rows, value_cols, query_full):
+    far, here = place[0], place[1]
     blocks = held_ref.shape[0]
     near = query_ref.shape[0]
     groups = 2 * near
     queries = groups * 128
-    width = 2 * queries
     for b in range(blocks):
         key_rows[b * 128 : (b + 1) * 128, :] = held_ref[b, 0:160, :].T
         value_cols[:, b * 128 : (b + 1) * 128] = held_ref[b, 160:288, :]
     for h in range(2):
         for g in range(groups):
             at = slice(h * queries + g * 128, h * queries + (g + 1) * 128)
-            from_row = g // near * QUERY_ROWS
+            first = g // near * QUERY_ROWS
             query_full[h * 64 : (h + 1) * 64, at] = query_ref[
-                g % near, from_row + h * 64 : from_row + (h + 1) * 64, :
+                g % near, first + h * 64 : first + (h + 1) * 64, :
             ]
             query_full[(1 - h) * 64 : (2 - h) * 64, at] = jnp.zeros((64, 128), BF16)
             query_full[128:160, at] = query_ref[
-                g % near, from_row + 128 + h * 32 : from_row + 160 + h * 32, :
+                g % near, first + 128 + h * 32 : first + 160 + h * 32, :
             ]
-    best[...] = jnp.full(best.shape, LOW, F32)
-    total[...] = jnp.zeros(total.shape, F32)
-    acc[...] = jnp.zeros(acc.shape, F32)
     factor = SCALE * LOG2E
-
-    def step(kb, masked):
-        keys = key_rows[pl.ds(pl.multiple_of(kb * KEYS, KEYS), KEYS), :]
-
-        for n in range(width // COLS):
-            first = n * COLS
-            cols = slice(first, first + COLS)
-            scores = jnp.dot(keys, query_full[:, cols], preferred_element_type=F32)
-            if masked:
-                row = lax.broadcasted_iota(jnp.int32, (KEYS, 1), 0)
-                key_at = (kb * (KEYS // 128) + row // 128) * queries + j * 128 + row % 128
-                col = lax.broadcasted_iota(jnp.int32, (1, COLS), 1) + first % queries
-                keep = key_at <= z * queries + col
-                scores = jnp.where(keep, scores, LOW)
-            old = best[:, cols]
-            new = jnp.maximum(old, jnp.max(scores, axis=0, keepdims=True))
-            weights = jnp.exp2(scores * factor - new * factor)
-            if masked:
-                weights = jnp.where(keep, weights, 0.0)
-            shrink = jnp.exp2((old - new) * factor)
-            best[:, cols] = new
-            total[:, cols] = total[:, cols] * shrink + jnp.sum(weights, axis=0, keepdims=True)
-            head = first // queries
-            values = value_cols[
-                head * 64 : (head + 1) * 64, pl.ds(pl.multiple_of(kb * KEYS, KEYS), KEYS)
-            ]
-            acc[:, cols] = acc[:, cols] * shrink + jnp.dot(
-                values, weights.astype(BF16), preferred_element_type=F32
-            )
-
-    whole = z * 128 // KEYS
-
-    def loop_body(kb, carry):
-        step(kb, False)
-        return carry
-
-    lax.fori_loop(0, whole, loop_body, 0)
-    step(whole, True)
-
-    for h in range(2):
-        span = slice(h * queries, (h + 1) * queries)
-        sums = jnp.maximum(total[:, span], 1e-30)
-        logsum = best[:, span] * SCALE + jnp.log(sums)
-        part = logsum.astype(BF16)
-        rest = logsum - part.astype(F32)
-        middle = rest.astype(BF16)
-        last = (rest - middle.astype(F32)).astype(BF16)
-        mixed = (acc[:, span] / sums).astype(BF16)
-        for g in range(groups):
-            at = slice(g * 128, (g + 1) * 128)
+    row = lax.broadcasted_iota(jnp.int32, (blocks * 128, 1), 0)
+    key_at = row // 128 * queries + here * 128 + row % 128 - far * queries
+
+    def score(first):
+        return jnp.dot(
+            key_rows[...], query_full[:, first : first + COLS], preferred_element_type=F32
+        )
+
+    def soften(first, scores):
+        col = lax.broadcasted_iota(jnp.int32, (1, COLS), 1) + first % queries
+        scores = jnp.where(key_at <= col, scores, LOW)
+        best = jnp.maximum(jnp.max(scores, axis=0, keepdims=True), FLOOR)
+        weights = jnp.exp2(scores * factor - best * factor)
+        total = jnp.maximum(jnp.sum(weights, axis=0, keepdims=True), 1e-30)
+        return weights.astype(BF16), total, best * SCALE + jnp.log(total)
+
+    logs = {}
+
+    def mix(first, weights, total, logsum):
+        h = first // queries
+        mixed = jnp.dot(
+            value_cols[h * 64 : (h + 1) * 64, :], weights, preferred_element_type=F32
+        )
+        mixed = (mixed * (1.0 / total)).astype(BF16)
+        high = logsum.astype(BF16).astype(F32)
+        middle = (logsum - high).astype(BF16).astype(F32)
+        low = logsum - high - middle
+        tail = jnp.concatenate([high, middle, low, jnp.zeros((5, COLS), F32)], axis=0)
+        for i in range(COLS // 128):
+            g = first % queries // 128 + i
+            at = slice(i * 128, (i + 1) * 128)
             out_ref[g, h * 64 : (h + 1) * 64, :] = mixed[:, at]
-            for i, piece in enumerate((part, middle, last)):
-                out_ref[g, 128 + 16 * (2 * i + h) : 144 + 16 * (2 * i + h), :] = jnp.broadcast_to(
-                    piece[:, at], (16, 128)
-                )
-
-
-OUT_ROWS = 224
+            if h == 0:
+                logs[g] = tail[:, at]
+            else:
+                both = jnp.concatenate([logs.pop(g), tail[:, at]], axis=0)
+                out_ref[g, 128:PART_ROWS, :] = both.astype(BF16)
+
+    tiles = 2 * queries // COLS
+    scores, softened = {}, {}
+    for n in range(tiles + 2):
+        if 0 <= n - 1 < tiles:
+            softened[n - 1] = soften((n - 1) * COLS, scores.pop(n - 1))
+        if n < tiles:
+            scores[n] = score(n * COLS)
+        if 0 <= n - 2 < tiles:
+            mix((n - 2) * COLS, *softened.pop(n - 2))
 
 
 def attend(place, held, joint):
     blocks, groups = held.shape[0], 2 * joint.shape[0]
     width = 2 * groups * 128
-    flops = 2 * blocks * 128 * width * (160 + 64)
     return pl.pallas_call(
         attention_kernel,
-        out_shape=jax.ShapeDtypeStruct((groups, OUT_ROWS, 128), BF16),
+        out_shape=jax.ShapeDtypeStruct((groups, PART_ROWS, 128), BF16),
         grid=(1,),
         in_specs=[
             pl.BlockSpec(memory_space=pltpu.SMEM),
             pl.BlockSpec(held.shape, lambda i: (0, 0, 0)),
             pl.BlockSpec((groups // 2, 2 * QUERY_ROWS, 128), lambda i: (0, 0, 0)),
         ],
-        out_specs=pl.BlockSpec((groups, OUT_ROWS, 128), lambda i: (0, 0, 0)),
+        out_specs=pl.BlockSpec((groups, PART_ROWS, 128), lambda i: (0, 0, 0)),
         scratch_shapes=[
             pltpu.VMEM((blocks * 128, 160), BF16),
             pltpu.VMEM((128, blocks * 128), BF16),
             pltpu.VMEM((160, width), BF16),
-            pltpu.VMEM((1, width), F32),
-            pltpu.VMEM((1, width), F32),
-            pltpu.VMEM((64, width), F32),
         ],
         cost_estimate=pl.CostEstimate(
-            flops=flops, bytes_accessed=4_000_000, transcendentals=blocks * 128 * width
+            flops=2 * blocks * 128 * width * (160 + 64),
+            bytes_accessed=2_000_000,
+            transcendentals=blocks * 128 * width,
         ),
         name="attend",
     )(place, held, joint)
@@ -218,6 +199,8 @@
     gates = jnp.concatenate([outer_gate, inner_gate, conv_input], axis=1)
     gates = gates.reshape(depth, -1, 128).swapaxes(0, 1).reshape(-1, 128)
     gates = copy_for_each(gates, Z)
+
+    edge = shifted(tokens[rows - (TAPS - 1) :], SP, 1)
 
     normed = rms_scale(tokens, pre_gain).astype(BF16)
     down = jnp.concatenate([latent_down, query_down], axis=1)
@@ -266,22 +249,24 @@
     parts = exchange(parts, GROUP)
 
     mine, other = (weight_rows(whole, depth, wide, cores) for whole in (joint, joint_other))
-    low, high = jnp.split(normed, 2, axis=1)
+    lead = 16
+    edge = jnp.pad(edge, ((lead - (TAPS - 1), 0), (0, 0)))
+    edge = rms_scale(edge, pre_gain).astype(BF16)
+    low, high = jnp.split(jnp.concatenate([edge, normed], axis=0), 2, axis=1)
     spread = jnp.dot(jnp.where(core == 0, low, high), mine, preferred_element_type=F32)
     spread += jnp.dot(jnp.where(core == 0, high, low), other, preferred_element_type=F32)
     outer_part, inner_part, signal = jnp.split(spread, 3, axis=1)
-    product = (inner_part * signal).astype(BF16)
-    edge_rows = shifted(product[rows - (TAPS - 1) :], SP, 1)
-    extended = jnp.concatenate([edge_rows, product], axis=0).astype(F32)
-    convolved = extended[0:rows] * conv_taps[0]
-    for offset in range(1, TAPS):
-        convolved = convolved + extended[offset : offset + rows] * conv_taps[offset]
-    conv_mixed = (outer_part * convolved).astype(BF16)
+    product = (inner_part * signal).astype(BF16).astype(F32)
+    convolved = sum(
+        product[lead - (TAPS - 1) + k : lead - (TAPS - 1) + k + rows] * conv_taps[k]
+        for k in range(TAPS)
+    )
+    conv_mixed = (outer_part[lead:] * convolved).astype(BF16)
     conv_projected = jnp.dot(conv_mixed, conv_output, preferred_element_type=F32)
 
     groups = parts.shape[0]
-    logs = parts[:, 128:].reshape(groups, 3, 2, 16, 128)[:, :, :, 0, :].astype(F32)
-    logs = logs[:, 0] + (logs[:, 1] + logs[:, 2])
+    logs = parts[:, 128:].reshape(groups, 2, 8, 128)[:, :, :3].astype(F32)
+    logs = logs[:, :, 0] + (logs[:, :, 1] + logs[:, :, 2])
     top = jnp.max(logs, axis=0)
     share = jnp.exp(logs - top)
     share_sum = jnp.sum(share, axis=0)

time: 137 us -> 136 us (level)
  the two profiles are of different devices: /device:TPU:384 before, /device:TPU:32 now
where the time goes in v4:
time: 136 us; the launch traced here: 135 us
  blocking collectives  48.6 us (36%)
  starting transfers between devices  35.4 us (26%)
  waiting for transfers between devices  16 us (12%)
  local copies, waits for them, and re-layouts  10.7 us (8%)
  Pallas kernels  9.4 us (7%)
  other arithmetic  7.93 us (6%)
  matrix products  6.21 us (5%)
    all_gather x1, blocking collectives, layer(): lax.all_gather(held, 'far', axis=0, tiled=True).reshape(-1, *held.shape)  36 us
    all_to_all x1, starting transfers between devices, copy_for_each(): return lax.all_to_all(copies, axis, split_axis=0, concat_axis=0, tiled=True)  15.2 us
    all_to_all x3, starting transfers between devices, exchange(): return lax.all_to_all(array, axis, split_axis=0, concat_axis=0, tiled=True)  13.6 us
    all_gather x1, blocking collectives, layer(): latents = lax.all_gather(latents, 'tp', axis=0)  12.6 us
    pallas_call x1, Pallas kernels, attend(): pl.pallas_call(attention_kernel, out_shape=jax.ShapeDtypeStruct((groups,...  9.4 us
    all_to_all x3, waiting for transfers between devices, exchange(): return lax.all_to_all(array, axis, split_axis=0, concat_axis=0, tiled=True)  7.52 us
    ppermute x1, waiting for transfers between devices, shifted(): lax.ppermute(value, axis, [(source, source + steps) for source in range(f...  4.65 us
    ppermute x1, waiting for transfers between devices, layer(): queries_other = lax.ppermute(queries, 'pair', [(0, 1), (1, 0)])  3.85 us
  transfers between devices with their start and end apart: 7, of which 3 were waited for; matrix products, arithmetic and copies ran while one was open for 10% of the time, Pallas kernels for 0%

profile of v4, /device:TPU:32, one launch (start us, length us, event | category | flops | bytes accessed | tf_op | source)
XLA Modules:
  0.0 135.4 jit_solution(569784916221153348)
XLA Ops:
  0.7 0.9 pad_maximum_fusion.7
  1.6 0.8 broadcast_in_dim.7
  2.4 15.2 %all-to-all-start = ((bf16[16,96,128]{2,1,0:T(8,128)(2,1)}), bf16[16,96,128]{2,1,0:T(8,128)(2,1)S(1)}, u32[]{:S(2)}, u32[]{:S(2)}) async-start(bf16[16,96,128]{2,1,0:T(8,128)(2,1)} %broadcast_in_dim.7), calls=%async_computation | async-start | bytes 786432 | tf_op jit(solution)/shard_map/all_to_all | solution.py:31
  17.6 1.2 fusion.20
  19.3 1.9 %fusion.14 = bf16[128,320]{0,1:T(8,128)(2,1)S(1)} fusion(bf16[128,2048]{1,0:T(8,128)(2,1)S(1)} %fusion.22, bf16[2048,192]{0,1:T(8,128)(2,1)} %param.24, bf16[2048,128]{0,1:T(8,128)(2,1)S(1)} %copy.21), kind=kOutput, calls=%fused_computation.16 | convolution fusion | flops 170434560 | bytes 1916928 | tf_op jit(solution)/shard_map/dot_general | solution.py:207
  21.2 12.6 %all-gather = bf16[512,320]{0,1:T(8,128)(2,1)S(1)} all-gather(bf16[128,320]{0,1:T(8,128)(2,1)S(1)} %fusion.14), channel_id=2, replica_groups=mesh['far'=8,'pair'=2,'x'=4,'core'=2,'tp'=4] {'tp'}, dimensions={0}, use_global_device_ids=true | all-gather | bytes 409600 | tf_op jit(solution)/shard_map/all_gather | solution.py:208
  34.0 0.6 copy-done.5
  35.9 2.1 %collective-permute-start.1 = (bf16[192,128]{1,0:T(8,128)(2,1)S(1)}, bf16[192,128]{1,0:T(8,128)(2,1)S(1)}, u32[]{:S(2)}, u32[]{:S(2)}) collective-permute-start(bf16[192,128]{1,0:T(8,128)(2,1)S(1)} %pad_maximum_fusion.4), channel_id=1, source_target_pairs={{0,32},{32,0},{1,33},{33,1},{2,34},{34,2},{3,35},{35,3},{4,36},{36... | collective-permute-start | bytes 147464 | tf_op jit(solution)/shard_map/ppermute | solution.py:225
  38.1 3.9 %collective-permute-done.1 = bf16[192,128]{1,0:T(8,128)(2,1)S(1)} collective-permute-done((bf16[192,128]{1,0:T(8,128)(2,1)S(1)}, bf16[192,128]{1,0:T(8,128)(2,1)S(1)}, u32[]{:S(2)}, u32[]{:S(2)}) %collective-permute-start.1) | collective-permute-done | bytes 49184 | tf_op jit(solution)/shard_map/ppermute | solution.py:225
  42.3 1.6 %pad_maximum_fusion = bf16[4,2,1152,128]{3,2,1,0:T(8,128)(2,1)} fusion(bf16[4,2,768,128]{3,2,1,0:T(8,128)(2,1)S(1)} %broadcast_in_dim.8, bf16[4,2,384,128]{3,2,1,0:T(8,128)(2,1)S(1)} %broadcast_in_dim.6), kind=kLoop, calls=%fused_computation.2 | loop fusion | flops 4718592 | bytes 4718592 | tf_op jit(solution)/shard_map/concatenate | solution.py:235
  43.9 4.4 %all-to-all-start.1 = ((bf16[8,1152,128]{2,1,0:T(8,128)(2,1)}), bf16[8,1152,128]{2,1,0:T(8,128)(2,1)S(1)}, u32[]{:S(2)}, u32[]{:S(2)}) async-start(bf16[8,1152,128]{2,1,0:T(8,128)(2,1)} %bitcast.10), calls=%async_computation.1 | async-start | bytes 4718592 | tf_op jit(solution)/shard_map/all_to_all | solution.py:41
  48.3 0.9 slice.98
  49.2 0.6 pad_add_fusion.place
  49.9 0.8 fusion.32
  51.0 1.1 fusion.17
  52.2 36.0 %all_gather.11 = bf16[2304,128]{1,0:T(8,128)(2,1)} all-gather(bf16[288,128]{1,0:T(8,128)(2,1)S(1)} %pad_maximum_fusion.3), channel_id=1, replica_groups=mesh['far'=8,'pair'=2,'x'=4,'core'=2,'tp'=4] {'far'}, dimensions={0}, use_global_device_ids=true | all-gather | bytes 663552 | tf_op jit(solution)/shard_map/all_gather | solution.py:246
  88.2 1.4 %copy-done.1 = bf16[8,1152,128]{2,1,0:T(8,128)(2,1)} copy-done((bf16[8,1152,128]{2,1,0:T(8,128)(2,1)}, bf16[8,1152,128]{2,1,0:T(8,128)(2,1)S(1)}, u32[]{:S(2)}) %copy-start.1) | copy-done | bytes 2359320
  89.6 9.4 %attend.1 = bf16[16,144,128]{2,1,0:T(8,128)(2,1)} custom-call(s32[2]{0:T(128)} %pad_add_fusion.place, bf16[8,288,128]{2,1,0:T(8,128)(2,1)} %bitcast.84, bf16[8,1152,128]{2,1,0:T(8,128)(2,1)} %copy-done.1), custom_call_target="tpu_custom_call" | custom-call | flops 1879048192 | bytes 2000000 | tf_op jit(solution)/shard_map/attend/pallas_call | solution.py:149
  99.0 5.3 %all-to-all-start.2 = ((bf16[16,144,128]{2,1,0:T(8,128)(2,1)}), bf16[16,144,128]{2,1,0:T(8,128)(2,1)S(1)}, u32[]{:S(2)}, u32[]{:S(2)}) async-start(bf16[16,144,128]{2,1,0:T(8,128)(2,1)} %attend.1), calls=%async_computation.2 | async-start | bytes 1179648 | tf_op jit(solution)/shard_map/all_to_all | solution.py:41
  104.4 2.0 %collective-permute-start.2 = (bf16[8,1152,128]{2,1,0:T(8,128)(2,1)}, bf16[8,1152,128]{2,1,0:T(8,128)(2,1)}, u32[]{:S(2)}, u32[]{:S(2)}) collective-permute-start(bf16[8,1152,128]{2,1,0:T(8,128)(2,1)} %copy-done.1), channel_id=1, source_target_pairs={{0,4},{4,0},{1,5},{5,1},{2,6},{6,2},{3,7},{7,3},{8,12},{12,8},{9,1... | collective-permute-start | bytes 7077896 | tf_op jit(solution)/shard_map/ppermute | solution.py:237
  106.4 0.8 slice.67
  107.2 2.5 %collective-permute-start = (bf16[2,2048]{1,0:T(2,128)(2,1)S(1)}, bf16[2,2048]{1,0:T(2,128)(2,1)S(1)}, u32[]{:S(2)}, u32[]{:S(2)}) collective-permute-start(bf16[2,2048]{1,0:T(2,128)(2,1)S(1)} %slice.67), channel_id=1, source_target_pairs={{0,4},{4,8},{8,12},{12,16},{16,20},{20,24},{24,28},{28,32},{32,36}... | collective-permute-start | bytes 24584 | tf_op jit(solution)/shard_map/ppermute | solution.py:47
  109.7 4.6 %collective-permute-done = bf16[2,2048]{1,0:T(2,128)(2,1)S(1)} collective-permute-done((bf16[2,2048]{1,0:T(2,128)(2,1)S(1)}, bf16[2,2048]{1,0:T(2,128)(2,1)S(1)}, u32[]{:S(2)}, u32[]{:S(2)}) %collective-permute-start) | collective-permute-done | bytes 8224 | tf_op jit(solution)/shard_map/ppermute | solution.py:47
  114.6 1.5 %slice.92 = bf16[8,768,128]{2,1,0:T(8,128)(2,1)S(1)} slice(bf16[8,1152,128]{2,1,0:T(8,128)(2,1)} %copy-done.1), slice={[0:8], [384:1152], [0:128]} | slice | bytes 3145728 | tf_op jit(solution)/shard_map/slice | solution.py:35
  117.9 1.5 %slice.93 = bf16[8,768,128]{2,1,0:T(8,128)(2,1)S(1)} slice(bf16[8,1152,128]{2,1,0:T(8,128)(2,1)} %collective-permute-done.2), slice={[0:8], [384:1152], [0:128]} | slice | bytes 3145728 | tf_op jit(solution)/shard_map/slice | solution.py:35
  119.4 0.5 copy.25
  120.8 0.7 copy-done.7
  121.5 1.1 fusion
  122.6 3.8 %all-to-all-start.3 = ((bf16[4,32,2048]{2,1,0:T(8,128)(2,1)}), bf16[4,32,2048]{2,1,0:T(8,128)(2,1)S(1)}, u32[]{:S(2)}, u32[]{:S(2)}) async-start(bf16[4,32,2048]{2,1,0:T(8,128)(2,1)} %bitcast.30), calls=%async_computation.3 | async-start | bytes 1048576 | tf_op jit(solution)/shard_map/all_to_all | solution.py:41
  126.4 0.6 log_add_fusion
  126.9 7.5 %all-to-all-done.3 = bf16[4,32,2048]{2,1,0:T(8,128)(2,1)S(1)} async-done(((bf16[4,32,2048]{2,1,0:T(8,128)(2,1)}), bf16[4,32,2048]{2,1,0:T(8,128)(2,1)S(1)}, u32[]{:S(2)}, u32[]{:S(2)}) %all-to-all-start.3) | async-done | bytes 524320 | tf_op jit(solution)/shard_map/all_to_all | solution.py:41
  134.7 0.8 multiply_convert_fusion
  (80 shorter events, 5.5 us)
Async XLA Ops:
  0.6 119.8 %copy-start = (bf16[256,2048]{1,0:T(8,128)(2,1)S(1)}, bf16[256,2048]{1,0:T(8,128)(2,1)}, u32[]{:S(2)}) copy-start(bf16[256,2048]{1,0:T(8,128)(2,1)} %param.33) | copy-start | bytes 3145732
  0.6 18.5 %copy-start.2 = (bf16[128,2048]{1,0:T(8,128)(2,1)S(1)}, bf16[128,2048]{1,0:T(8,128)(2,1)}, u32[]{:S(2)}) copy-start(bf16[128,2048]{1,0:T(8,128)(2,1)} %param.18) | copy-start | bytes 1572868
  0.7 18.2 %copy-start.6 = (bf16[2048,128]{1,0:T(8,128)(2,1)S(1)}, bf16[2048,128]{1,0:T(8,128)(2,1)}, u32[]{:S(2)}) copy-start(bf16[2048,128]{1,0:T(8,128)(2,1)} %param.25) | copy-start | bytes 1572868
  0.7 18.5 %copy-start.12 = (f32[2048]{0:T(1024)S(1)}, f32[2048]{0:T(1024)}, u32[]{:S(2)}) copy-start(f32[2048]{0:T(1024)} %param.19) | copy-start | bytes 24580
  2.4 39.5 %all-to-all-start = ((bf16[16,96,128]{2,1,0:T(8,128)(2,1)}), bf16[16,96,128]{2,1,0:T(8,128)(2,1)S(1)}, u32[]{:S(2)}, u32[]{:S(2)}) async-start(bf16[16,96,128]{2,1,0:T(8,128)(2,1)} %broadcast_in_dim.7), calls=%async_computation | async-start | bytes 786432 | tf_op jit(solution)/shard_map/all_to_all | solution.py:31
  19.3 15.5 %copy-start.3 = (bf16[128,2048]{1,0:T(8,128)(2,1)}, bf16[128,2048]{1,0:T(8,128)(2,1)S(1)}, u32[]{:S(2)}) copy-start(bf16[128,2048]{1,0:T(8,128)(2,1)S(1)} %fusion.22) | copy-start | bytes 1572868
  19.3 15.5 %copy-start.10 = (bf16[2048,32]{0,1:T(8,128)(2,1)S(1)}, bf16[2048,32]{0,1:T(8,128)(2,1)}, u32[]{:S(2)}) copy-start(bf16[2048,32]{0,1:T(8,128)(2,1)} %param.26) | copy-start | bytes 393220
  21.2 13.9 %copy-start.14 = (f32[768]{0:T(1024)S(1)}, f32[768]{0:T(1024)}, u32[]{:S(2)}) copy-start(f32[768]{0:T(1024)} %param.27) | copy-start | bytes 9220
  21.2 14.2 %copy-start.11 = (bf16[768,64]{0,1:T(8,128)(2,1)S(1)}, bf16[768,64]{0,1:T(8,128)(2,1)}, u32[]{:S(2)}) copy-start(bf16[768,64]{0,1:T(8,128)(2,1)} %param.30) | copy-start | bytes 294916
  21.2 14.4 %copy-start.8 = (bf16[768,128]{1,0:T(8,128)(2,1)S(1)}, bf16[768,128]{1,0:T(8,128)(2,1)}, u32[]{:S(2)}) copy-start(bf16[768,128]{1,0:T(8,128)(2,1)} %param.29) | copy-start | bytes 589828
  33.9 0.7 copy-start.5
  35.9 6.0 %collective-permute-start.1 = (bf16[192,128]{1,0:T(8,128)(2,1)S(1)}, bf16[192,128]{1,0:T(8,128)(2,1)S(1)}, u32[]{:S(2)}, u32[]{:S(2)}) collective-permute-start(bf16[192,128]{1,0:T(8,128)(2,1)S(1)} %pad_maximum_fusion.4), channel_id=1, source_target_pairs={{0,32},{32,0},{1,33},{33,1},{2,34},{34,2},{3,35},{35,3},{4,36},{36... | collective-permute-start | bytes 147464 | tf_op jit(solution)/shard_map/ppermute | solution.py:225
  43.9 6.9 %copy-start.9 = (bf16[512,128]{1,0:T(8,128)(2,1)S(1)}, bf16[512,128]{1,0:T(8,128)(2,1)}, u32[]{:S(2)}) copy-start(bf16[512,128]{1,0:T(8,128)(2,1)} %param.32) | copy-start | bytes 393220
  43.9 44.4 %all-to-all-start.1 = ((bf16[8,1152,128]{2,1,0:T(8,128)(2,1)}), bf16[8,1152,128]{2,1,0:T(8,128)(2,1)S(1)}, u32[]{:S(2)}, u32[]{:S(2)}) async-start(bf16[8,1152,128]{2,1,0:T(8,128)(2,1)} %bitcast.10), calls=%async_computation.1 | async-start | bytes 4718592 | tf_op jit(solution)/shard_map/all_to_all | solution.py:41
  88.2 1.4 %copy-start.1 = (bf16[8,1152,128]{2,1,0:T(8,128)(2,1)}, bf16[8,1152,128]{2,1,0:T(8,128)(2,1)S(1)}, u32[]{:S(2)}) copy-start(bf16[8,1152,128]{2,1,0:T(8,128)(2,1)S(1)} %all-to-all-done.1.query_ref) | copy-start | bytes 7077892
  89.6 20.0 %copy-start.15 = (f32[3,256]{1,0:T(4,128)S(1)}, f32[3,256]{1,0:T(4,128)}, u32[]{:S(2)}) copy-start(f32[3,256]{1,0:T(4,128)} %param.23) | copy-start | bytes 9220
  99.0 18.6 %all-to-all-start.2 = ((bf16[16,144,128]{2,1,0:T(8,128)(2,1)}), bf16[16,144,128]{2,1,0:T(8,128)(2,1)S(1)}, u32[]{:S(2)}, u32[]{:S(2)}) async-start(bf16[16,144,128]{2,1,0:T(8,128)(2,1)} %attend.1), calls=%async_computation.2 | async-start | bytes 1179648 | tf_op jit(solution)/shard_map/all_to_all | solution.py:41
  104.4 13.5 %collective-permute-start.2 = (bf16[8,1152,128]{2,1,0:T(8,128)(2,1)}, bf16[8,1152,128]{2,1,0:T(8,128)(2,1)}, u32[]{:S(2)}, u32[]{:S(2)}) collective-permute-start(bf16[8,1152,128]{2,1,0:T(8,128)(2,1)} %copy-done.1), channel_id=1, source_target_pairs={{0,4},{4,0},{1,5},{5,1},{2,6},{6,2},{3,7},{7,3},{8,12},{12,8},{9,1... | collective-permute-start | bytes 7077896 | tf_op jit(solution)/shard_map/ppermute | solution.py:237
  107.2 7.2 %collective-permute-start = (bf16[2,2048]{1,0:T(2,128)(2,1)S(1)}, bf16[2,2048]{1,0:T(2,128)(2,1)S(1)}, u32[]{:S(2)}, u32[]{:S(2)}) collective-permute-start(bf16[2,2048]{1,0:T(2,128)(2,1)S(1)} %slice.67), channel_id=1, source_target_pairs={{0,4},{4,8},{8,12},{12,16},{16,20},{20,24},{24,28},{28,32},{32,36}... | collective-permute-start | bytes 24584 | tf_op jit(solution)/shard_map/ppermute | solution.py:47
  116.1 1.0 copy-start.4
  120.4 1.0 copy-start.7
  121.5 13.2 %copy-start.13 = (f32[2048]{0:T(1024)S(1)}, f32[2048]{0:T(1024)}, u32[]{:S(2)}) copy-start(f32[2048]{0:T(1024)} %param.35) | copy-start | bytes 24580
  122.6 11.9 %all-to-all-start.3 = ((bf16[4,32,2048]{2,1,0:T(8,128)(2,1)}), bf16[4,32,2048]{2,1,0:T(8,128)(2,1)S(1)}, u32[]{:S(2)}, u32[]{:S(2)}) async-start(bf16[4,32,2048]{2,1,0:T(8,128)(2,1)} %bitcast.30), calls=%async_computation.3 | async-start | bytes 1048576 | tf_op jit(solution)/shard_map/all_to_all | solution.py:41

commit v5 on v4

--- a/solution.py
+++ b/solution.py
@@ -26,11 +26,6 @@
 F32 = jnp.float32
 
 
-def copy_for_each(array, axis):
-    copies = jnp.broadcast_to(array, (lax.axis_size(axis), *array.shape))
-    return lax.all_to_all(copies, axis, split_axis=0, concat_axis=0, tiled=True)
-
-
 def weight_rows(joint, depth, wide, cores):
     rows = joint[:, 2 * QUERY_ROWS :].reshape(wide, cores, -1, 6, depth, 128)
     rows = rows.transpose(2, 0, 1, 4, 3, 5)
@@ -73,8 +68,8 @@
 FLOOR = -1e29
 
 
-def attention_kernel(place, held_ref, query_ref, out_ref, key_rows, value_cols, query_full):
-    far, here = place[0], place[1]
+def attention_kernel(held_ref, query_ref, out_ref, key_rows, value_cols, query_full):
+    far, here = lax.axis_index("far"), lax.axis_index(GROUP)
     blocks = held_ref.shape[0]
     near = query_ref.shape[0]
     groups = 2 * near
@@ -143,7 +138,7 @@
             mix((n - 2) * COLS, *softened.pop(n - 2))
 
 
-def attend(place, held, joint):
+def attend(held, joint):
     blocks, groups = held.shape[0], 2 * joint.shape[0]
     width = 2 * groups * 128
     return pl.pallas_call(
@@ -151,7 +146,6 @@
         out_shape=jax.ShapeDtypeStruct((groups, PART_ROWS, 128), BF16),
         grid=(1,),
         in_specs=[
-            pl.BlockSpec(memory_space=pltpu.SMEM),
             pl.BlockSpec(held.shape, lambda i: (0, 0, 0)),
             pl.BlockSpec((groups // 2, 2 * QUERY_ROWS, 128), lambda i: (0, 0, 0)),
         ],
@@ -167,7 +161,102 @@
             transcendentals=blocks * 128 * width,
         ),
         name="attend",
-    )(place, held, joint)
+    )(held, joint)
+
+
+def dot_nt(left, right):
+    return lax.dot_general(left, right, (((1,), (1,)), ((), ())), preferred_element_type=F32)
+
+
+def gates_kernel(outer_ref, inner_ref, signal_ref, out_ref):
+    depth = outer_ref.shape[0]
+    at = 0
+    for ref in (outer_ref, inner_ref, signal_ref):
+        for first in range(0, ref.shape[1], 128):
+            block = ref[:, first : first + 128]
+            for d in range(out_ref.shape[0]):
+                out_ref[d, at : at + depth, :] = block
+            at += depth
+
+
+def spread_gates(gates, copies):
+    depth, width = gates[0].shape
+    return pl.pallas_call(
+        gates_kernel,
+        out_shape=jax.ShapeDtypeStruct((copies, 3 * depth * width // 128, 128), BF16),
+        cost_estimate=pl.CostEstimate(flops=1_000_000, bytes_accessed=400_000, transcendentals=0),
+        name="spread_gates",
+    )(*gates)
+
+
+def entry_kernel(tokens, gain, latent_down, query_down, rotary_down, normed_ref, latent_ref, rot_ref):
+    wide = tokens[...].astype(F32)
+    scale = lax.rsqrt(jnp.mean(wide * wide, axis=-1, keepdims=True) + eps)
+    normed = (wide * scale * gain[...]).astype(BF16)
+    normed_ref[...] = normed
+    n = latent_down.shape[1]
+    latent_ref[:, :n] = jnp.dot(
+        normed, latent_down[...], preferred_element_type=F32
+    ).astype(BF16)
+    latent_ref[:, n:] = dot_nt(normed, query_down[...]).astype(BF16)
+    rot_ref[...] = dot_nt(rotary_down[...], normed)
+
+
+def entry(tokens, gain, latent_down, query_down, rotary_down):
+    rows, width = tokens.shape
+    columns = latent_down.shape[1] + query_down.shape[1]
+    return pl.pallas_call(
+        entry_kernel,
+        out_shape=(
+            jax.ShapeDtypeStruct((rows, width), BF16),
+            jax.ShapeDtypeStruct((rows, columns), BF16),
+            jax.ShapeDtypeStruct((ROPE, rows), F32),
+        ),
+        cost_estimate=pl.CostEstimate(
+            flops=2 * rows * width * 384, bytes_accessed=2_500_000, transcendentals=rows
+        ),
+        name="entry",
+    )(tokens, gain.reshape(1, -1), latent_down, query_down.T, rotary_down.T)
+
+
+def merge_kernel(parts_ref, conv_ref, weight_ref, out_ref, logsum_ref):
+    groups = parts_ref.shape[0]
+    tails = parts_ref[:, 128:PART_ROWS, :].astype(F32)
+    heads = []
+    for h in range(2):
+        logs = tails[:, 8 * h, :] + (tails[:, 8 * h + 1, :] + tails[:, 8 * h + 2, :])
+        top = jnp.max(logs, axis=0, keepdims=True)
+        share = jnp.exp(logs - top)
+        share_sum = jnp.sum(share, axis=0, keepdims=True)
+        logsum_ref[h : h + 1, :] = top + jnp.log(share_sum)
+        share = share / share_sum
+        mixed = jnp.zeros((VDIM, 128), F32)
+        for g in range(groups):
+            part = parts_ref[g, h * VDIM : (h + 1) * VDIM, :].astype(F32)
+            mixed = mixed + part * share[g : g + 1, :]
+        heads.append(mixed)
+    mixed = jnp.concatenate(heads, axis=0).T.astype(BF16)
+    for first in range(0, out_ref.shape[1], 512):
+        at = slice(first, first + 512)
+        out_ref[:, at] = (
+            conv_ref[:, at]
+            + jnp.dot(mixed, weight_ref[:, at], preferred_element_type=F32)
+        ).astype(BF16)
+
+
+def merge(parts, conv_projected, heads_output):
+    rows, width = conv_projected.shape
+    return pl.pallas_call(
+        merge_kernel,
+        out_shape=(
+            jax.ShapeDtypeStruct((rows, width), BF16),
+            jax.ShapeDtypeStruct((2, rows), F32),
+        ),
+        cost_estimate=pl.CostEstimate(
+            flops=2 * rows * width * 128, bytes_accessed=2_000_000, transcendentals=rows * 32
+        ),
+        name="merge",
+    )(parts, conv_projected, heads_output)
 
 
 def layer(
@@ -192,26 +281,22 @@
 ):
     rows = tokens.shape[0]
     sp_index = lax.axis_index(SP)
-    place = jnp.stack([lax.axis_index("far"), lax.axis_index(GROUP)]).astype(jnp.int32)
     core = lax.axis_index("core")
 
     depth = outer_gate.shape[0]
-    gates = jnp.concatenate([outer_gate, inner_gate, conv_input], axis=1)
-    gates = gates.reshape(depth, -1, 128).swapaxes(0, 1).reshape(-1, 128)
-    gates = copy_for_each(gates, Z)
+    gates = spread_gates((outer_gate, inner_gate, conv_input), lax.axis_size(Z))
+    gates = exchange(gates, Z)
 
     edge = shifted(tokens[rows - (TAPS - 1) :], SP, 1)
 
-    normed = rms_scale(tokens, pre_gain).astype(BF16)
-    down = jnp.concatenate([latent_down, query_down], axis=1)
-    latents = jnp.dot(normed, down, preferred_element_type=F32).astype(BF16)
+    normed, latents, key_raw = entry(tokens, pre_gain, latent_down, query_down, rotary_down)
     latents = lax.all_gather(latents, "tp", axis=0)
 
     positions = sp_index * rows + jnp.arange(rows, dtype=jnp.int32)
     frequency = rope_theta ** (-jnp.arange(ROPE // 2, dtype=F32) / (ROPE // 2))
     angles = positions.astype(F32)[None, :] * frequency[:, None]
     cosine, sine = jnp.cos(angles), jnp.sin(angles)
-    key_turned = rotate_rows(dot_t(normed, rotary_down), cosine, sine).astype(BF16)
+    key_turned = rotate_rows(key_raw, cosine, sine).astype(BF16)
 
     n_latent = latent_down.shape[1]
     key_latent = jnp.moveaxis(latents[:, :, :n_latent], 0, 1).reshape(rows, -1)
@@ -245,7 +330,7 @@
     )
     held = lax.all_gather(held, "far", axis=0, tiled=True).reshape(-1, *held.shape)
 
-    parts = attend(place, held, joint)
+    parts = attend(held, joint)
     parts = exchange(parts, GROUP)
 
     mine, other = (weight_rows(whole, depth, wide, cores) for whole in (joint, joint_other))
@@ -264,20 +349,7 @@
     conv_mixed = (outer_part[lead:] * convolved).astype(BF16)
     conv_projected = jnp.dot(conv_mixed, conv_output, preferred_element_type=F32)
 
-    groups = parts.shape[0]
-    logs = parts[:, 128:].reshape(groups, 2, 8, 128)[:, :, :3].astype(F32)
-    logs = logs[:, :, 0] + (logs[:, :, 1] + logs[:, :, 2])
-    top = jnp.max(logs, axis=0)
-    share = jnp.exp(logs - top)
-    share_sum = jnp.sum(share, axis=0)
-    row_logsum = top + jnp.log(share_sum)
-    share = share / share_sum
-    mixed_parts = parts[:, :128].reshape(groups, 2, VDIM, 128).astype(F32)
-    heads = jnp.sum(mixed_parts * share[:, :, None, :], axis=0).astype(BF16).reshape(-1, rows)
-    heads_projected = lax.dot_general(
-        heads, heads_output, (((0,), (0,)), ((), ())), preferred_element_type=F32
-    )
-    projected = (conv_projected + heads_projected).astype(BF16)
+    projected, row_logsum = merge(parts, conv_projected, heads_output)
     tp = lax.axis_size("tp")
     arrived = exchange(projected.reshape(tp, rows // tp, -1), "tp")
     projected = arrived.astype(F32).sum(axis=0)

time: 136 us -> 167 us (1.23)
  the two profiles are of different devices: /device:TPU:32 before, /device:TPU:1 now
where the time goes in v5:
time: 167 us; the launch traced here: 164 us
  blocking collectives  57.8 us (35%)
  starting transfers between devices  41.8 us (25%)
  waiting for transfers between devices  27.2 us (16%)
  Pallas kernels  16.9 us (10%)
  local copies, waits for them, and re-layouts  9.83 us (6%)
  matrix products  4.85 us (3%)
  other arithmetic  4.4 us (3%)
    all_gather x1, blocking collectives, layer(): lax.all_gather(held, 'far', axis=0, tiled=True).reshape(-1, *held.shape)  32.2 us
    all_to_all x3, starting transfers between devices, exchange(): return lax.all_to_all(array, axis, split_axis=0, concat_axis=0, tiled=True)  31.8 us
    all_to_all x3, waiting for transfers between devices, exchange(): return lax.all_to_all(array, axis, split_axis=0, concat_axis=0, tiled=True)  24.7 us
    all_to_all x1, blocking collectives, exchange(): return lax.all_to_all(array, axis, split_axis=0, concat_axis=0, tiled=True)  13.7 us
    all_gather x1, blocking collectives, layer(): latents = lax.all_gather(latents, 'tp', axis=0)  11.9 us
    pallas_call x1, Pallas kernels, attend(): pl.pallas_call(attention_kernel, out_shape=jax.ShapeDtypeStruct((groups,...  9.41 us
    ppermute x1, starting transfers between devices, shifted(): lax.ppermute(value, axis, [(source, source + steps) for source in range(f...  3.73 us
    ppermute x1, starting transfers between devices, layer(): queries_other = lax.ppermute(queries, 'pair', [(0, 1), (1, 0)])  3.39 us
  transfers between devices with their start and end apart: 6, of which 3 were waited for; matrix products, arithmetic and copies ran while one was open for 9% of the time, Pallas kernels for 8%

profile of v5, /device:TPU:1, one launch (start us, length us, event | category | flops | bytes accessed | tf_op | source)
XLA Modules:
  0.0 163.8 jit_solution(15214833993154938689)
XLA Ops:
  0.6 1.6 spread_gates.1
  2.3 15.9 %all-to-all-start = ((bf16[16,96,128]{2,1,0:T(8,128)(2,1)}), bf16[16,96,128]{2,1,0:T(8,128)(2,1)S(1)}, u32[]{:S(2)}, u32[]{:S(2)}) async-start(bf16[16,96,128]{2,1,0:T(8,128)(2,1)} %spread_gates.1), calls=%async_computation | async-start | bytes 786432 | tf_op jit(solution)/shard_map/all_to_all | solution.py:36
  18.2 3.0 %entry.1 = (bf16[128,2048]{1,0:T(8,128)(2,1)}, bf16[128,320]{1,0:T(8,128)(2,1)}, f32[32,128]{1,0:T(8,128)}) custom-call(bf16[128,2048]{1,0:T(8,128)(2,1)} %tokens.1, f32[1,2048]{1,0:T(1,128)} %bitcast.76, bf16[2048,128]{1,0:T(8,128)(2,1)} %latent_down.1, bf16[192,2048]{1,0:T(8,128)(2,1)} %bitcast.69, bf16[32,2048]{1,0:T(8,128)(2,1)} %bitcast.75), custom_call_target="tpu_custom_call" | custom-call | flops 201326592 | bytes 2500000 | tf_op jit(solution)/shard_map/entry/pallas_call | solution.py:208
  21.1 11.9 %all-gather = bf16[512,320]{1,0:T(8,128)(2,1)S(1)} all-gather(bf16[128,320]{1,0:T(8,128)(2,1)} %get-tuple-element.7), channel_id=2, replica_groups=mesh['far'=8,'pair'=2,'x'=4,'core'=2,'tp'=4] {'tp'}, dimensions={0}, use_global_device_ids=true | all-gather | bytes 409600 | tf_op jit(solution)/shard_map/all_gather | solution.py:293
  33.0 0.7 copy-done.2
  34.9 3.4 %collective-permute-start = (bf16[192,128]{1,0:T(8,128)(2,1)S(1)}, bf16[192,128]{1,0:T(8,128)(2,1)S(1)}, u32[]{:S(2)}, u32[]{:S(2)}) collective-permute-start(bf16[192,128]{1,0:T(8,128)(2,1)S(1)} %pad_maximum_fusion.4), channel_id=1, source_target_pairs={{0,32},{32,0},{1,33},{33,1},{2,34},{34,2},{3,35},{35,3},{4,36},{36... | collective-permute-start | bytes 147464 | tf_op jit(solution)/shard_map/ppermute | solution.py:310
  38.3 1.9 %collective-permute-done = bf16[192,128]{1,0:T(8,128)(2,1)S(1)} collective-permute-done((bf16[192,128]{1,0:T(8,128)(2,1)S(1)}, bf16[192,128]{1,0:T(8,128)(2,1)S(1)}, u32[]{:S(2)}, u32[]{:S(2)}) %collective-permute-start) | collective-permute-done | bytes 49184 | tf_op jit(solution)/shard_map/ppermute | solution.py:310
  40.6 1.6 pad_maximum_fusion
  42.1 7.6 %all-to-all-start.1 = ((bf16[8,1152,128]{2,1,0:T(8,128)(2,1)}), bf16[8,1152,128]{2,1,0:T(8,128)(2,1)S(1)}, u32[]{:S(2)}, u32[]{:S(2)}) async-start(bf16[8,1152,128]{2,1,0:T(8,128)(2,1)} %bitcast.17), calls=%async_computation.1 | async-start | bytes 4718592 | tf_op jit(solution)/shard_map/all_to_all | solution.py:36
  49.7 1.6 slice.65
  51.3 1.0 copy.24
  52.4 0.6 copy-done.3
  53.0 1.0 fusion.20
  54.0 24.7 %all-to-all-done.1.query_ref = bf16[8,1152,128]{2,1,0:T(8,128)(2,1)S(1)} async-done(((bf16[8,1152,128]{2,1,0:T(8,128)(2,1)}), bf16[8,1152,128]{2,1,0:T(8,128)(2,1)S(1)}, u32[]{:S(2)}, u32[]{:S(2)}) %all-to-all-start.1) | async-done | bytes 2359328 | tf_op jit(solution)/shard_map/all_to_all | solution.py:36
  78.7 2.9 %collective-permute-start.2 = (bf16[8,1152,128]{2,1,0:T(8,128)(2,1)S(1)}, bf16[8,1152,128]{2,1,0:T(8,128)(2,1)}, u32[]{:S(2)}, u32[]{:S(2)}) collective-permute-start(bf16[8,1152,128]{2,1,0:T(8,128)(2,1)S(1)} %all-to-all-done.1.query_ref), channel_id=1, source_target_pairs={{0,4},{4,0},{1,5},{5,1},{2,6},{6,2},{3,7},{7,3},{8,12},{12,8},{9,1... | collective-permute-start | bytes 7077896 | tf_op jit(solution)/shard_map/ppermute | solution.py:322
  81.6 1.1 fusion.10
  82.8 1.1 fusion.9
  83.9 32.2 %all_gather.11 = bf16[2304,128]{1,0:T(8,128)(2,1)} all-gather(bf16[288,128]{1,0:T(8,128)(2,1)S(1)} %pad_maximum_fusion.3), channel_id=1, replica_groups=mesh['far'=8,'pair'=2,'x'=4,'core'=2,'tp'=4] {'far'}, dimensions={0}, use_global_device_ids=true | all-gather | bytes 663552 | tf_op jit(solution)/shard_map/all_gather | solution.py:331
  116.2 9.4 %attend.1 = bf16[16,144,128]{2,1,0:T(8,128)(2,1)} custom-call(bf16[8,288,128]{2,1,0:T(8,128)(2,1)} %bitcast.70, bf16[8,1152,128]{2,1,0:T(8,128)(2,1)} %copy-done.1), custom_call_target="tpu_custom_call" | custom-call | flops 1879048192 | bytes 2000000 | tf_op jit(solution)/shard_map/attend/pallas_call | solution.py:144
  125.6 8.4 %all-to-all-start.2 = ((bf16[16,144,128]{2,1,0:T(8,128)(2,1)}), bf16[16,144,128]{2,1,0:T(8,128)(2,1)}, u32[]{:S(2)}, u32[]{:S(2)}) async-start(bf16[16,144,128]{2,1,0:T(8,128)(2,1)} %attend.1), calls=%async_computation.2 | async-start | bytes 1179648 | tf_op jit(solution)/shard_map/all_to_all | solution.py:36
  133.9 0.8 slice.55
  134.7 3.7 %collective-permute-start.1 = (bf16[2,2048]{1,0:T(2,128)(2,1)S(1)}, bf16[2,2048]{1,0:T(2,128)(2,1)S(1)}, u32[]{:S(2)}, u32[]{:S(2)}) collective-permute-start(bf16[2,2048]{1,0:T(2,128)(2,1)S(1)} %slice.55), channel_id=1, source_target_pairs={{0,4},{4,8},{8,12},{12,16},{16,20},{20,24},{24,28},{28,32},{32,36}... | collective-permute-start | bytes 24584 | tf_op jit(solution)/shard_map/ppermute | solution.py:42
  138.5 0.7 collective-permute-done.1
  139.4 1.5 slice.69
  140.9 0.5 copy.22
  141.5 0.5 copy-done.12
  142.4 1.5 slice.70
  143.9 0.5 copy.23
  144.9 1.3 fusion.30.conv_ref
  146.3 2.9 %merge.1 = (bf16[128,2048]{1,0:T(8,128)(2,1)}, f32[2,128]{1,0:T(2,128)}) custom-call(bf16[16,144,128]{2,1,0:T(8,128)(2,1)} %all-to-all-done.2.parts_ref, f32[128,2048]{1,0:T(8,128)} %fusion.30.conv_ref, bf16[128,2048]{1,0:T(8,128)(2,1)} %weight_ref.1), custom_call_target="tpu_custom_call" | custom-call | flops 67108864 | bytes 2000000 | tf_op jit(solution)/shard_map/merge/pallas_call | solution.py:249
  149.1 13.7 %all_to_all.20 = bf16[4,32,2048]{2,1,0:T(8,128)(2,1)S(1)} all-to-all(bf16[4,32,2048]{2,1,0:T(8,128)(2,1)} %bitcast.71), channel_id=1, replica_groups=mesh['far'=8,'pair'=2,'x'=4,'core'=2,'tp'=4] {'tp'}, dimensions={0} | all-to-all | bytes 1048576 | tf_op jit(solution)/shard_map/all_to_all | solution.py:36
  163.0 0.8 multiply_convert_fusion
  (56 shorter events, 2.9 us)
Async XLA Ops:
  0.6 144.3 %copy-start = (bf16[256,2048]{1,0:T(8,128)(2,1)S(1)}, bf16[256,2048]{1,0:T(8,128)(2,1)}, u32[]{:S(2)}) copy-start(bf16[256,2048]{1,0:T(8,128)(2,1)} %param.33) | copy-start | bytes 3145732
  2.3 31.8 %copy-start.9 = (f32[768]{0:T(1024)S(1)}, f32[768]{0:T(1024)}, u32[]{:S(2)}) copy-start(f32[768]{0:T(1024)} %param.27) | copy-start | bytes 9220
  2.3 38.0 %all-to-all-start = ((bf16[16,96,128]{2,1,0:T(8,128)(2,1)}), bf16[16,96,128]{2,1,0:T(8,128)(2,1)S(1)}, u32[]{:S(2)}, u32[]{:S(2)}) async-start(bf16[16,96,128]{2,1,0:T(8,128)(2,1)} %spread_gates.1), calls=%async_computation | async-start | bytes 786432 | tf_op jit(solution)/shard_map/all_to_all | solution.py:36
  18.1 16.3 %copy-start.5 = (bf16[768,64]{0,1:T(8,128)(2,1)S(1)}, bf16[768,64]{0,1:T(8,128)(2,1)}, u32[]{:S(2)}) copy-start(bf16[768,64]{0,1:T(8,128)(2,1)} %param.30) | copy-start | bytes 294916
  18.2 16.5 %copy-start.4 = (bf16[768,128]{1,0:T(8,128)(2,1)S(1)}, bf16[768,128]{1,0:T(8,128)(2,1)}, u32[]{:S(2)}) copy-start(bf16[768,128]{1,0:T(8,128)(2,1)} %param.29) | copy-start | bytes 589828
  21.1 13.1 %copy-start.7 = (f32[32,128]{1,0:T(8,128)S(1)}, f32[32,128]{1,0:T(8,128)}, u32[]{:S(2)}) copy-start(f32[32,128]{1,0:T(8,128)} %get-tuple-element.8) | copy-start | bytes 49156
  33.0 0.7 copy-start.2
  34.9 5.3 %collective-permute-start = (bf16[192,128]{1,0:T(8,128)(2,1)S(1)}, bf16[192,128]{1,0:T(8,128)(2,1)S(1)}, u32[]{:S(2)}, u32[]{:S(2)}) collective-permute-start(bf16[192,128]{1,0:T(8,128)(2,1)S(1)} %pad_maximum_fusion.4), channel_id=1, source_target_pairs={{0,32},{32,0},{1,33},{33,1},{2,34},{34,2},{3,35},{35,3},{4,36},{36... | collective-permute-start | bytes 147464 | tf_op jit(solution)/shard_map/ppermute | solution.py:310
  42.1 10.9 %copy-start.11 = (f32[512]{0:T(512)S(1)}, f32[512]{0:T(512)}, u32[]{:S(2)}) copy-start(f32[512]{0:T(512)} %param.28) | copy-start | bytes 6148
  42.1 36.6 %all-to-all-start.1 = ((bf16[8,1152,128]{2,1,0:T(8,128)(2,1)}), bf16[8,1152,128]{2,1,0:T(8,128)(2,1)S(1)}, u32[]{:S(2)}, u32[]{:S(2)}) async-start(bf16[8,1152,128]{2,1,0:T(8,128)(2,1)} %bitcast.17), calls=%async_computation.1 | async-start | bytes 4718592 | tf_op jit(solution)/shard_map/all_to_all | solution.py:36
  52.3 0.7 copy-start.3
  78.7 37.4 %copy-start.1 = (bf16[8,1152,128]{2,1,0:T(8,128)(2,1)}, bf16[8,1152,128]{2,1,0:T(8,128)(2,1)S(1)}, u32[]{:S(2)}) copy-start(bf16[8,1152,128]{2,1,0:T(8,128)(2,1)S(1)} %all-to-all-done.1.query_ref) | copy-start | bytes 7077892
  78.7 63.6 %collective-permute-start.2 = (bf16[8,1152,128]{2,1,0:T(8,128)(2,1)S(1)}, bf16[8,1152,128]{2,1,0:T(8,128)(2,1)}, u32[]{:S(2)}, u32[]{:S(2)}) collective-permute-start(bf16[8,1152,128]{2,1,0:T(8,128)(2,1)S(1)} %all-to-all-done.1.query_ref), channel_id=1, source_target_pairs={{0,4},{4,0},{1,5},{5,1},{2,6},{6,2},{3,7},{7,3},{8,12},{12,8},{9,1... | collective-permute-start | bytes 7077896 | tf_op jit(solution)/shard_map/ppermute | solution.py:322
  116.2 22.3 %copy-start.10 = (f32[3,256]{1,0:T(4,128)S(1)}, f32[3,256]{1,0:T(4,128)}, u32[]{:S(2)}) copy-start(f32[3,256]{1,0:T(4,128)} %param.23) | copy-start | bytes 9220
  116.2 23.1 %copy-start.6 = (f32[2048]{0:T(1024)S(1)}, f32[2048]{0:T(1024)}, u32[]{:S(2)}) copy-start(f32[2048]{0:T(1024)} %param.19) | copy-start | bytes 24580
  125.6 20.7 %all-to-all-start.2 = ((bf16[16,144,128]{2,1,0:T(8,128)(2,1)}), bf16[16,144,128]{2,1,0:T(8,128)(2,1)}, u32[]{:S(2)}, u32[]{:S(2)}) async-start(bf16[16,144,128]{2,1,0:T(8,128)(2,1)} %attend.1), calls=%async_computation.2 | async-start | bytes 1179648 | tf_op jit(solution)/shard_map/all_to_all | solution.py:36
  134.7 4.4 %collective-permute-start.1 = (bf16[2,2048]{1,0:T(2,128)(2,1)S(1)}, bf16[2,2048]{1,0:T(2,128)(2,1)S(1)}, u32[]{:S(2)}, u32[]{:S(2)}) collective-permute-start(bf16[2,2048]{1,0:T(2,128)(2,1)S(1)} %slice.55), channel_id=1, source_target_pairs={{0,4},{4,8},{8,12},{12,16},{16,20},{20,24},{24,28},{28,32},{32,36}... | collective-permute-start | bytes 24584 | tf_op jit(solution)/shard_map/ppermute | solution.py:42
  140.9 1.0 copy-start.12
  146.2 16.8 %copy-start.8 = (f32[2048]{0:T(1024)S(1)}, f32[2048]{0:T(1024)}, u32[]{:S(2)}) copy-start(f32[2048]{0:T(1024)} %param.35) | copy-start | bytes 24580

commit v6 on v5

--- a/solution.py
+++ b/solution.py
@@ -24,12 +24,6 @@
 LOW = -1e30
 BF16 = jnp.bfloat16
 F32 = jnp.float32
-
-
-def weight_rows(joint, depth, wide, cores):
-    rows = joint[:, 2 * QUERY_ROWS :].reshape(wide, cores, -1, 6, depth, 128)
-    rows = rows.transpose(2, 0, 1, 4, 3, 5)
-    return rows.reshape(-1, 6 * 128)
 
 
 def exchange(array, axis):
@@ -147,7 +141,7 @@
         grid=(1,),
         in_specs=[
             pl.BlockSpec(held.shape, lambda i: (0, 0, 0)),
-            pl.BlockSpec((groups // 2, 2 * QUERY_ROWS, 128), lambda i: (0, 0, 0)),
+            pl.BlockSpec((groups // 2, 2 * QUERY_ROWS, 128), lambda i: (0, 2, 0)),
         ],
         out_specs=pl.BlockSpec((groups, PART_ROWS, 128), lambda i: (0, 0, 0)),
         scratch_shapes=[
@@ -155,6 +149,7 @@
             pltpu.VMEM((128, blocks * 128), BF16),
             pltpu.VMEM((160, width), BF16),
         ],
+        compiler_params=pltpu.CompilerParams(vmem_limit_bytes=56 << 20),
         cost_estimate=pl.CostEstimate(
             flops=2 * blocks * 128 * width * (160 + 64),
             bytes_accessed=2_000_000,
@@ -219,7 +214,77 @@
     )(tokens, gain.reshape(1, -1), latent_down, query_down.T, rotary_down.T)
 
 
-def merge_kernel(parts_ref, conv_ref, weight_ref, out_ref, logsum_ref):
+LEAD = 16
+
+
+def conv_kernel(
+    mine_ref, other_ref, normed_ref, edge_ref, gain_ref, taps_ref, output_ref, out_ref,
+    rows_ref, weight_ref, product_ref,
+):
+    core = lax.axis_index("core")
+    near, _, _ = mine_ref.shape
+    count, width = normed_ref.shape
+    half = width // 2
+    wide = edge_ref[...].astype(F32)
+    scale = lax.rsqrt(jnp.mean(wide * wide, axis=-1, keepdims=True) + eps)
+    rows_ref[:LEAD, :] = (wide * scale * gain_ref[...]).astype(BF16)
+    rows_ref[LEAD:, :] = normed_ref[...]
+    columns = weight_ref.shape[1]
+    depth = 128 // near
+    for side, ref in enumerate((mine_ref, other_ref)):
+        for block in range(half // 128):
+            for source in range(near):
+                to = side * half + block * 128 + source * depth
+                for b in range(columns // 128):
+                    at = (block * (columns // 128) + b) * depth
+                    weight_ref[to : to + depth, b * 128 : (b + 1) * 128] = ref[
+                        source, at : at + depth, :
+                    ]
+    own = pl.ds(pl.multiple_of(core * half, half), half)
+    rest = pl.ds(pl.multiple_of((1 - core) * half, half), half)
+    spread = jnp.dot(rows_ref[:, own], weight_ref[:half, :], preferred_element_type=F32)
+    spread += jnp.dot(rows_ref[:, rest], weight_ref[half:, :], preferred_element_type=F32)
+    third = columns // 3
+    product = spread[:, third : 2 * third] * spread[:, 2 * third :]
+    product_ref[...] = product.astype(BF16).astype(F32)
+    convolved = jnp.zeros((count, third), F32)
+    for k in range(TAPS):
+        first = LEAD - (TAPS - 1) + k
+        convolved = convolved + product_ref[first : first + count, :] * taps_ref[k : k + 1, :]
+    mixed = (spread[LEAD:, :third] * convolved).astype(BF16)
+    for first in range(0, out_ref.shape[1], 512):
+        at = slice(first, first + 512)
+        out_ref[:, at] = jnp.dot(mixed, output_ref[:, at], preferred_element_type=F32)
+
+
+def convolve(joint, joint_other, normed, edge, gain, taps, output):
+    count, width = normed.shape
+    third, out_width = output.shape
+    near = joint.shape[0]
+    weights = pl.BlockSpec((near, joint.shape[1] - 2 * QUERY_ROWS, 128), lambda i: (0, 0, 0))
+    whole = [pl.BlockSpec(a.shape, lambda i: (0, 0)) for a in (normed, edge, gain, taps, output)]
+    return pl.pallas_call(
+        conv_kernel,
+        out_shape=jax.ShapeDtypeStruct((count, out_width), F32),
+        grid=(1,),
+        in_specs=[weights, weights, *whole],
+        out_specs=pl.BlockSpec((count, out_width), lambda i: (0, 0)),
+        scratch_shapes=[
+            pltpu.VMEM((LEAD + count, width), BF16),
+            pltpu.VMEM((width, 3 * third), BF16),
+            pltpu.VMEM((LEAD + count, third), F32),
+        ],
+        cost_estimate=pl.CostEstimate(
+            flops=2 * count * (width * 3 * third + third * out_width),
+            bytes_accessed=6_000_000,
+            transcendentals=0,
+        ),
+        compiler_params=pltpu.CompilerParams(vmem_limit_bytes=30 << 20),
+        name="convolve",
+    )(joint, joint_other, normed, edge, gain, taps, output)
+
+
+def merge_kernel(parts_ref, conv_ref, weight_ref, out_ref, top_ref, log_ref):
     groups = parts_ref.shape[0]
     tails = parts_ref[:, 128:PART_ROWS, :].astype(F32)
     heads = []
@@ -228,7 +293,8 @@
         top = jnp.max(logs, axis=0, keepdims=True)
         share = jnp.exp(logs - top)
         share_sum = jnp.sum(share, axis=0, keepdims=True)
-        logsum_ref[h : h + 1, :] = top + jnp.log(share_sum)
+        top_ref[h : h + 1, :] = top
+        log_ref[h : h + 1, :] = jnp.log(share_sum)
         share = share / share_sum
         mixed = jnp.zeros((VDIM, 128), F32)
         for g in range(groups):
@@ -251,10 +317,12 @@
         out_shape=(
             jax.ShapeDtypeStruct((rows, width), BF16),
             jax.ShapeDtypeStruct((2, rows), F32),
+            jax.ShapeDtypeStruct((2, rows), F32),
         ),
         cost_estimate=pl.CostEstimate(
             flops=2 * rows * width * 128, bytes_accessed=2_000_000, transcendentals=rows * 32
         ),
+        compiler_params=pltpu.CompilerParams(vmem_limit_bytes=16 << 20),
         name="merge",
     )(parts, conv_projected, heads_output)
 
@@ -281,13 +349,11 @@
 ):
     rows = tokens.shape[0]
     sp_index = lax.axis_index(SP)
-    core = lax.axis_index("core")
-
-    depth = outer_gate.shape[0]
+
     gates = spread_gates((outer_gate, inner_gate, conv_input), lax.axis_size(Z))
     gates = exchange(gates, Z)
 
-    edge = shifted(tokens[rows - (TAPS - 1) :], SP, 1)
+    edge = shifted(tokens[rows - LEAD :], SP, 1)
 
     normed, latents, key_raw = entry(tokens, pre_gain, latent_down, query_down, rotary_down)
     latents = lax.all_gather(latents, "tp", axis=0)
@@ -317,7 +383,7 @@
     halves = gates.reshape(cores, -1, 128)
     both = jnp.broadcast_to(jnp.concatenate(both, axis=0), (wide, cores, 2 * QUERY_ROWS, 128))
     halves = jnp.broadcast_to(halves, (wide, *halves.shape))
-    sent = jnp.concatenate([both, halves], axis=2)
+    sent = jnp.concatenate([halves, both], axis=2)
     joint = exchange(sent.reshape(-1, *sent.shape[2:]), GROUP[1:])
     joint_other = lax.ppermute(joint, "core", [(0, 1), (1, 0)])
     held = jnp.concatenate(
@@ -333,25 +399,19 @@
     parts = attend(held, joint)
     parts = exchange(parts, GROUP)
 
-    mine, other = (weight_rows(whole, depth, wide, cores) for whole in (joint, joint_other))
-    lead = 16
-    edge = jnp.pad(edge, ((lead - (TAPS - 1), 0), (0, 0)))
-    edge = rms_scale(edge, pre_gain).astype(BF16)
-    low, high = jnp.split(jnp.concatenate([edge, normed], axis=0), 2, axis=1)
-    spread = jnp.dot(jnp.where(core == 0, low, high), mine, preferred_element_type=F32)
-    spread += jnp.dot(jnp.where(core == 0, high, low), other, preferred_element_type=F32)
-    outer_part, inner_part, signal = jnp.split(spread, 3, axis=1)
-    product = (inner_part * signal).astype(BF16).astype(F32)
-    convolved = sum(
-        product[lead - (TAPS - 1) + k : lead - (TAPS - 1) + k + rows] * conv_taps[k]
-        for k in range(TAPS)
+    conv_projected = convolve(
+        joint,
+        joint_other,
+        normed,
+        edge,
+        pre_gain.reshape(1, -1),
+        conv_taps,
+        conv_output,
     )
-    conv_mixed = (outer_part[lead:] * convolved).astype(BF16)
-    conv_projected = jnp.dot(conv_mixed, conv_output, preferred_element_type=F32)
-
-    projected, row_logsum = merge(parts, conv_projected, heads_output)
+    projected, top, log_total = merge(parts, conv_projected, heads_output)
     tp = lax.axis_size("tp")
     arrived = exchange(projected.reshape(tp, rows // tp, -1), "tp")
+    row_logsum = top + log_total
     projected = arrived.astype(F32).sum(axis=0)
     mixed = rms_scale(projected, post_gain).astype(BF16)
     return (mixed, row_logsum)

time: 167 us -> 164 us (0.982)
  the two profiles are of different devices: /device:TPU:1 before, /device:TPU:32 now
where the time goes in v6:
time: 164 us; the launch traced here: 163 us
  blocking collectives  49.3 us (30%)
  waiting for transfers between devices  48.5 us (30%)
  starting transfers between devices  34 us (21%)
  Pallas kernels  18.2 us (11%)
  local copies, waits for them, and re-layouts  6.49 us (4%)
  other arithmetic  4.56 us (3%)
    all_to_all x4, waiting for transfers between devices, exchange(): return lax.all_to_all(array, axis, split_axis=0, concat_axis=0, tiled=True)  36.6 us
    all_gather x1, blocking collectives, layer(): lax.all_gather(held, 'far', axis=0, tiled=True).reshape(-1, *held.shape)  36.1 us
    all_to_all x4, starting transfers between devices, exchange(): return lax.all_to_all(array, axis, split_axis=0, concat_axis=0, tiled=True)  28 us
    all_gather x1, blocking collectives, layer(): latents = lax.all_gather(latents, 'tp', axis=0)  13.2 us
    pallas_call x1, Pallas kernels, attend(): pl.pallas_call(attention_kernel, out_shape=jax.ShapeDtypeStruct((groups,...  9.37 us
    ppermute x1, waiting for transfers between devices, shifted(): lax.ppermute(value, axis, [(source, source + steps) for source in range(f...  7.98 us
    unnamed x30, local copies, waits for them, and re-layouts  5.3 us
    ppermute x1, waiting for transfers between devices, layer(): queries_other = lax.ppermute(queries, 'pair', [(0, 1), (1, 0)])  3.95 us
  transfers between devices with their start and end apart: 7, of which 4 were waited for; matrix products, arithmetic and copies ran while one was open for 2% of the time, Pallas kernels for 9%

profile of v6, /device:TPU:32, one launch (start us, length us, event | category | flops | bytes accessed | tf_op | source)
XLA Modules:
  0.0 162.9 jit_solution(13118850925308777504)
XLA Ops:
  0.7 1.6 spread_gates.1
  2.2 15.3 %all-to-all-start = ((bf16[16,96,128]{2,1,0:T(8,128)(2,1)}), bf16[16,96,128]{2,1,0:T(8,128)(2,1)S(1)}, u32[]{:S(2)}, u32[]{:S(2)}) async-start(bf16[16,96,128]{2,1,0:T(8,128)(2,1)} %spread_gates.1), calls=%async_computation | async-start | bytes 786432 | tf_op jit(solution)/shard_map/all_to_all | solution.py:30
  17.6 2.9 %entry.1 = (bf16[128,2048]{1,0:T(8,128)(2,1)}, bf16[128,320]{1,0:T(8,128)(2,1)}, f32[32,128]{1,0:T(8,128)}) custom-call(bf16[128,2048]{1,0:T(8,128)(2,1)} %tokens.1, f32[1,2048]{1,0:T(1,128)} %bitcast.42, bf16[2048,128]{1,0:T(8,128)(2,1)} %latent_down.1, bf16[192,2048]{1,0:T(8,128)(2,1)} %bitcast.48, bf16[32,2048]{1,0:T(8,128)(2,1)} %bitcast.53), custom_call_target="tpu_custom_call" | custom-call | flops 201326592 | bytes 2500000 | tf_op jit(solution)/shard_map/entry/pallas_call | solution.py:203
  20.5 13.2 %all-gather = bf16[512,320]{1,0:T(8,128)(2,1)S(1)} all-gather(bf16[128,320]{1,0:T(8,128)(2,1)} %get-tuple-element.8), channel_id=2, replica_groups=mesh['far'=8,'pair'=2,'x'=4,'core'=2,'tp'=4] {'tp'}, dimensions={0}, use_global_device_ids=true | all-gather | bytes 409600 | tf_op jit(solution)/shard_map/all_gather | solution.py:359
  34.1 0.2 fusion.4
  34.3 0.8 multiply_cosine_fusion
  35.3 0.3 fusion.2
  35.6 2.0 %collective-permute-start = (bf16[192,128]{1,0:T(8,128)(2,1)S(1)}, bf16[192,128]{1,0:T(8,128)(2,1)S(1)}, u32[]{:S(2)}, u32[]{:S(2)}) collective-permute-start(bf16[192,128]{1,0:T(8,128)(2,1)S(1)} %pad_maximum_fusion.3), channel_id=1, source_target_pairs={{0,32},{32,0},{1,33},{33,1},{2,34},{34,2},{3,35},{35,3},{4,36},{36... | collective-permute-start | bytes 147464 | tf_op jit(solution)/shard_map/ppermute | solution.py:376
  37.6 4.0 %collective-permute-done = bf16[192,128]{1,0:T(8,128)(2,1)S(1)} collective-permute-done((bf16[192,128]{1,0:T(8,128)(2,1)S(1)}, bf16[192,128]{1,0:T(8,128)(2,1)S(1)}, u32[]{:S(2)}, u32[]{:S(2)}) %collective-permute-start) | collective-permute-done | bytes 49184 | tf_op jit(solution)/shard_map/ppermute | solution.py:376
  41.8 0.2 broadcast_in_dim.4
  42.0 1.6 pad_maximum_fusion
  43.6 4.4 %all-to-all-start.1 = ((bf16[8,1152,128]{2,1,0:T(8,128)(2,1)}), bf16[8,1152,128]{2,1,0:T(8,128)(2,1)S(1)}, u32[]{:S(2)}, u32[]{:S(2)}) async-start(bf16[8,1152,128]{2,1,0:T(8,128)(2,1)} %bitcast.44), calls=%async_computation.1 | async-start | bytes 4718592 | tf_op jit(solution)/shard_map/all_to_all | solution.py:30
  48.4 0.2 fusion
  48.7 0.2 fusion.1
  48.9 29.1 %all-to-all-done.1.query_ref.mine_ref = bf16[8,1152,128]{2,1,0:T(8,128)(2,1)S(1)} async-done(((bf16[8,1152,128]{2,1,0:T(8,128)(2,1)}), bf16[8,1152,128]{2,1,0:T(8,128)(2,1)S(1)}, u32[]{:S(2)}, u32[]{:S(2)}) %all-to-all-start.1) | async-done | bytes 2359328 | tf_op jit(solution)/shard_map/all_to_all | solution.py:30
  78.0 1.9 %collective-permute-start.1 = (bf16[8,1152,128]{2,1,0:T(8,128)(2,1)S(1)}, bf16[8,1152,128]{2,1,0:T(8,128)(2,1)}, u32[]{:S(2)}, u32[]{:S(2)}) collective-permute-start(bf16[8,1152,128]{2,1,0:T(8,128)(2,1)S(1)} %all-to-all-done.1.query_ref.mine_ref), channel_id=1, source_target_pairs={{0,4},{4,0},{1,5},{5,1},{2,6},{6,2},{3,7},{7,3},{8,12},{12,8},{9,1... | collective-permute-start | bytes 7077896 | tf_op jit(solution)/shard_map/ppermute | solution.py:388
  79.9 36.1 %all_gather.11 = bf16[2304,128]{1,0:T(8,128)(2,1)} all-gather(bf16[288,128]{1,0:T(8,128)(2,1)S(1)} %pad_maximum_fusion.2), channel_id=1, replica_groups=mesh['far'=8,'pair'=2,'x'=4,'core'=2,'tp'=4] {'far'}, dimensions={0}, use_global_device_ids=true | all-gather | bytes 663552 | tf_op jit(solution)/shard_map/all_gather | solution.py:397
  116.0 9.4 %attend.1 = bf16[16,144,128]{2,1,0:T(8,128)(2,1)} custom-call(bf16[8,288,128]{2,1,0:T(8,128)(2,1)} %bitcast.49, bf16[8,1152,128]{2,1,0:T(8,128)(2,1)} %copy-done.1), custom_call_target="tpu_custom_call" | custom-call | flops 1879048192 | bytes 2000000 | tf_op jit(solution)/shard_map/attend/pallas_call | solution.py:138
  125.4 4.0 %all-to-all-start.2 = ((bf16[16,144,128]{2,1,0:T(8,128)(2,1)}), bf16[16,144,128]{2,1,0:T(8,128)(2,1)S(1)}, u32[]{:S(2)}, u32[]{:S(2)}) async-start(bf16[16,144,128]{2,1,0:T(8,128)(2,1)} %attend.1), calls=%async_computation.2 | async-start | bytes 1179648 | tf_op jit(solution)/shard_map/all_to_all | solution.py:30
  129.4 0.8 slice.27
  130.3 2.0 %collective-permute-start.2 = (bf16[16,2048]{1,0:T(8,128)(2,1)S(1)}, bf16[16,2048]{1,0:T(8,128)(2,1)S(1)}, u32[]{:S(2)}, u32[]{:S(2)}) collective-permute-start(bf16[16,2048]{1,0:T(8,128)(2,1)S(1)} %slice.27), channel_id=1, source_target_pairs={{0,4},{4,8},{8,12},{12,16},{16,20},{20,24},{24,28},{28,32},{32,36}... | collective-permute-start | bytes 196616 | tf_op jit(solution)/shard_map/ppermute | solution.py:36
  132.3 8.0 %collective-permute-done.2.edge_ref = bf16[16,2048]{1,0:T(8,128)(2,1)S(1)} collective-permute-done((bf16[16,2048]{1,0:T(8,128)(2,1)S(1)}, bf16[16,2048]{1,0:T(8,128)(2,1)S(1)}, u32[]{:S(2)}, u32[]{:S(2)}) %collective-permute-start.2) | collective-permute-done | bytes 65568 | tf_op jit(solution)/shard_map/ppermute | solution.py:36
  140.3 1.7 %copy-done.2 = bf16[8,1152,128]{2,1,0:T(8,128)(2,1)S(1)} copy-done((bf16[8,1152,128]{2,1,0:T(8,128)(2,1)S(1)}, bf16[8,1152,128]{2,1,0:T(8,128)(2,1)}, u32[]{:S(2)}) %copy-start.2) | copy-done | bytes 2359320
  142.0 1.2 copy-done.3
  143.2 1.0 copy-done.4
  144.2 3.0 %convolve.1.conv_ref = f32[128,2048]{1,0:T(8,128)S(1)} custom-call(bf16[8,1152,128]{2,1,0:T(8,128)(2,1)S(1)} %copy-done.2, bf16[8,1152,128]{2,1,0:T(8,128)(2,1)} %collective-permute-done.1.other_ref, bf16[128,2048]{1,0:T(8,128)(2,1)S(1)} %copy-done.4, bf16[16,2048]{1,0:T(8,128)(2,1)S(1)} %collective-permute-done.2.edge_ref, f32[1,2048]{1,0:T(1,128)S(1)} %bitcast.43, ...), custom_call_target="tpu_custom_call" | custom-call | flops 536870912 | bytes 6000000 | tf_op jit(solution)/shard_map/convolve/pallas_call | solution.py:266
  147.3 1.0 copy-done.5
  148.3 1.3 merge.1
  149.6 4.2 %all-to-all-start.3 = ((bf16[4,32,2048]{2,1,0:T(8,128)(2,1)}), bf16[4,32,2048]{2,1,0:T(8,128)(2,1)S(1)}, u32[]{:S(2)}, u32[]{:S(2)}) async-start(bf16[4,32,2048]{2,1,0:T(8,128)(2,1)} %bitcast.18), calls=%async_computation.3 | async-start | bytes 1048576 | tf_op jit(solution)/shard_map/all_to_all | solution.py:30
  153.8 0.6 add.66
  154.4 7.5 %all-to-all-done.3 = bf16[4,32,2048]{2,1,0:T(8,128)(2,1)S(1)} async-done(((bf16[4,32,2048]{2,1,0:T(8,128)(2,1)}), bf16[4,32,2048]{2,1,0:T(8,128)(2,1)S(1)}, u32[]{:S(2)}, u32[]{:S(2)}) %all-to-all-start.3) | async-done | bytes 524320 | tf_op jit(solution)/shard_map/all_to_all | solution.py:30
  162.2 0.8 multiply_convert_fusion
  (49 shorter events, 1.3 us)
Async XLA Ops:
  0.6 34.7 %copy-start = (bf16[768,128]{1,0:T(8,128)(2,1)S(1)}, bf16[768,128]{1,0:T(8,128)(2,1)}, u32[]{:S(2)}) copy-start(bf16[768,128]{1,0:T(8,128)(2,1)} %param.29) | copy-start | bytes 589828
  0.6 33.4 %copy-start.12 = (f32[768]{0:T(1024)S(1)}, f32[768]{0:T(1024)}, u32[]{:S(2)}) copy-start(f32[768]{0:T(1024)} %param.27) | copy-start | bytes 9220
  2.2 32.9 %copy-start.10 = (bf16[768,64]{0,1:T(8,128)(2,1)S(1)}, bf16[768,64]{0,1:T(8,128)(2,1)}, u32[]{:S(2)}) copy-start(bf16[768,64]{0,1:T(8,128)(2,1)} %param.30) | copy-start | bytes 294916
  2.2 39.4 %all-to-all-start = ((bf16[16,96,128]{2,1,0:T(8,128)(2,1)}), bf16[16,96,128]{2,1,0:T(8,128)(2,1)S(1)}, u32[]{:S(2)}, u32[]{:S(2)}) async-start(bf16[16,96,128]{2,1,0:T(8,128)(2,1)} %spread_gates.1), calls=%async_computation | async-start | bytes 786432 | tf_op jit(solution)/shard_map/all_to_all | solution.py:30
  35.6 6.0 %collective-permute-start = (bf16[192,128]{1,0:T(8,128)(2,1)S(1)}, bf16[192,128]{1,0:T(8,128)(2,1)S(1)}, u32[]{:S(2)}, u32[]{:S(2)}) collective-permute-start(bf16[192,128]{1,0:T(8,128)(2,1)S(1)} %pad_maximum_fusion.3), channel_id=1, source_target_pairs={{0,32},{32,0},{1,33},{33,1},{2,34},{34,2},{3,35},{35,3},{4,36},{36... | collective-permute-start | bytes 147464 | tf_op jit(solution)/shard_map/ppermute | solution.py:376
  43.6 4.7 %copy-start.13 = (f32[512]{0:T(512)S(1)}, f32[512]{0:T(512)}, u32[]{:S(2)}) copy-start(f32[512]{0:T(512)} %param.28) | copy-start | bytes 6148
  43.6 4.8 %copy-start.8 = (bf16[512,128]{1,0:T(8,128)(2,1)S(1)}, bf16[512,128]{1,0:T(8,128)(2,1)}, u32[]{:S(2)}) copy-start(bf16[512,128]{1,0:T(8,128)(2,1)} %param.31) | copy-start | bytes 393220
  43.6 5.1 %copy-start.9 = (bf16[512,128]{1,0:T(8,128)(2,1)S(1)}, bf16[512,128]{1,0:T(8,128)(2,1)}, u32[]{:S(2)}) copy-start(bf16[512,128]{1,0:T(8,128)(2,1)} %param.32) | copy-start | bytes 393220
  43.6 34.4 %all-to-all-start.1 = ((bf16[8,1152,128]{2,1,0:T(8,128)(2,1)}), bf16[8,1152,128]{2,1,0:T(8,128)(2,1)S(1)}, u32[]{:S(2)}, u32[]{:S(2)}) async-start(bf16[8,1152,128]{2,1,0:T(8,128)(2,1)} %bitcast.44), calls=%async_computation.1 | async-start | bytes 4718592 | tf_op jit(solution)/shard_map/all_to_all | solution.py:30
  78.0 38.0 %copy-start.1 = (bf16[8,1152,128]{2,1,0:T(8,128)(2,1)}, bf16[8,1152,128]{2,1,0:T(8,128)(2,1)S(1)}, u32[]{:S(2)}) copy-start(bf16[8,1152,128]{2,1,0:T(8,128)(2,1)S(1)} %all-to-all-done.1.query_ref.mine_ref) | copy-start | bytes 7077892
  78.0 62.3 %collective-permute-start.1 = (bf16[8,1152,128]{2,1,0:T(8,128)(2,1)S(1)}, bf16[8,1152,128]{2,1,0:T(8,128)(2,1)}, u32[]{:S(2)}, u32[]{:S(2)}) collective-permute-start(bf16[8,1152,128]{2,1,0:T(8,128)(2,1)S(1)} %all-to-all-done.1.query_ref.mine_ref), channel_id=1, source_target_pairs={{0,4},{4,0},{1,5},{5,1},{2,6},{6,2},{3,7},{7,3},{8,12},{12,8},{9,1... | collective-permute-start | bytes 7077896 | tf_op jit(solution)/shard_map/ppermute | solution.py:388
  116.0 24.3 %copy-start.6 = (f32[2048]{0:T(1024)S(1)}, f32[2048]{0:T(1024)}, u32[]{:S(2)}) copy-start(f32[2048]{0:T(1024)} %param.19) | copy-start | bytes 24580
  116.0 24.3 %copy-start.7 = (f32[3,256]{1,0:T(4,128)S(1)}, f32[3,256]{1,0:T(4,128)}, u32[]{:S(2)}) copy-start(f32[3,256]{1,0:T(4,128)} %taps_ref.1) | copy-start | bytes 9220
  125.4 21.9 %all-to-all-start.2 = ((bf16[16,144,128]{2,1,0:T(8,128)(2,1)}), bf16[16,144,128]{2,1,0:T(8,128)(2,1)S(1)}, u32[]{:S(2)}, u32[]{:S(2)}) async-start(bf16[16,144,128]{2,1,0:T(8,128)(2,1)} %attend.1), calls=%async_computation.2 | async-start | bytes 1179648 | tf_op jit(solution)/shard_map/all_to_all | solution.py:30
  130.3 10.0 %collective-permute-start.2 = (bf16[16,2048]{1,0:T(8,128)(2,1)S(1)}, bf16[16,2048]{1,0:T(8,128)(2,1)S(1)}, u32[]{:S(2)}, u32[]{:S(2)}) collective-permute-start(bf16[16,2048]{1,0:T(8,128)(2,1)S(1)} %slice.27), channel_id=1, source_target_pairs={{0,4},{4,8},{8,12},{12,16},{16,20},{20,24},{24,28},{28,32},{32,36}... | collective-permute-start | bytes 196616 | tf_op jit(solution)/shard_map/ppermute | solution.py:36
  140.3 1.7 %copy-start.2 = (bf16[8,1152,128]{2,1,0:T(8,128)(2,1)S(1)}, bf16[8,1152,128]{2,1,0:T(8,128)(2,1)}, u32[]{:S(2)}) copy-start(bf16[8,1152,128]{2,1,0:T(8,128)(2,1)} %copy-done.1) | copy-start | bytes 7077892
  142.0 1.2 copy-start.3
  143.2 1.0 copy-start.4
  147.3 1.0 copy-start.5
  148.3 13.8 %copy-start.11 = (f32[2048]{0:T(1024)S(1)}, f32[2048]{0:T(1024)}, u32[]{:S(2)}) copy-start(f32[2048]{0:T(1024)} %param.35) | copy-start | bytes 24580
  149.6 12.3 %all-to-all-start.3 = ((bf16[4,32,2048]{2,1,0:T(8,128)(2,1)}), bf16[4,32,2048]{2,1,0:T(8,128)(2,1)S(1)}, u32[]{:S(2)}, u32[]{:S(2)}) async-start(bf16[4,32,2048]{2,1,0:T(8,128)(2,1)} %bitcast.18), calls=%async_computation.3 | async-start | bytes 1048576 | tf_op jit(solution)/shard_map/all_to_all | solution.py:30

commit v7 on v6

--- a/solution.py
+++ b/solution.py
@@ -137,7 +137,7 @@
     width = 2 * groups * 128
     return pl.pallas_call(
         attention_kernel,
-        out_shape=jax.ShapeDtypeStruct((groups, PART_ROWS, 128), BF16),
+        out_shape=pltpu.HBM((groups, PART_ROWS, 128), BF16),
         grid=(1,),
         in_specs=[
             pl.BlockSpec(held.shape, lambda i: (0, 0, 0)),
@@ -149,7 +149,7 @@
             pltpu.VMEM((128, blocks * 128), BF16),
             pltpu.VMEM((160, width), BF16),
         ],
-        compiler_params=pltpu.CompilerParams(vmem_limit_bytes=56 << 20),
+        compiler_params=pltpu.CompilerParams(vmem_limit_bytes=48 << 20),
         cost_estimate=pl.CostEstimate(
             flops=2 * blocks * 128 * width * (160 + 64),
             bytes_accessed=2_000_000,
@@ -184,11 +184,14 @@
     )(*gates)
 
 
-def entry_kernel(tokens, gain, latent_down, query_down, rotary_down, normed_ref, latent_ref, rot_ref):
+def entry_kernel(
+    tokens, gain, latent_down, query_down, rotary_down, normed_ref, tail_ref, latent_ref, rot_ref
+):
     wide = tokens[...].astype(F32)
     scale = lax.rsqrt(jnp.mean(wide * wide, axis=-1, keepdims=True) + eps)
     normed = (wide * scale * gain[...]).astype(BF16)
     normed_ref[...] = normed
+    tail_ref[...] = normed[normed.shape[0] - LEAD :, :]
     n = latent_down.shape[1]
     latent_ref[:, :n] = jnp.dot(
         normed, latent_down[...], preferred_element_type=F32
@@ -204,6 +207,7 @@
         entry_kernel,
         out_shape=(
             jax.ShapeDtypeStruct((rows, width), BF16),
+            jax.ShapeDtypeStruct((LEAD, width), BF16),
             jax.ShapeDtypeStruct((rows, columns), BF16),
             jax.ShapeDtypeStruct((ROPE, rows), F32),
         ),
@@ -218,16 +222,14 @@
 
 
 def conv_kernel(
-    mine_ref, other_ref, normed_ref, edge_ref, gain_ref, taps_ref, output_ref, out_ref,
+    mine_ref, other_ref, normed_ref, edge_ref, taps_ref, output_ref, out_ref,
     rows_ref, weight_ref, product_ref,
 ):
     core = lax.axis_index("core")
     near, _, _ = mine_ref.shape
     count, width = normed_ref.shape
     half = width // 2
-    wide = edge_ref[...].astype(F32)
-    scale = lax.rsqrt(jnp.mean(wide * wide, axis=-1, keepdims=True) + eps)
-    rows_ref[:LEAD, :] = (wide * scale * gain_ref[...]).astype(BF16)
+    rows_ref[:LEAD, :] = edge_ref[...]
     rows_ref[LEAD:, :] = normed_ref[...]
     columns = weight_ref.shape[1]
     depth = 128 // near
@@ -257,15 +259,15 @@
         out_ref[:, at] = jnp.dot(mixed, output_ref[:, at], preferred_element_type=F32)
 
 
-def convolve(joint, joint_other, normed, edge, gain, taps, output):
+def convolve(joint, joint_other, normed, edge, taps, output):
     count, width = normed.shape
     third, out_width = output.shape
     near = joint.shape[0]
     weights = pl.BlockSpec((near, joint.shape[1] - 2 * QUERY_ROWS, 128), lambda i: (0, 0, 0))
-    whole = [pl.BlockSpec(a.shape, lambda i: (0, 0)) for a in (normed, edge, gain, taps, output)]
+    whole = [pl.BlockSpec(a.shape, lambda i: (0, 0)) for a in (normed, edge, taps, output)]
     return pl.pallas_call(
         conv_kernel,
-        out_shape=jax.ShapeDtypeStruct((count, out_width), F32),
+        out_shape=pltpu.HBM((count, out_width), F32),
         grid=(1,),
         in_specs=[weights, weights, *whole],
         out_specs=pl.BlockSpec((count, out_width), lambda i: (0, 0)),
@@ -281,7 +283,14 @@
         ),
         compiler_params=pltpu.CompilerParams(vmem_limit_bytes=30 << 20),
         name="convolve",
-    )(joint, joint_other, normed, edge, gain, taps, output)
+    )(
+        joint,
+        joint_other,
+        pltpu.with_memory_space_constraint(normed, pltpu.HBM),
+        edge,
+        taps,
+        pltpu.with_memory_space_constraint(output, pltpu.HBM),
+    )
 
 
 def merge_kernel(parts_ref, conv_ref, weight_ref, out_ref, top_ref, log_ref):
@@ -324,7 +333,11 @@
         ),
         compiler_params=pltpu.CompilerParams(vmem_limit_bytes=16 << 20),
         name="merge",
-    )(parts, conv_projected, heads_output)
+    )(
+        parts,
+        pltpu.with_memory_space_constraint(conv_projected, pltpu.HBM),
+        pltpu.with_memory_space_constraint(heads_output, pltpu.HBM),
+    )
 
 
 def layer(
@@ -353,9 +366,8 @@
     gates = spread_gates((outer_gate, inner_gate, conv_input), lax.axis_size(Z))
     gates = exchange(gates, Z)
 
-    edge = shifted(tokens[rows - LEAD :], SP, 1)
-
-    normed, latents, key_raw = entry(tokens, pre_gain, latent_down, query_down, rotary_down)
+    normed, tail, latents, key_raw = entry(tokens, pre_gain, latent_down, query_down, rotary_down)
+    edge = shifted(tail, SP, 1)
     latents = lax.all_gather(latents, "tp", axis=0)
 
     positions = sp_index * rows + jnp.arange(rows, dtype=jnp.int32)
@@ -404,7 +416,6 @@
         joint_other,
         normed,
         edge,
-        pre_gain.reshape(1, -1),
         conv_taps,
         conv_output,
     )

time: 164 us -> 158 us (0.963)
  the two profiles are of different devices: /device:TPU:32 before, /device:TPU:1 now
where the time goes in v7:
time: 158 us; the launch traced here: 156 us
  starting transfers between devices  45.3 us (29%)
  waiting for transfers between devices  42.7 us (27%)
  blocking collectives  41.7 us (26%)
  Pallas kernels  19.8 us (13%)
  other arithmetic  4.55 us (3%)
    all_to_all x4, waiting for transfers between devices, exchange(): return lax.all_to_all(array, axis, split_axis=0, concat_axis=0, tiled=True)  37 us
    all_to_all x4, starting transfers between devices, exchange(): return lax.all_to_all(array, axis, split_axis=0, concat_axis=0, tiled=True)  35.5 us
    all_gather x1, blocking collectives, layer(): lax.all_gather(held, 'far', axis=0, tiled=True).reshape(-1, *held.shape)  30 us
    all_gather x1, blocking collectives, layer(): latents = lax.all_gather(latents, 'tp', axis=0)  11.8 us
    pallas_call x1, Pallas kernels, attend(): pl.pallas_call(attention_kernel, out_shape=pltpu.HBM((groups, PART_ROWS,...  8.13 us
    pallas_call x1, Pallas kernels, convolve(): pl.pallas_call(conv_kernel, out_shape=pltpu.HBM((count, out_width), F32),...  4.48 us
    ppermute x1, waiting for transfers between devices, shifted(): lax.ppermute(value, axis, [(source, source + steps) for source in range(f...  3.83 us
    ppermute x1, starting transfers between devices, shifted(): lax.ppermute(value, axis, [(source, source + steps) for source in range(f...  3.55 us
  transfers between devices with their start and end apart: 7, of which 4 were waited for; matrix products, arithmetic and copies ran while one was open for 2% of the time, Pallas kernels for 10%

profile of v7, /device:TPU:1, one launch (start us, length us, event | category | flops | bytes accessed | tf_op | source)
XLA Modules:
  0.0 156.5 jit_solution(4001054391077313793)
XLA Ops:
  0.7 1.6 %spread_gates.1 = bf16[16,96,128]{2,1,0:T(8,128)(2,1)} custom-call(bf16[16,256]{1,0:T(8,128)(2,1)} %outer_ref.1, bf16[16,256]{1,0:T(8,128)(2,1)} %inner_ref.1, bf16[16,256]{1,0:T(8,128)(2,1)} %signal_ref.1), custom_call_target="tpu_custom_call" | custom-call | flops 1000000 | bytes 400000 | tf_op jit(solution)/shard_map/spread_gates/pallas_call | solution.py:179
  2.2 15.9 %all-to-all-start = ((bf16[16,96,128]{2,1,0:T(8,128)(2,1)}), bf16[16,96,128]{2,1,0:T(8,128)(2,1)S(1)}, u32[]{:S(2)}, u32[]{:S(2)}) async-start(bf16[16,96,128]{2,1,0:T(8,128)(2,1)} %spread_gates.1), calls=%async_computation | async-start | bytes 786432 | tf_op jit(solution)/shard_map/all_to_all | solution.py:30
  18.1 2.9 %entry.1 = (bf16[128,2048]{1,0:T(8,128)(2,1)}, bf16[16,2048]{1,0:T(8,128)(2,1)}, bf16[128,320]{1,0:T(8,128)(2,1)}, f32[32,128]{1,0:T(8,128)}) custom-call(bf16[128,2048]{1,0:T(8,128)(2,1)} %tokens.1, f32[1,2048]{1,0:T(1,128)} %bitcast.52, bf16[2048,128]{1,0:T(8,128)(2,1)} %latent_down.1, bf16[192,2048]{1,0:T(8,128)(2,1)} %bitcast.47, bf16[32,2048]{1,0:T(8,128)(2,1)} %bitcast.51), custom_call_target="tpu_custom_call" | custom-call | flops 201326592 | bytes 2500000 | tf_op jit(solution)/shard_map/entry/pallas_call | solution.py:206
  21.1 11.8 %all-gather = bf16[512,320]{1,0:T(8,128)(2,1)S(1)} all-gather(bf16[128,320]{1,0:T(8,128)(2,1)} %get-tuple-element.9), channel_id=2, replica_groups=mesh['far'=8,'pair'=2,'x'=4,'core'=2,'tp'=4] {'tp'}, dimensions={0}, use_global_device_ids=true | all-gather | bytes 409600 | tf_op jit(solution)/shard_map/all_gather | solution.py:371
  32.9 0.2 copy.23
  33.2 0.2 fusion.4
  33.3 0.8 multiply_cosine_fusion
  34.2 0.2 fusion.7
  34.4 0.3 fusion.2
  34.7 3.4 %collective-permute-start = (bf16[192,128]{1,0:T(8,128)(2,1)S(1)}, bf16[192,128]{1,0:T(8,128)(2,1)S(1)}, u32[]{:S(2)}, u32[]{:S(2)}) collective-permute-start(bf16[192,128]{1,0:T(8,128)(2,1)S(1)} %pad_maximum_fusion.3), channel_id=1, source_target_pairs={{0,32},{32,0},{1,33},{33,1},{2,34},{34,2},{3,35},{35,3},{4,36},{36... | collective-permute-start | bytes 147464 | tf_op jit(solution)/shard_map/ppermute | solution.py:388
  38.0 1.9 %collective-permute-done = bf16[192,128]{1,0:T(8,128)(2,1)S(1)} collective-permute-done((bf16[192,128]{1,0:T(8,128)(2,1)S(1)}, bf16[192,128]{1,0:T(8,128)(2,1)S(1)}, u32[]{:S(2)}, u32[]{:S(2)}) %collective-permute-start) | collective-permute-done | bytes 49184 | tf_op jit(solution)/shard_map/ppermute | solution.py:388
  40.1 0.2 broadcast_in_dim.4
  40.3 1.6 %pad_maximum_fusion = bf16[4,2,1152,128]{3,2,1,0:T(8,128)(2,1)} fusion(bf16[4,2,384,128]{3,2,1,0:T(8,128)(2,1)S(1)} %broadcast_in_dim.5, bf16[4,2,768,128]{3,2,1,0:T(8,128)(2,1)S(1)} %broadcast_in_dim.4), kind=kLoop, calls=%fused_computation | loop fusion | flops 4718592 | bytes 4718592 | tf_op jit(solution)/shard_map/concatenate | solution.py:398
  41.9 7.6 %all-to-all-start.1 = ((bf16[8,1152,128]{2,1,0:T(8,128)(2,1)}), bf16[8,1152,128]{2,1,0:T(8,128)(2,1)S(1)}, u32[]{:S(2)}, u32[]{:S(2)}) async-start(bf16[8,1152,128]{2,1,0:T(8,128)(2,1)} %bitcast.43), calls=%async_computation.1 | async-start | bytes 4718592 | tf_op jit(solution)/shard_map/all_to_all | solution.py:30
  49.5 0.1 copy.22
  49.7 0.1 fusion.6
  49.9 0.2 fusion
  50.1 0.2 fusion.1
  50.4 28.1 %all-to-all-done.1.query_ref.mine_ref = bf16[8,1152,128]{2,1,0:T(8,128)(2,1)S(1)} async-done(((bf16[8,1152,128]{2,1,0:T(8,128)(2,1)}), bf16[8,1152,128]{2,1,0:T(8,128)(2,1)S(1)}, u32[]{:S(2)}, u32[]{:S(2)}) %all-to-all-start.1) | async-done | bytes 2359328 | tf_op jit(solution)/shard_map/all_to_all | solution.py:30
  78.5 2.9 %collective-permute-start.1 = (bf16[8,1152,128]{2,1,0:T(8,128)(2,1)S(1)}, bf16[8,1152,128]{2,1,0:T(8,128)(2,1)}, u32[]{:S(2)}, u32[]{:S(2)}) collective-permute-start(bf16[8,1152,128]{2,1,0:T(8,128)(2,1)S(1)} %all-to-all-done.1.query_ref.mine_ref), channel_id=1, source_target_pairs={{0,4},{4,0},{1,5},{5,1},{2,6},{6,2},{3,7},{7,3},{8,12},{12,8},{9,1... | collective-permute-start | bytes 7077896 | tf_op jit(solution)/shard_map/ppermute | solution.py:400
  81.4 30.0 %all_gather.11 = bf16[2304,128]{1,0:T(8,128)(2,1)S(1)} all-gather(bf16[288,128]{1,0:T(8,128)(2,1)S(1)} %pad_maximum_fusion.2), channel_id=1, replica_groups=mesh['far'=8,'pair'=2,'x'=4,'core'=2,'tp'=4] {'far'}, dimensions={0}, use_global_device_ids=true | all-gather | bytes 663552 | tf_op jit(solution)/shard_map/all_gather | solution.py:409
  111.3 8.1 %attend.1 = bf16[16,144,128]{2,1,0:T(8,128)(2,1)} custom-call(bf16[8,288,128]{2,1,0:T(8,128)(2,1)S(1)} %bitcast.42, bf16[8,1152,128]{2,1,0:T(8,128)(2,1)S(1)} %all-to-all-done.1.query_ref.mine_ref), custom_call_target="tpu_custom_call" | custom-call | flops 1879048192 | bytes 2000000 | tf_op jit(solution)/shard_map/attend/pallas_call | solution.py:138
  119.5 8.2 %all-to-all-start.2 = ((bf16[16,144,128]{2,1,0:T(8,128)(2,1)}), bf16[16,144,128]{2,1,0:T(8,128)(2,1)S(1)}, u32[]{:S(2)}, u32[]{:S(2)}) async-start(bf16[16,144,128]{2,1,0:T(8,128)(2,1)} %attend.1), calls=%async_computation.2 | async-start | bytes 1179648 | tf_op jit(solution)/shard_map/all_to_all | solution.py:30
  127.7 3.5 %collective-permute-start.2 = (bf16[16,2048]{1,0:T(8,128)(2,1)S(1)}, bf16[16,2048]{1,0:T(8,128)(2,1)S(1)}, u32[]{:S(2)}, u32[]{:S(2)}) collective-permute-start(bf16[16,2048]{1,0:T(8,128)(2,1)S(1)} %copy-done.8), channel_id=1, source_target_pairs={{0,4},{4,8},{8,12},{12,16},{16,20},{20,24},{24,28},{28,32},{32,36}... | collective-permute-start | bytes 196616 | tf_op jit(solution)/shard_map/ppermute | solution.py:36
  131.2 3.8 %collective-permute-done.2.edge_ref = bf16[16,2048]{1,0:T(8,128)(2,1)S(1)} collective-permute-done((bf16[16,2048]{1,0:T(8,128)(2,1)S(1)}, bf16[16,2048]{1,0:T(8,128)(2,1)S(1)}, u32[]{:S(2)}, u32[]{:S(2)}) %collective-permute-start.2) | collective-permute-done | bytes 65568 | tf_op jit(solution)/shard_map/ppermute | solution.py:36
  135.1 4.5 %convolve.1.conv_ref = f32[128,2048]{1,0:T(8,128)} custom-call(bf16[8,1152,128]{2,1,0:T(8,128)(2,1)S(1)} %all-to-all-done.1.query_ref.mine_ref, bf16[8,1152,128]{2,1,0:T(8,128)(2,1)} %collective-permute-done.1.other_ref, bf16[128,2048]{1,0:T(8,128)(2,1)} %get-tuple-element.11.normed_ref, bf16[16,2048]{1,0:T(8,128)(2,1)S(1)} %collective-permute-done.2.edge_ref, ...), custom_call_target="tpu_custom_call" | custom-call | flops 536870912 | bytes 6000000 | tf_op jit(solution)/shard_map/convolve/pallas_call | solution.py:268
  139.6 2.7 %merge.1 = (bf16[128,2048]{1,0:T(8,128)(2,1)}, f32[2,128]{1,0:T(2,128)S(1)}, f32[2,128]{1,0:T(2,128)S(1)}) custom-call(bf16[16,144,128]{2,1,0:T(8,128)(2,1)S(1)} %all-to-all-done.2.parts_ref, f32[128,2048]{1,0:T(8,128)} %convolve.1.conv_ref, bf16[128,2048]{1,0:T(8,128)(2,1)} %weight_ref.1), custom_call_target="tpu_custom_call" | custom-call | flops 67108864 | bytes 2000000 | tf_op jit(solution)/shard_map/merge/pallas_call | solution.py:324
  142.2 3.9 %all-to-all-start.3 = ((bf16[4,32,2048]{2,1,0:T(8,128)(2,1)}), bf16[4,32,2048]{2,1,0:T(8,128)(2,1)S(1)}, u32[]{:S(2)}, u32[]{:S(2)}) async-start(bf16[4,32,2048]{2,1,0:T(8,128)(2,1)} %bitcast.18), calls=%async_computation.3 | async-start | bytes 1048576 | tf_op jit(solution)/shard_map/all_to_all | solution.py:30
  146.1 0.6 add.66
  146.7 8.9 %all-to-all-done.3 = bf16[4,32,2048]{2,1,0:T(8,128)(2,1)S(1)} async-done(((bf16[4,32,2048]{2,1,0:T(8,128)(2,1)}), bf16[4,32,2048]{2,1,0:T(8,128)(2,1)S(1)}, u32[]{:S(2)}, u32[]{:S(2)}) %all-to-all-start.3) | async-done | bytes 524320 | tf_op jit(solution)/shard_map/all_to_all | solution.py:30
  155.6 0.1 multiply_reduce_fusion.1
  155.7 0.8 multiply_convert_fusion
  (38 shorter events, 0.6 us)
Async XLA Ops:
  0.6 33.8 %copy-start = (bf16[768,128]{1,0:T(8,128)(2,1)S(1)}, bf16[768,128]{1,0:T(8,128)(2,1)}, u32[]{:S(2)}) copy-start(bf16[768,128]{1,0:T(8,128)(2,1)} %param.29) | copy-start | bytes 589828
  0.6 32.5 %copy-start.6 = (f32[768]{0:T(1024)S(1)}, f32[768]{0:T(1024)}, u32[]{:S(2)}) copy-start(f32[768]{0:T(1024)} %param.27) | copy-start | bytes 9220
  2.2 31.9 %copy-start.4 = (bf16[768,64]{0,1:T(8,128)(2,1)S(1)}, bf16[768,64]{0,1:T(8,128)(2,1)}, u32[]{:S(2)}) copy-start(bf16[768,64]{0,1:T(8,128)(2,1)} %param.30) | copy-start | bytes 294916
  2.2 37.8 %all-to-all-start = ((bf16[16,96,128]{2,1,0:T(8,128)(2,1)}), bf16[16,96,128]{2,1,0:T(8,128)(2,1)S(1)}, u32[]{:S(2)}, u32[]{:S(2)}) async-start(bf16[16,96,128]{2,1,0:T(8,128)(2,1)} %spread_gates.1), calls=%async_computation | async-start | bytes 786432 | tf_op jit(solution)/shard_map/all_to_all | solution.py:30
  34.7 5.3 %collective-permute-start = (bf16[192,128]{1,0:T(8,128)(2,1)S(1)}, bf16[192,128]{1,0:T(8,128)(2,1)S(1)}, u32[]{:S(2)}, u32[]{:S(2)}) collective-permute-start(bf16[192,128]{1,0:T(8,128)(2,1)S(1)} %pad_maximum_fusion.3), channel_id=1, source_target_pairs={{0,32},{32,0},{1,33},{33,1},{2,34},{34,2},{3,35},{35,3},{4,36},{36... | collective-permute-start | bytes 147464 | tf_op jit(solution)/shard_map/ppermute | solution.py:388
  41.9 7.8 %copy-start.7 = (f32[512]{0:T(512)S(1)}, f32[512]{0:T(512)}, u32[]{:S(2)}) copy-start(f32[512]{0:T(512)} %param.28) | copy-start | bytes 6148
  41.9 8.0 %copy-start.2 = (bf16[512,128]{1,0:T(8,128)(2,1)S(1)}, bf16[512,128]{1,0:T(8,128)(2,1)}, u32[]{:S(2)}) copy-start(bf16[512,128]{1,0:T(8,128)(2,1)} %param.31) | copy-start | bytes 393220
  41.9 8.2 %copy-start.3 = (bf16[512,128]{1,0:T(8,128)(2,1)S(1)}, bf16[512,128]{1,0:T(8,128)(2,1)}, u32[]{:S(2)}) copy-start(bf16[512,128]{1,0:T(8,128)(2,1)} %param.32) | copy-start | bytes 393220
  41.9 36.6 %all-to-all-start.1 = ((bf16[8,1152,128]{2,1,0:T(8,128)(2,1)}), bf16[8,1152,128]{2,1,0:T(8,128)(2,1)S(1)}, u32[]{:S(2)}, u32[]{:S(2)}) async-start(bf16[8,1152,128]{2,1,0:T(8,128)(2,1)} %bitcast.43), calls=%async_computation.1 | async-start | bytes 4718592 | tf_op jit(solution)/shard_map/all_to_all | solution.py:30
  78.5 56.6 %collective-permute-start.1 = (bf16[8,1152,128]{2,1,0:T(8,128)(2,1)S(1)}, bf16[8,1152,128]{2,1,0:T(8,128)(2,1)}, u32[]{:S(2)}, u32[]{:S(2)}) collective-permute-start(bf16[8,1152,128]{2,1,0:T(8,128)(2,1)S(1)} %all-to-all-done.1.query_ref.mine_ref), channel_id=1, source_target_pairs={{0,4},{4,0},{1,5},{5,1},{2,6},{6,2},{3,7},{7,3},{8,12},{12,8},{9,1... | collective-permute-start | bytes 7077896 | tf_op jit(solution)/shard_map/ppermute | solution.py:400
  111.3 16.4 %copy-start.8 = (bf16[16,2048]{1,0:T(8,128)(2,1)S(1)}, bf16[16,2048]{1,0:T(8,128)(2,1)}, u32[]{:S(2)}) copy-start(bf16[16,2048]{1,0:T(8,128)(2,1)} %get-tuple-element.12) | copy-start | bytes 196612
  111.3 23.8 %copy-start.1 = (f32[3,256]{1,0:T(4,128)S(1)}, f32[3,256]{1,0:T(4,128)}, u32[]{:S(2)}) copy-start(f32[3,256]{1,0:T(4,128)} %taps_ref.1) | copy-start | bytes 9220
  119.5 20.1 %all-to-all-start.2 = ((bf16[16,144,128]{2,1,0:T(8,128)(2,1)}), bf16[16,144,128]{2,1,0:T(8,128)(2,1)S(1)}, u32[]{:S(2)}, u32[]{:S(2)}) async-start(bf16[16,144,128]{2,1,0:T(8,128)(2,1)} %attend.1), calls=%async_computation.2 | async-start | bytes 1179648 | tf_op jit(solution)/shard_map/all_to_all | solution.py:30
  127.7 7.4 %collective-permute-start.2 = (bf16[16,2048]{1,0:T(8,128)(2,1)S(1)}, bf16[16,2048]{1,0:T(8,128)(2,1)S(1)}, u32[]{:S(2)}, u32[]{:S(2)}) collective-permute-start(bf16[16,2048]{1,0:T(8,128)(2,1)S(1)} %copy-done.8), channel_id=1, source_target_pairs={{0,4},{4,8},{8,12},{12,16},{16,20},{20,24},{24,28},{28,32},{32,36}... | collective-permute-start | bytes 196616 | tf_op jit(solution)/shard_map/ppermute | solution.py:36
  139.6 16.2 %copy-start.5 = (f32[2048]{0:T(1024)S(1)}, f32[2048]{0:T(1024)}, u32[]{:S(2)}) copy-start(f32[2048]{0:T(1024)} %param.35) | copy-start | bytes 24580
  142.2 13.3 %all-to-all-start.3 = ((bf16[4,32,2048]{2,1,0:T(8,128)(2,1)}), bf16[4,32,2048]{2,1,0:T(8,128)(2,1)S(1)}, u32[]{:S(2)}, u32[]{:S(2)}) async-start(bf16[4,32,2048]{2,1,0:T(8,128)(2,1)} %bitcast.18), calls=%async_computation.3 | async-start | bytes 1048576 | tf_op jit(solution)/shard_map/all_to_all | solution.py:30

commit v8 on v7

--- a/solution.py
+++ b/solution.py
@@ -68,6 +68,7 @@
     near = query_ref.shape[0]
     groups = 2 * near
     queries = groups * 128
+    pair = lax.axis_index("pair")
     for b in range(blocks):
         key_rows[b * 128 : (b + 1) * 128, :] = held_ref[b, 0:160, :].T
         value_cols[:, b * 128 : (b + 1) * 128] = held_ref[b, 160:288, :]
@@ -92,7 +93,9 @@
         )
 
     def soften(first, scores):
-        col = lax.broadcasted_iota(jnp.int32, (1, COLS), 1) + first % queries
+        side = pair if first % queries < near * 128 else 1 - pair
+        col = lax.broadcasted_iota(jnp.int32, (1, COLS), 1) + first % (near * 128)
+        col = col + side * (near * 128)
         scores = jnp.where(key_at <= col, scores, LOW)
         best = jnp.maximum(jnp.max(scores, axis=0, keepdims=True), FLOOR)
         weights = jnp.exp2(scores * factor - best * factor)
@@ -113,13 +116,15 @@
         tail = jnp.concatenate([high, middle, low, jnp.zeros((5, COLS), F32)], axis=0)
         for i in range(COLS // 128):
             g = first % queries // 128 + i
+            side = pair if g < near else 1 - pair
+            to = side * near + g % near
             at = slice(i * 128, (i + 1) * 128)
-            out_ref[g, h * 64 : (h + 1) * 64, :] = mixed[:, at]
+            out_ref[to, h * 64 : (h + 1) * 64, :] = mixed[:, at]
             if h == 0:
                 logs[g] = tail[:, at]
             else:
                 both = jnp.concatenate([logs.pop(g), tail[:, at]], axis=0)
-                out_ref[g, 128:PART_ROWS, :] = both.astype(BF16)
+                out_ref[to, 128:PART_ROWS, :] = both.astype(BF16)
 
     tiles = 2 * queries // COLS
     scores, softened = {}, {}
@@ -293,34 +298,36 @@
     )
 
 
-def merge_kernel(parts_ref, conv_ref, weight_ref, out_ref, top_ref, log_ref):
-    groups = parts_ref.shape[0]
-    tails = parts_ref[:, 128:PART_ROWS, :].astype(F32)
-    heads = []
-    for h in range(2):
-        logs = tails[:, 8 * h, :] + (tails[:, 8 * h + 1, :] + tails[:, 8 * h + 2, :])
-        top = jnp.max(logs, axis=0, keepdims=True)
-        share = jnp.exp(logs - top)
-        share_sum = jnp.sum(share, axis=0, keepdims=True)
-        top_ref[h : h + 1, :] = top
-        log_ref[h : h + 1, :] = jnp.log(share_sum)
-        share = share / share_sum
-        mixed = jnp.zeros((VDIM, 128), F32)
-        for g in range(groups):
-            part = parts_ref[g, h * VDIM : (h + 1) * VDIM, :].astype(F32)
-            mixed = mixed + part * share[g : g + 1, :]
-        heads.append(mixed)
-    mixed = jnp.concatenate(heads, axis=0).T.astype(BF16)
-    for first in range(0, out_ref.shape[1], 512):
-        at = slice(first, first + 512)
-        out_ref[:, at] = (
-            conv_ref[:, at]
-            + jnp.dot(mixed, weight_ref[:, at], preferred_element_type=F32)
-        ).astype(BF16)
+def merge_kernel(parts_ref, conv_ref, weight_ref, out_ref, top_ref, log_ref, mixed_ref):
+    @pl.when(pl.program_id(0) == 0)
+    def mix():
+        groups = parts_ref.shape[0]
+        tails = parts_ref[:, 128:PART_ROWS, :].astype(F32)
+        heads = []
+        for h in range(2):
+            logs = tails[:, 8 * h, :] + (tails[:, 8 * h + 1, :] + tails[:, 8 * h + 2, :])
+            top = jnp.max(logs, axis=0, keepdims=True)
+            share = jnp.exp(logs - top)
+            share_sum = jnp.sum(share, axis=0, keepdims=True)
+            top_ref[h : h + 1, :] = top
+            log_ref[h : h + 1, :] = jnp.log(share_sum)
+            share = share / share_sum
+            mixed = jnp.zeros((VDIM, 128), F32)
+            for g in range(groups):
+                part = parts_ref[g, h * VDIM : (h + 1) * VDIM, :].astype(F32)
+                mixed = mixed + part * share[g : g + 1, :]
+            heads.append(mixed)
+        mixed_ref[...] = jnp.concatenate(heads, axis=0).T.astype(BF16)
+
+    added = jnp.dot(mixed_ref[...], weight_ref[...], preferred_element_type=F32)
+    out_ref[...] = (conv_ref[...] + added).astype(BF16)
 
 
 def merge(parts, conv_projected, heads_output):
     rows, width = conv_projected.shape
+    step = width // 4
+    columns = pl.BlockSpec((rows, step), lambda i: (0, i))
+    small = pl.BlockSpec((2, rows), lambda i: (0, 0))
     return pl.pallas_call(
         merge_kernel,
         out_shape=(
@@ -328,6 +335,14 @@
             jax.ShapeDtypeStruct((2, rows), F32),
             jax.ShapeDtypeStruct((2, rows), F32),
         ),
+        grid=(width // step,),
+        in_specs=[
+            pl.BlockSpec(parts.shape, lambda i: (0, 0, 0)),
+            columns,
+            pl.BlockSpec((heads_output.shape[0], step), lambda i: (0, i)),
+        ],
+        out_specs=(columns, small, small),
+        scratch_shapes=[pltpu.VMEM((rows, heads_output.shape[0]), BF16)],
         cost_estimate=pl.CostEstimate(
             flops=2 * rows * width * 128, bytes_accessed=2_000_000, transcendentals=rows * 32
         ),
@@ -386,16 +401,11 @@
     turned = rotate_rows(turned, cosine, sine).astype(BF16).reshape(-1, rows)
     queries = jnp.concatenate([query_nope, turned], axis=0)
     queries_other = lax.ppermute(queries, "pair", [(0, 1), (1, 0)])
-    first_of_pair = lax.axis_index("pair") == 0
-    both = [
-        jnp.where(first_of_pair, queries, queries_other),
-        jnp.where(first_of_pair, queries_other, queries),
-    ]
     _, wide, cores = (lax.axis_size(name) for name in GROUP)
     halves = gates.reshape(cores, -1, 128)
-    both = jnp.broadcast_to(jnp.concatenate(both, axis=0), (wide, cores, 2 * QUERY_ROWS, 128))
     halves = jnp.broadcast_to(halves, (wide, *halves.shape))
-    sent = jnp.concatenate([halves, both], axis=2)
+    both = [jnp.broadcast_to(q, (wide, cores, *q.shape)) for q in (queries, queries_other)]
+    sent = jnp.concatenate([halves, *both], axis=2)
     joint = exchange(sent.reshape(-1, *sent.shape[2:]), GROUP[1:])
     joint_other = lax.ppermute(joint, "core", [(0, 1), (1, 0)])
     held = jnp.concatenate(

time: 158 us -> 159 us (level)
  no operation moved by 1% of the time
where the time goes in v8:
time: 159 us; the launch traced here: 157 us
  starting transfers between devices  45.6 us (29%)
  waiting for transfers between devices  42.7 us (27%)
  blocking collectives  41.4 us (26%)
  Pallas kernels  20.8 us (13%)
  other arithmetic  4.52 us (3%)
    all_to_all x4, waiting for transfers between devices, exchange(): return lax.all_to_all(array, axis, split_axis=0, concat_axis=0, tiled=True)  37 us
    all_to_all x4, starting transfers between devices, exchange(): return lax.all_to_all(array, axis, split_axis=0, concat_axis=0, tiled=True)  35.8 us
    all_gather x1, blocking collectives, layer(): lax.all_gather(held, 'far', axis=0, tiled=True).reshape(-1, *held.shape)  29.6 us
    all_gather x1, blocking collectives, layer(): latents = lax.all_gather(latents, 'tp', axis=0)  11.8 us
    pallas_call x1, Pallas kernels, attend(): pl.pallas_call(attention_kernel, out_shape=pltpu.HBM((groups, PART_ROWS,...  7.83 us
    pallas_call x1, Pallas kernels, convolve(): pl.pallas_call(conv_kernel, out_shape=pltpu.HBM((count, out_width), F32),...  4.49 us
    pallas_call x1, Pallas kernels, merge(): pl.pallas_call(merge_kernel, out_shape=(jax.ShapeDtypeStruct((rows, width...  4 us
    ppermute x1, waiting for transfers between devices, shifted(): lax.ppermute(value, axis, [(source, source + steps) for source in range(f...  3.83 us
  transfers between devices with their start and end apart: 7, of which 4 were waited for; matrix products, arithmetic and copies ran while one was open for 2% of the time, Pallas kernels for 10%

profile of v8, /device:TPU:1, one launch (start us, length us, event | category | flops | bytes accessed | tf_op | source)
XLA Modules:
  0.0 157.4 jit_solution(15541679800800389176)
XLA Ops:
  0.6 1.6 spread_gates.1
  2.2 15.9 %all-to-all-start = ((bf16[16,96,128]{2,1,0:T(8,128)(2,1)}), bf16[16,96,128]{2,1,0:T(8,128)(2,1)S(1)}, u32[]{:S(2)}, u32[]{:S(2)}) async-start(bf16[16,96,128]{2,1,0:T(8,128)(2,1)} %spread_gates.1), calls=%async_computation | async-start | bytes 786432 | tf_op jit(solution)/shard_map/all_to_all | solution.py:30
  18.1 2.9 %entry.1 = (bf16[128,2048]{1,0:T(8,128)(2,1)}, bf16[16,2048]{1,0:T(8,128)(2,1)}, bf16[128,320]{1,0:T(8,128)(2,1)}, f32[32,128]{1,0:T(8,128)}) custom-call(bf16[128,2048]{1,0:T(8,128)(2,1)} %tokens.1, f32[1,2048]{1,0:T(1,128)} %bitcast.51, bf16[2048,128]{1,0:T(8,128)(2,1)} %latent_down.1, bf16[192,2048]{1,0:T(8,128)(2,1)} %bitcast.47, bf16[32,2048]{1,0:T(8,128)(2,1)} %bitcast.49), custom_call_target="tpu_custom_call" | custom-call | flops 201326592 | bytes 2500000 | tf_op jit(solution)/shard_map/entry/pallas_call | solution.py:211
  21.0 11.8 %all-gather = bf16[512,320]{1,0:T(8,128)(2,1)S(1)} all-gather(bf16[128,320]{1,0:T(8,128)(2,1)} %get-tuple-element.9), channel_id=2, replica_groups=mesh['far'=8,'pair'=2,'x'=4,'core'=2,'tp'=4] {'tp'}, dimensions={0}, use_global_device_ids=true | all-gather | bytes 409600 | tf_op jit(solution)/shard_map/all_gather | solution.py:386
  32.8 0.2 copy.23
  33.1 0.8 multiply_cosine_fusion
  34.0 0.2 fusion.4
  34.2 0.2 fusion.7
  34.4 0.3 fusion.2
  34.7 3.4 %collective-permute-start = (bf16[192,128]{1,0:T(8,128)(2,1)S(1)}, bf16[192,128]{1,0:T(8,128)(2,1)S(1)}, u32[]{:S(2)}, u32[]{:S(2)}) collective-permute-start(bf16[192,128]{1,0:T(8,128)(2,1)S(1)} %pad_maximum_fusion.2), channel_id=1, source_target_pairs={{0,32},{32,0},{1,33},{33,1},{2,34},{34,2},{3,35},{35,3},{4,36},{36... | collective-permute-start | bytes 147464 | tf_op jit(solution)/shard_map/ppermute | solution.py:403
  38.1 1.9 %collective-permute-done = bf16[192,128]{1,0:T(8,128)(2,1)S(1)} collective-permute-done((bf16[192,128]{1,0:T(8,128)(2,1)S(1)}, bf16[192,128]{1,0:T(8,128)(2,1)S(1)}, u32[]{:S(2)}, u32[]{:S(2)}) %collective-permute-start) | collective-permute-done | bytes 49184 | tf_op jit(solution)/shard_map/ppermute | solution.py:403
  40.1 0.2 broadcast_in_dim.6
  40.3 1.6 %pad_maximum_fusion = bf16[4,2,1152,128]{3,2,1,0:T(8,128)(2,1)} fusion(bf16[4,2,192,128]{3,2,1,0:T(8,128)(2,1)S(1)} %broadcast_in_dim.8, bf16[4,2,192,128]{3,2,1,0:T(8,128)(2,1)S(1)} %broadcast_in_dim.7, bf16[4,2,768,128]{3,2,1,0:T(8,128)(2,1)S(1)} %broadcast_in_dim.6), kind=kLoop, calls=%fused_computation | loop fusion | flops 7077888 | bytes 4718592 | tf_op jit(solution)/shard_map/concatenate | solution.py:408
  41.9 7.6 %all-to-all-start.1 = ((bf16[8,1152,128]{2,1,0:T(8,128)(2,1)}), bf16[8,1152,128]{2,1,0:T(8,128)(2,1)S(1)}, u32[]{:S(2)}, u32[]{:S(2)}) async-start(bf16[8,1152,128]{2,1,0:T(8,128)(2,1)} %bitcast.43), calls=%async_computation.1 | async-start | bytes 4718592 | tf_op jit(solution)/shard_map/all_to_all | solution.py:30
  49.5 0.1 copy.22
  49.7 0.1 fusion.6
  49.9 0.2 fusion
  50.1 0.2 fusion.1
  50.4 28.1 %all-to-all-done.1.query_ref.mine_ref = bf16[8,1152,128]{2,1,0:T(8,128)(2,1)S(1)} async-done(((bf16[8,1152,128]{2,1,0:T(8,128)(2,1)}), bf16[8,1152,128]{2,1,0:T(8,128)(2,1)S(1)}, u32[]{:S(2)}, u32[]{:S(2)}) %all-to-all-start.1) | async-done | bytes 2359328 | tf_op jit(solution)/shard_map/all_to_all | solution.py:30
  78.5 2.9 %collective-permute-start.1 = (bf16[8,1152,128]{2,1,0:T(8,128)(2,1)S(1)}, bf16[8,1152,128]{2,1,0:T(8,128)(2,1)}, u32[]{:S(2)}, u32[]{:S(2)}) collective-permute-start(bf16[8,1152,128]{2,1,0:T(8,128)(2,1)S(1)} %all-to-all-done.1.query_ref.mine_ref), channel_id=1, source_target_pairs={{0,4},{4,0},{1,5},{5,1},{2,6},{6,2},{3,7},{7,3},{8,12},{12,8},{9,1... | collective-permute-start | bytes 7077896 | tf_op jit(solution)/shard_map/ppermute | solution.py:410
  81.3 29.6 %all_gather.11 = bf16[2304,128]{1,0:T(8,128)(2,1)S(1)} all-gather(bf16[288,128]{1,0:T(8,128)(2,1)S(1)} %pad_maximum_fusion.1), channel_id=1, replica_groups=mesh['far'=8,'pair'=2,'x'=4,'core'=2,'tp'=4] {'far'}, dimensions={0}, use_global_device_ids=true | all-gather | bytes 663552 | tf_op jit(solution)/shard_map/all_gather | solution.py:419
  110.9 7.8 %attend.1 = bf16[16,144,128]{2,1,0:T(8,128)(2,1)} custom-call(bf16[8,288,128]{2,1,0:T(8,128)(2,1)S(1)} %bitcast.42, bf16[8,1152,128]{2,1,0:T(8,128)(2,1)S(1)} %all-to-all-done.1.query_ref.mine_ref), custom_call_target="tpu_custom_call" | custom-call | flops 1879048192 | bytes 2000000 | tf_op jit(solution)/shard_map/attend/pallas_call | solution.py:143
  118.8 8.5 %all-to-all-start.2 = ((bf16[16,144,128]{2,1,0:T(8,128)(2,1)}), bf16[16,144,128]{2,1,0:T(8,128)(2,1)S(1)}, u32[]{:S(2)}, u32[]{:S(2)}) async-start(bf16[16,144,128]{2,1,0:T(8,128)(2,1)} %attend.1), calls=%async_computation.2 | async-start | bytes 1179648 | tf_op jit(solution)/shard_map/all_to_all | solution.py:30
  127.3 3.5 %collective-permute-start.2 = (bf16[16,2048]{1,0:T(8,128)(2,1)S(1)}, bf16[16,2048]{1,0:T(8,128)(2,1)S(1)}, u32[]{:S(2)}, u32[]{:S(2)}) collective-permute-start(bf16[16,2048]{1,0:T(8,128)(2,1)S(1)} %copy-done.8), channel_id=1, source_target_pairs={{0,4},{4,8},{8,12},{12,16},{16,20},{20,24},{24,28},{28,32},{32,36}... | collective-permute-start | bytes 196616 | tf_op jit(solution)/shard_map/ppermute | solution.py:36
  130.9 3.8 %collective-permute-done.2.edge_ref = bf16[16,2048]{1,0:T(8,128)(2,1)S(1)} collective-permute-done((bf16[16,2048]{1,0:T(8,128)(2,1)S(1)}, bf16[16,2048]{1,0:T(8,128)(2,1)S(1)}, u32[]{:S(2)}, u32[]{:S(2)}) %collective-permute-start.2) | collective-permute-done | bytes 65568 | tf_op jit(solution)/shard_map/ppermute | solution.py:36
  134.7 4.5 %convolve.1.conv_ref = f32[128,2048]{1,0:T(8,128)} custom-call(bf16[8,1152,128]{2,1,0:T(8,128)(2,1)S(1)} %all-to-all-done.1.query_ref.mine_ref, bf16[8,1152,128]{2,1,0:T(8,128)(2,1)} %collective-permute-done.1.other_ref, bf16[128,2048]{1,0:T(8,128)(2,1)} %get-tuple-element.11.normed_ref, bf16[16,2048]{1,0:T(8,128)(2,1)S(1)} %collective-permute-done.2.edge_ref, ...), custom_call_target="tpu_custom_call" | custom-call | flops 536870912 | bytes 6000000 | tf_op jit(solution)/shard_map/convolve/pallas_call | solution.py:273
  139.2 4.0 %merge.1 = (bf16[128,2048]{1,0:T(8,128)(2,1)}, f32[2,128]{1,0:T(2,128)S(1)}, f32[2,128]{1,0:T(2,128)S(1)}) custom-call(bf16[16,144,128]{2,1,0:T(8,128)(2,1)S(1)} %all-to-all-done.2.parts_ref, f32[128,2048]{1,0:T(8,128)} %convolve.1.conv_ref, bf16[128,2048]{1,0:T(8,128)(2,1)} %weight_ref.1), custom_call_target="tpu_custom_call" | custom-call | flops 67108864 | bytes 2000000 | tf_op jit(solution)/shard_map/merge/pallas_call | solution.py:331
  143.2 3.8 %all-to-all-start.3 = ((bf16[4,32,2048]{2,1,0:T(8,128)(2,1)}), bf16[4,32,2048]{2,1,0:T(8,128)(2,1)S(1)}, u32[]{:S(2)}, u32[]{:S(2)}) async-start(bf16[4,32,2048]{2,1,0:T(8,128)(2,1)} %bitcast.18), calls=%async_computation.3 | async-start | bytes 1048576 | tf_op jit(solution)/shard_map/all_to_all | solution.py:30
  147.0 0.6 add.66
  147.6 8.9 %all-to-all-done.3 = bf16[4,32,2048]{2,1,0:T(8,128)(2,1)S(1)} async-done(((bf16[4,32,2048]{2,1,0:T(8,128)(2,1)}), bf16[4,32,2048]{2,1,0:T(8,128)(2,1)S(1)}, u32[]{:S(2)}, u32[]{:S(2)}) %all-to-all-start.3) | async-done | bytes 524320 | tf_op jit(solution)/shard_map/all_to_all | solution.py:30
  156.5 0.1 multiply_reduce_fusion.1
  156.7 0.8 multiply_convert_fusion
  (37 shorter events, 0.5 us)
Async XLA Ops:
  0.6 33.7 %copy-start = (bf16[768,128]{1,0:T(8,128)(2,1)S(1)}, bf16[768,128]{1,0:T(8,128)(2,1)}, u32[]{:S(2)}) copy-start(bf16[768,128]{1,0:T(8,128)(2,1)} %param.29) | copy-start | bytes 589828
  2.2 31.8 %copy-start.6 = (f32[768]{0:T(1024)S(1)}, f32[768]{0:T(1024)}, u32[]{:S(2)}) copy-start(f32[768]{0:T(1024)} %param.27) | copy-start | bytes 9220
  2.2 31.9 %copy-start.4 = (bf16[768,64]{0,1:T(8,128)(2,1)S(1)}, bf16[768,64]{0,1:T(8,128)(2,1)}, u32[]{:S(2)}) copy-start(bf16[768,64]{0,1:T(8,128)(2,1)} %param.30) | copy-start | bytes 294916
  2.2 37.8 %all-to-all-start = ((bf16[16,96,128]{2,1,0:T(8,128)(2,1)}), bf16[16,96,128]{2,1,0:T(8,128)(2,1)S(1)}, u32[]{:S(2)}, u32[]{:S(2)}) async-start(bf16[16,96,128]{2,1,0:T(8,128)(2,1)} %spread_gates.1), calls=%async_computation | async-start | bytes 786432 | tf_op jit(solution)/shard_map/all_to_all | solution.py:30
  34.7 5.3 %collective-permute-start = (bf16[192,128]{1,0:T(8,128)(2,1)S(1)}, bf16[192,128]{1,0:T(8,128)(2,1)S(1)}, u32[]{:S(2)}, u32[]{:S(2)}) collective-permute-start(bf16[192,128]{1,0:T(8,128)(2,1)S(1)} %pad_maximum_fusion.2), channel_id=1, source_target_pairs={{0,32},{32,0},{1,33},{33,1},{2,34},{34,2},{3,35},{35,3},{4,36},{36... | collective-permute-start | bytes 147464 | tf_op jit(solution)/shard_map/ppermute | solution.py:403
  41.9 7.8 %copy-start.7 = (f32[512]{0:T(512)S(1)}, f32[512]{0:T(512)}, u32[]{:S(2)}) copy-start(f32[512]{0:T(512)} %param.28) | copy-start | bytes 6148
  41.9 8.0 %copy-start.2 = (bf16[512,128]{1,0:T(8,128)(2,1)S(1)}, bf16[512,128]{1,0:T(8,128)(2,1)}, u32[]{:S(2)}) copy-start(bf16[512,128]{1,0:T(8,128)(2,1)} %param.31) | copy-start | bytes 393220
  41.9 8.2 %copy-start.3 = (bf16[512,128]{1,0:T(8,128)(2,1)S(1)}, bf16[512,128]{1,0:T(8,128)(2,1)}, u32[]{:S(2)}) copy-start(bf16[512,128]{1,0:T(8,128)(2,1)} %param.32) | copy-start | bytes 393220
  41.9 36.6 %all-to-all-start.1 = ((bf16[8,1152,128]{2,1,0:T(8,128)(2,1)}), bf16[8,1152,128]{2,1,0:T(8,128)(2,1)S(1)}, u32[]{:S(2)}, u32[]{:S(2)}) async-start(bf16[8,1152,128]{2,1,0:T(8,128)(2,1)} %bitcast.43), calls=%async_computation.1 | async-start | bytes 4718592 | tf_op jit(solution)/shard_map/all_to_all | solution.py:30
  78.5 56.3 %collective-permute-start.1 = (bf16[8,1152,128]{2,1,0:T(8,128)(2,1)S(1)}, bf16[8,1152,128]{2,1,0:T(8,128)(2,1)}, u32[]{:S(2)}, u32[]{:S(2)}) collective-permute-start(bf16[8,1152,128]{2,1,0:T(8,128)(2,1)S(1)} %all-to-all-done.1.query_ref.mine_ref), channel_id=1, source_target_pairs={{0,4},{4,0},{1,5},{5,1},{2,6},{6,2},{3,7},{7,3},{8,12},{12,8},{9,1... | collective-permute-start | bytes 7077896 | tf_op jit(solution)/shard_map/ppermute | solution.py:410
  110.9 16.4 %copy-start.8 = (bf16[16,2048]{1,0:T(8,128)(2,1)S(1)}, bf16[16,2048]{1,0:T(8,128)(2,1)}, u32[]{:S(2)}) copy-start(bf16[16,2048]{1,0:T(8,128)(2,1)} %get-tuple-element.12) | copy-start | bytes 196612
  110.9 23.8 %copy-start.1 = (f32[3,256]{1,0:T(4,128)S(1)}, f32[3,256]{1,0:T(4,128)}, u32[]{:S(2)}) copy-start(f32[3,256]{1,0:T(4,128)} %taps_ref.1) | copy-start | bytes 9220
  118.8 20.4 %all-to-all-start.2 = ((bf16[16,144,128]{2,1,0:T(8,128)(2,1)}), bf16[16,144,128]{2,1,0:T(8,128)(2,1)S(1)}, u32[]{:S(2)}, u32[]{:S(2)}) async-start(bf16[16,144,128]{2,1,0:T(8,128)(2,1)} %attend.1), calls=%async_computation.2 | async-start | bytes 1179648 | tf_op jit(solution)/shard_map/all_to_all | solution.py:30
  127.3 7.4 %collective-permute-start.2 = (bf16[16,2048]{1,0:T(8,128)(2,1)S(1)}, bf16[16,2048]{1,0:T(8,128)(2,1)S(1)}, u32[]{:S(2)}, u32[]{:S(2)}) collective-permute-start(bf16[16,2048]{1,0:T(8,128)(2,1)S(1)} %copy-done.8), channel_id=1, source_target_pairs={{0,4},{4,8},{8,12},{12,16},{16,20},{20,24},{24,28},{28,32},{32,36}... | collective-permute-start | bytes 196616 | tf_op jit(solution)/shard_map/ppermute | solution.py:36
  139.2 17.5 %copy-start.5 = (f32[2048]{0:T(1024)S(1)}, f32[2048]{0:T(1024)}, u32[]{:S(2)}) copy-start(f32[2048]{0:T(1024)} %param.35) | copy-start | bytes 24580
  143.2 13.3 %all-to-all-start.3 = ((bf16[4,32,2048]{2,1,0:T(8,128)(2,1)}), bf16[4,32,2048]{2,1,0:T(8,128)(2,1)S(1)}, u32[]{:S(2)}, u32[]{:S(2)}) async-start(bf16[4,32,2048]{2,1,0:T(8,128)(2,1)} %bitcast.18), calls=%async_computation.3 | async-start | bytes 1048576 | tf_op jit(solution)/shard_map/all_to_all | solution.py:30

commit v9 on v7

--- a/solution.py
+++ b/solution.py
@@ -68,6 +68,7 @@
     near = query_ref.shape[0]
     groups = 2 * near
     queries = groups * 128
+    pair = lax.axis_index("pair")
     for b in range(blocks):
         key_rows[b * 128 : (b + 1) * 128, :] = held_ref[b, 0:160, :].T
         value_cols[:, b * 128 : (b + 1) * 128] = held_ref[b, 160:288, :]
@@ -92,7 +93,9 @@
         )
 
     def soften(first, scores):
-        col = lax.broadcasted_iota(jnp.int32, (1, COLS), 1) + first % queries
+        side = pair if first % queries < near * 128 else 1 - pair
+        col = lax.broadcasted_iota(jnp.int32, (1, COLS), 1) + first % (near * 128)
+        col = col + side * (near * 128)
         scores = jnp.where(key_at <= col, scores, LOW)
         best = jnp.maximum(jnp.max(scores, axis=0, keepdims=True), FLOOR)
         weights = jnp.exp2(scores * factor - best * factor)
@@ -113,13 +116,15 @@
         tail = jnp.concatenate([high, middle, low, jnp.zeros((5, COLS), F32)], axis=0)
         for i in range(COLS // 128):
             g = first % queries // 128 + i
+            side = pair if g < near else 1 - pair
+            to = side * near + g % near
             at = slice(i * 128, (i + 1) * 128)
-            out_ref[g, h * 64 : (h + 1) * 64, :] = mixed[:, at]
+            out_ref[to, h * 64 : (h + 1) * 64, :] = mixed[:, at]
             if h == 0:
                 logs[g] = tail[:, at]
             else:
                 both = jnp.concatenate([logs.pop(g), tail[:, at]], axis=0)
-                out_ref[g, 128:PART_ROWS, :] = both.astype(BF16)
+                out_ref[to, 128:PART_ROWS, :] = both.astype(BF16)
 
     tiles = 2 * queries // COLS
     scores, softened = {}, {}
@@ -219,10 +224,11 @@
 
 
 LEAD = 16
+MERGE_STEPS = 1
 
 
 def conv_kernel(
-    mine_ref, other_ref, normed_ref, edge_ref, taps_ref, output_ref, out_ref,
+    mine_ref, other_ref, normed_ref, edge_ref, taps_ref, out_ref,
     rows_ref, weight_ref, product_ref,
 ):
     core = lax.axis_index("core")
@@ -253,48 +259,50 @@
     for k in range(TAPS):
         first = LEAD - (TAPS - 1) + k
         convolved = convolved + product_ref[first : first + count, :] * taps_ref[k : k + 1, :]
-    mixed = (spread[LEAD:, :third] * convolved).astype(BF16)
-    for first in range(0, out_ref.shape[1], 512):
-        at = slice(first, first + 512)
-        out_ref[:, at] = jnp.dot(mixed, output_ref[:, at], preferred_element_type=F32)
-
-
-def convolve(joint, joint_other, normed, edge, taps, output):
+    out_ref[...] = (spread[LEAD:, :third] * convolved).astype(BF16)
+
+
+def convolve(joint, joint_other, normed, edge, taps):
     count, width = normed.shape
-    third, out_width = output.shape
+    third = taps.shape[1]
     near = joint.shape[0]
     weights = pl.BlockSpec((near, joint.shape[1] - 2 * QUERY_ROWS, 128), lambda i: (0, 0, 0))
-    whole = [pl.BlockSpec(a.shape, lambda i: (0, 0)) for a in (normed, edge, taps, output)]
+    whole = [pl.BlockSpec(a.shape, lambda i: (0, 0)) for a in (normed, edge, taps)]
     return pl.pallas_call(
         conv_kernel,
-        out_shape=pltpu.HBM((count, out_width), F32),
+        out_shape=jax.ShapeDtypeStruct((count, third), BF16),
         grid=(1,),
         in_specs=[weights, weights, *whole],
-        out_specs=pl.BlockSpec((count, out_width), lambda i: (0, 0)),
+        out_specs=pl.BlockSpec((count, third), lambda i: (0, 0)),
         scratch_shapes=[
             pltpu.VMEM((LEAD + count, width), BF16),
             pltpu.VMEM((width, 3 * third), BF16),
             pltpu.VMEM((LEAD + count, third), F32),
         ],
         cost_estimate=pl.CostEstimate(
-            flops=2 * count * (width * 3 * third + third * out_width),
-            bytes_accessed=6_000_000,
-            transcendentals=0,
+            flops=2 * count * width * 3 * third, bytes_accessed=4_000_000, transcendentals=0
         ),
         compiler_params=pltpu.CompilerParams(vmem_limit_bytes=30 << 20),
         name="convolve",
-    )(
-        joint,
-        joint_other,
-        pltpu.with_memory_space_constraint(normed, pltpu.HBM),
-        edge,
-        taps,
-        pltpu.with_memory_space_constraint(output, pltpu.HBM),
-    )
-
-
-def merge_kernel(parts_ref, conv_ref, weight_ref, out_ref, top_ref, log_ref):
+    )(joint, joint_other, pltpu.with_memory_space_constraint(normed, pltpu.HBM), edge, taps)
+
+
+def merge_kernel(
+    parts_ref, conv_ref, output_hbm, weight_hbm, out_ref, top_ref, log_ref,
+    output_ref, weight_ref, output_sems, weight_sems,
+):
     groups = parts_ref.shape[0]
+    copies = []
+    for i in range(MERGE_STEPS):
+        width = out_ref.shape[1] // MERGE_STEPS
+        at = slice(i * width, (i + 1) * width)
+        pair = (
+            pltpu.make_async_copy(output_hbm.at[:, at], output_ref.at[:, at], output_sems.at[i]),
+            pltpu.make_async_copy(weight_hbm.at[:, at], weight_ref.at[:, at], weight_sems.at[i]),
+        )
+        for copy in pair:
+            copy.start()
+        copies.append((at, pair))
     tails = parts_ref[:, 128:PART_ROWS, :].astype(F32)
     heads = []
     for h in range(2):
@@ -311,16 +319,16 @@
             mixed = mixed + part * share[g : g + 1, :]
         heads.append(mixed)
     mixed = jnp.concatenate(heads, axis=0).T.astype(BF16)
-    for first in range(0, out_ref.shape[1], 512):
-        at = slice(first, first + 512)
-        out_ref[:, at] = (
-            conv_ref[:, at]
-            + jnp.dot(mixed, weight_ref[:, at], preferred_element_type=F32)
-        ).astype(BF16)
-
-
-def merge(parts, conv_projected, heads_output):
-    rows, width = conv_projected.shape
+    for at, pair in copies:
+        for copy in pair:
+            copy.wait()
+        added = jnp.dot(conv_ref[...], output_ref[:, at], preferred_element_type=F32)
+        added += jnp.dot(mixed, weight_ref[:, at], preferred_element_type=F32)
+        out_ref[:, at] = added.astype(BF16)
+
+
+def merge(parts, conv_mixed, conv_output, heads_output):
+    rows, width = conv_mixed.shape[0], heads_output.shape[1]
     return pl.pallas_call(
         merge_kernel,
         out_shape=(
@@ -328,14 +336,27 @@
             jax.ShapeDtypeStruct((2, rows), F32),
             jax.ShapeDtypeStruct((2, rows), F32),
         ),
+        in_specs=[
+            pl.BlockSpec(memory_space=pltpu.VMEM),
+            pl.BlockSpec(memory_space=pltpu.VMEM),
+            pl.BlockSpec(memory_space=pltpu.HBM),
+            pl.BlockSpec(memory_space=pltpu.HBM),
+        ],
+        scratch_shapes=[
+            pltpu.VMEM(conv_output.shape, BF16),
+            pltpu.VMEM(heads_output.shape, BF16),
+            pltpu.SemaphoreType.DMA((MERGE_STEPS,)),
+            pltpu.SemaphoreType.DMA((MERGE_STEPS,)),
+        ],
         cost_estimate=pl.CostEstimate(
-            flops=2 * rows * width * 128, bytes_accessed=2_000_000, transcendentals=rows * 32
+            flops=2 * rows * width * 384, bytes_accessed=2_500_000, transcendentals=rows * 32
         ),
         compiler_params=pltpu.CompilerParams(vmem_limit_bytes=16 << 20),
         name="merge",
     )(
         parts,
-        pltpu.with_memory_space_constraint(conv_projected, pltpu.HBM),
+        conv_mixed,
+        pltpu.with_memory_space_constraint(conv_output, pltpu.HBM),
         pltpu.with_memory_space_constraint(heads_output, pltpu.HBM),
     )
 
@@ -386,16 +407,11 @@
     turned = rotate_rows(turned, cosine, sine).astype(BF16).reshape(-1, rows)
     queries = jnp.concatenate([query_nope, turned], axis=0)
     queries_other = lax.ppermute(queries, "pair", [(0, 1), (1, 0)])
-    first_of_pair = lax.axis_index("pair") == 0
-    both = [
-        jnp.where(first_of_pair, queries, queries_other),
-        jnp.where(first_of_pair, queries_other, queries),
-    ]
     _, wide, cores = (lax.axis_size(name) for name in GROUP)
     halves = gates.reshape(cores, -1, 128)
-    both = jnp.broadcast_to(jnp.concatenate(both, axis=0), (wide, cores, 2 * QUERY_ROWS, 128))
     halves = jnp.broadcast_to(halves, (wide, *halves.shape))
-    sent = jnp.concatenate([halves, both], axis=2)
+    both = [jnp.broadcast_to(q, (wide, cores, *q.shape)) for q in (queries, queries_other)]
+    sent = jnp.concatenate([halves, *both], axis=2)
     joint = exchange(sent.reshape(-1, *sent.shape[2:]), GROUP[1:])
     joint_other = lax.ppermute(joint, "core", [(0, 1), (1, 0)])
     held = jnp.concatenate(
@@ -411,15 +427,9 @@
     parts = attend(held, joint)
     parts = exchange(parts, GROUP)
 
-    conv_projected = convolve(
-        joint,
-        joint_other,
-        normed,
-        edge,
-        conv_taps,
-        conv_output,
-    )
-    projected, top, log_total = merge(parts, conv_projected, heads_output)
+    conv_mixed = convolve(joint, joint_other, normed, edge, conv_taps)
+
+    projected, top, log_total = merge(parts, conv_mixed, conv_output, heads_output)
     tp = lax.axis_size("tp")
     arrived = exchange(projected.reshape(tp, rows // tp, -1), "tp")
     row_logsum = top + log_total

time: 158 us -> 156 us (0.987)
  the two profiles are of different devices: /device:TPU:1 before, /device:TPU:32 now
where the time goes in v9:
time: 156 us
  waiting for transfers between devices  49.4 us (32%)
  blocking collectives  46.4 us (30%)
  starting transfers between devices  34.9 us (22%)
  Pallas kernels  17.8 us (11%)
  other arithmetic  4.52 us (3%)
    all_to_all x4, waiting for transfers between devices, exchange(): return lax.all_to_all(array, axis, split_axis=0, concat_axis=0, tiled=True)  36.6 us
    all_gather x1, blocking collectives, layer(): lax.all_gather(held, 'far', axis=0, tiled=True).reshape(-1, *held.shape)  33.2 us
    all_to_all x4, starting transfers between devices, exchange(): return lax.all_to_all(array, axis, split_axis=0, concat_axis=0, tiled=True)  29 us
    all_gather x1, blocking collectives, layer(): latents = lax.all_gather(latents, 'tp', axis=0)  13.2 us
    ppermute x1, waiting for transfers between devices, shifted(): lax.ppermute(value, axis, [(source, source + steps) for source in range(f...  8.81 us
    pallas_call x1, Pallas kernels, attend(): pl.pallas_call(attention_kernel, out_shape=pltpu.HBM((groups, PART_ROWS,...  7.85 us
    ppermute x1, waiting for transfers between devices, layer(): queries_other = lax.ppermute(queries, 'pair', [(0, 1), (1, 0)])  3.96 us
  transfers between devices with their start and end apart: 7, of which 4 were waited for; matrix products, arithmetic and copies ran while one was open for 2% of the time, Pallas kernels for 9%

profile of v9, /device:TPU:32, one launch (start us, length us, event | category | flops | bytes accessed | tf_op | source)
XLA Modules:
  0.0 155.5 jit_solution(4645258646654156702)
XLA Ops:
  0.6 1.6 %spread_gates.1 = bf16[16,96,128]{2,1,0:T(8,128)(2,1)} custom-call(bf16[16,256]{1,0:T(8,128)(2,1)} %outer_ref.1, bf16[16,256]{1,0:T(8,128)(2,1)} %inner_ref.1, bf16[16,256]{1,0:T(8,128)(2,1)} %signal_ref.1), custom_call_target="tpu_custom_call" | custom-call | flops 1000000 | bytes 400000 | tf_op jit(solution)/shard_map/spread_gates/pallas_call | solution.py:184
  2.2 15.3 %all-to-all-start = ((bf16[16,96,128]{2,1,0:T(8,128)(2,1)}), bf16[16,96,128]{2,1,0:T(8,128)(2,1)S(1)}, u32[]{:S(2)}, u32[]{:S(2)}) async-start(bf16[16,96,128]{2,1,0:T(8,128)(2,1)} %spread_gates.1), calls=%async_computation | async-start | bytes 786432 | tf_op jit(solution)/shard_map/all_to_all | solution.py:30
  17.6 2.9 %entry.1 = (bf16[128,2048]{1,0:T(8,128)(2,1)}, bf16[16,2048]{1,0:T(8,128)(2,1)}, bf16[128,320]{1,0:T(8,128)(2,1)}, f32[32,128]{1,0:T(8,128)}) custom-call(bf16[128,2048]{1,0:T(8,128)(2,1)} %tokens.1, f32[1,2048]{1,0:T(1,128)} %bitcast.51, bf16[2048,128]{1,0:T(8,128)(2,1)} %latent_down.1, bf16[192,2048]{1,0:T(8,128)(2,1)} %bitcast.47, bf16[32,2048]{1,0:T(8,128)(2,1)} %bitcast.49), custom_call_target="tpu_custom_call" | custom-call | flops 201326592 | bytes 2500000 | tf_op jit(solution)/shard_map/entry/pallas_call | solution.py:211
  20.5 13.2 %all-gather = bf16[512,320]{1,0:T(8,128)(2,1)S(1)} all-gather(bf16[128,320]{1,0:T(8,128)(2,1)} %get-tuple-element.9), channel_id=2, replica_groups=mesh['far'=8,'pair'=2,'x'=4,'core'=2,'tp'=4] {'tp'}, dimensions={0}, use_global_device_ids=true | all-gather | bytes 409600 | tf_op jit(solution)/shard_map/all_gather | solution.py:392
  33.8 0.2 copy.23
  34.1 0.8 multiply_cosine_fusion
  34.9 0.2 fusion.4
  35.1 0.2 fusion.7
  35.3 0.3 fusion.2
  35.6 2.0 %collective-permute-start = (bf16[192,128]{1,0:T(8,128)(2,1)S(1)}, bf16[192,128]{1,0:T(8,128)(2,1)S(1)}, u32[]{:S(2)}, u32[]{:S(2)}) collective-permute-start(bf16[192,128]{1,0:T(8,128)(2,1)S(1)} %pad_maximum_fusion.2), channel_id=1, source_target_pairs={{0,32},{32,0},{1,33},{33,1},{2,34},{34,2},{3,35},{35,3},{4,36},{36... | collective-permute-start | bytes 147464 | tf_op jit(solution)/shard_map/ppermute | solution.py:409
  37.6 4.0 %collective-permute-done = bf16[192,128]{1,0:T(8,128)(2,1)S(1)} collective-permute-done((bf16[192,128]{1,0:T(8,128)(2,1)S(1)}, bf16[192,128]{1,0:T(8,128)(2,1)S(1)}, u32[]{:S(2)}, u32[]{:S(2)}) %collective-permute-start) | collective-permute-done | bytes 49184 | tf_op jit(solution)/shard_map/ppermute | solution.py:409
  41.7 0.2 broadcast_in_dim.6
  41.9 1.6 %pad_maximum_fusion = bf16[4,2,1152,128]{3,2,1,0:T(8,128)(2,1)} fusion(bf16[4,2,192,128]{3,2,1,0:T(8,128)(2,1)S(1)} %broadcast_in_dim.8, bf16[4,2,192,128]{3,2,1,0:T(8,128)(2,1)S(1)} %broadcast_in_dim.7, bf16[4,2,768,128]{3,2,1,0:T(8,128)(2,1)S(1)} %broadcast_in_dim.6), kind=kLoop, calls=%fused_computation | loop fusion | flops 7077888 | bytes 4718592 | tf_op jit(solution)/shard_map/concatenate | solution.py:414
  43.5 4.4 %all-to-all-start.1 = ((bf16[8,1152,128]{2,1,0:T(8,128)(2,1)}), bf16[8,1152,128]{2,1,0:T(8,128)(2,1)S(1)}, u32[]{:S(2)}, u32[]{:S(2)}) async-start(bf16[8,1152,128]{2,1,0:T(8,128)(2,1)} %bitcast.43), calls=%async_computation.1 | async-start | bytes 4718592 | tf_op jit(solution)/shard_map/all_to_all | solution.py:30
  48.0 0.1 copy.22
  48.2 0.1 fusion.6
  48.4 0.2 fusion
  48.6 0.2 fusion.1
  48.9 29.1 %all-to-all-done.1.query_ref.mine_ref = bf16[8,1152,128]{2,1,0:T(8,128)(2,1)S(1)} async-done(((bf16[8,1152,128]{2,1,0:T(8,128)(2,1)}), bf16[8,1152,128]{2,1,0:T(8,128)(2,1)S(1)}, u32[]{:S(2)}, u32[]{:S(2)}) %all-to-all-start.1) | async-done | bytes 2359328 | tf_op jit(solution)/shard_map/all_to_all | solution.py:30
  77.9 1.9 %collective-permute-start.1 = (bf16[8,1152,128]{2,1,0:T(8,128)(2,1)S(1)}, bf16[8,1152,128]{2,1,0:T(8,128)(2,1)}, u32[]{:S(2)}, u32[]{:S(2)}) collective-permute-start(bf16[8,1152,128]{2,1,0:T(8,128)(2,1)S(1)} %all-to-all-done.1.query_ref.mine_ref), channel_id=1, source_target_pairs={{0,4},{4,0},{1,5},{5,1},{2,6},{6,2},{3,7},{7,3},{8,12},{12,8},{9,1... | collective-permute-start | bytes 7077896 | tf_op jit(solution)/shard_map/ppermute | solution.py:416
  79.8 33.2 %all_gather.11 = bf16[2304,128]{1,0:T(8,128)(2,1)S(1)} all-gather(bf16[288,128]{1,0:T(8,128)(2,1)S(1)} %pad_maximum_fusion.1), channel_id=1, replica_groups=mesh['far'=8,'pair'=2,'x'=4,'core'=2,'tp'=4] {'far'}, dimensions={0}, use_global_device_ids=true | all-gather | bytes 663552 | tf_op jit(solution)/shard_map/all_gather | solution.py:425
  113.1 7.9 %attend.1 = bf16[16,144,128]{2,1,0:T(8,128)(2,1)} custom-call(bf16[8,288,128]{2,1,0:T(8,128)(2,1)S(1)} %bitcast.42, bf16[8,1152,128]{2,1,0:T(8,128)(2,1)S(1)} %all-to-all-done.1.query_ref.mine_ref), custom_call_target="tpu_custom_call" | custom-call | flops 1879048192 | bytes 2000000 | tf_op jit(solution)/shard_map/attend/pallas_call | solution.py:143
  120.9 5.1 %all-to-all-start.2 = ((bf16[16,144,128]{2,1,0:T(8,128)(2,1)}), bf16[16,144,128]{2,1,0:T(8,128)(2,1)S(1)}, u32[]{:S(2)}, u32[]{:S(2)}) async-start(bf16[16,144,128]{2,1,0:T(8,128)(2,1)} %attend.1), calls=%async_computation.2 | async-start | bytes 1179648 | tf_op jit(solution)/shard_map/all_to_all | solution.py:30
  126.0 2.0 %collective-permute-start.2 = (bf16[16,2048]{1,0:T(8,128)(2,1)S(1)}, bf16[16,2048]{1,0:T(8,128)(2,1)S(1)}, u32[]{:S(2)}, u32[]{:S(2)}) collective-permute-start(bf16[16,2048]{1,0:T(8,128)(2,1)S(1)} %copy-done.8), channel_id=1, source_target_pairs={{0,4},{4,8},{8,12},{12,16},{16,20},{20,24},{24,28},{28,32},{32,36}... | collective-permute-start | bytes 196616 | tf_op jit(solution)/shard_map/ppermute | solution.py:36
  128.0 8.8 %collective-permute-done.2.edge_ref = bf16[16,2048]{1,0:T(8,128)(2,1)S(1)} collective-permute-done((bf16[16,2048]{1,0:T(8,128)(2,1)S(1)}, bf16[16,2048]{1,0:T(8,128)(2,1)S(1)}, u32[]{:S(2)}, u32[]{:S(2)}) %collective-permute-start.2) | collective-permute-done | bytes 65568 | tf_op jit(solution)/shard_map/ppermute | solution.py:36
  136.9 2.8 %convolve.1.conv_ref = bf16[128,256]{1,0:T(8,128)(2,1)S(1)} custom-call(bf16[8,1152,128]{2,1,0:T(8,128)(2,1)S(1)} %all-to-all-done.1.query_ref.mine_ref, bf16[8,1152,128]{2,1,0:T(8,128)(2,1)} %collective-permute-done.1.other_ref, bf16[128,2048]{1,0:T(8,128)(2,1)} %get-tuple-element.11.normed_ref, bf16[16,2048]{1,0:T(8,128)(2,1)S(1)} %collective-permute-done.2.edge_ref, ...), custom_call_target="tpu_custom_call" | custom-call | flops 402653184 | bytes 4000000 | tf_op jit(solution)/shard_map/convolve/pallas_call | solution.py:271
  139.7 2.7 %merge.1 = (bf16[128,2048]{1,0:T(8,128)(2,1)}, f32[2,128]{1,0:T(2,128)S(1)}, f32[2,128]{1,0:T(2,128)S(1)}) custom-call(bf16[16,144,128]{2,1,0:T(8,128)(2,1)S(1)} %all-to-all-done.2.parts_ref, bf16[128,256]{1,0:T(8,128)(2,1)S(1)} %convolve.1.conv_ref, bf16[256,2048]{1,0:T(8,128)(2,1)} %output_hbm.1, bf16[128,2048]{1,0:T(8,128)(2,1)} %weight_hbm.1), custom_call_target="tpu_custom_call" | custom-call | flops 201326592 | bytes 2500000 | tf_op jit(solution)/shard_map/merge/pallas_call | solution.py:332
  142.4 4.1 %all-to-all-start.3 = ((bf16[4,32,2048]{2,1,0:T(8,128)(2,1)}), bf16[4,32,2048]{2,1,0:T(8,128)(2,1)S(1)}, u32[]{:S(2)}, u32[]{:S(2)}) async-start(bf16[4,32,2048]{2,1,0:T(8,128)(2,1)} %bitcast.18), calls=%async_computation.3 | async-start | bytes 1048576 | tf_op jit(solution)/shard_map/all_to_all | solution.py:30
  146.5 0.6 add.66
  147.0 7.5 %all-to-all-done.3 = bf16[4,32,2048]{2,1,0:T(8,128)(2,1)S(1)} async-done(((bf16[4,32,2048]{2,1,0:T(8,128)(2,1)}), bf16[4,32,2048]{2,1,0:T(8,128)(2,1)S(1)}, u32[]{:S(2)}, u32[]{:S(2)}) %all-to-all-start.3) | async-done | bytes 524320 | tf_op jit(solution)/shard_map/all_to_all | solution.py:30
  154.6 0.1 multiply_reduce_fusion.1
  154.8 0.8 multiply_convert_fusion
  (37 shorter events, 0.5 us)
Async XLA Ops:
  0.6 34.7 %copy-start = (bf16[768,128]{1,0:T(8,128)(2,1)S(1)}, bf16[768,128]{1,0:T(8,128)(2,1)}, u32[]{:S(2)}) copy-start(bf16[768,128]{1,0:T(8,128)(2,1)} %param.29) | copy-start | bytes 589828
  2.2 32.7 %copy-start.6 = (f32[768]{0:T(1024)S(1)}, f32[768]{0:T(1024)}, u32[]{:S(2)}) copy-start(f32[768]{0:T(1024)} %param.27) | copy-start | bytes 9220
  2.2 32.9 %copy-start.4 = (bf16[768,64]{0,1:T(8,128)(2,1)S(1)}, bf16[768,64]{0,1:T(8,128)(2,1)}, u32[]{:S(2)}) copy-start(bf16[768,64]{0,1:T(8,128)(2,1)} %param.30) | copy-start | bytes 294916
  2.2 39.4 %all-to-all-start = ((bf16[16,96,128]{2,1,0:T(8,128)(2,1)}), bf16[16,96,128]{2,1,0:T(8,128)(2,1)S(1)}, u32[]{:S(2)}, u32[]{:S(2)}) async-start(bf16[16,96,128]{2,1,0:T(8,128)(2,1)} %spread_gates.1), calls=%async_computation | async-start | bytes 786432 | tf_op jit(solution)/shard_map/all_to_all | solution.py:30
  35.6 6.0 %collective-permute-start = (bf16[192,128]{1,0:T(8,128)(2,1)S(1)}, bf16[192,128]{1,0:T(8,128)(2,1)S(1)}, u32[]{:S(2)}, u32[]{:S(2)}) collective-permute-start(bf16[192,128]{1,0:T(8,128)(2,1)S(1)} %pad_maximum_fusion.2), channel_id=1, source_target_pairs={{0,32},{32,0},{1,33},{33,1},{2,34},{34,2},{3,35},{35,3},{4,36},{36... | collective-permute-start | bytes 147464 | tf_op jit(solution)/shard_map/ppermute | solution.py:409
  43.5 4.7 %copy-start.7 = (f32[512]{0:T(512)S(1)}, f32[512]{0:T(512)}, u32[]{:S(2)}) copy-start(f32[512]{0:T(512)} %param.28) | copy-start | bytes 6148
  43.5 4.8 %copy-start.2 = (bf16[512,128]{1,0:T(8,128)(2,1)S(1)}, bf16[512,128]{1,0:T(8,128)(2,1)}, u32[]{:S(2)}) copy-start(bf16[512,128]{1,0:T(8,128)(2,1)} %param.31) | copy-start | bytes 393220
  43.5 5.1 %copy-start.3 = (bf16[512,128]{1,0:T(8,128)(2,1)S(1)}, bf16[512,128]{1,0:T(8,128)(2,1)}, u32[]{:S(2)}) copy-start(bf16[512,128]{1,0:T(8,128)(2,1)} %param.32) | copy-start | bytes 393220
  43.5 34.4 %all-to-all-start.1 = ((bf16[8,1152,128]{2,1,0:T(8,128)(2,1)}), bf16[8,1152,128]{2,1,0:T(8,128)(2,1)S(1)}, u32[]{:S(2)}, u32[]{:S(2)}) async-start(bf16[8,1152,128]{2,1,0:T(8,128)(2,1)} %bitcast.43), calls=%async_computation.1 | async-start | bytes 4718592 | tf_op jit(solution)/shard_map/all_to_all | solution.py:30
  77.9 58.9 %collective-permute-start.1 = (bf16[8,1152,128]{2,1,0:T(8,128)(2,1)S(1)}, bf16[8,1152,128]{2,1,0:T(8,128)(2,1)}, u32[]{:S(2)}, u32[]{:S(2)}) collective-permute-start(bf16[8,1152,128]{2,1,0:T(8,128)(2,1)S(1)} %all-to-all-done.1.query_ref.mine_ref), channel_id=1, source_target_pairs={{0,4},{4,0},{1,5},{5,1},{2,6},{6,2},{3,7},{7,3},{8,12},{12,8},{9,1... | collective-permute-start | bytes 7077896 | tf_op jit(solution)/shard_map/ppermute | solution.py:416
  113.1 12.9 %copy-start.8 = (bf16[16,2048]{1,0:T(8,128)(2,1)S(1)}, bf16[16,2048]{1,0:T(8,128)(2,1)}, u32[]{:S(2)}) copy-start(bf16[16,2048]{1,0:T(8,128)(2,1)} %get-tuple-element.12) | copy-start | bytes 196612
  113.1 23.8 %copy-start.1 = (f32[3,256]{1,0:T(4,128)S(1)}, f32[3,256]{1,0:T(4,128)}, u32[]{:S(2)}) copy-start(f32[3,256]{1,0:T(4,128)} %taps_ref.1) | copy-start | bytes 9220
  120.9 18.7 %all-to-all-start.2 = ((bf16[16,144,128]{2,1,0:T(8,128)(2,1)}), bf16[16,144,128]{2,1,0:T(8,128)(2,1)S(1)}, u32[]{:S(2)}, u32[]{:S(2)}) async-start(bf16[16,144,128]{2,1,0:T(8,128)(2,1)} %attend.1), calls=%async_computation.2 | async-start | bytes 1179648 | tf_op jit(solution)/shard_map/all_to_all | solution.py:30
  126.0 10.8 %collective-permute-start.2 = (bf16[16,2048]{1,0:T(8,128)(2,1)S(1)}, bf16[16,2048]{1,0:T(8,128)(2,1)S(1)}, u32[]{:S(2)}, u32[]{:S(2)}) collective-permute-start(bf16[16,2048]{1,0:T(8,128)(2,1)S(1)} %copy-done.8), channel_id=1, source_target_pairs={{0,4},{4,8},{8,12},{12,16},{16,20},{20,24},{24,28},{28,32},{32,36}... | collective-permute-start | bytes 196616 | tf_op jit(solution)/shard_map/ppermute | solution.py:36
  139.6 15.1 %copy-start.5 = (f32[2048]{0:T(1024)S(1)}, f32[2048]{0:T(1024)}, u32[]{:S(2)}) copy-start(f32[2048]{0:T(1024)} %param.35) | copy-start | bytes 24580
  142.4 12.2 %all-to-all-start.3 = ((bf16[4,32,2048]{2,1,0:T(8,128)(2,1)}), bf16[4,32,2048]{2,1,0:T(8,128)(2,1)S(1)}, u32[]{:S(2)}, u32[]{:S(2)}) async-start(bf16[4,32,2048]{2,1,0:T(8,128)(2,1)} %bitcast.18), calls=%async_computation.3 | async-start | bytes 1048576 | tf_op jit(solution)/shard_map/all_to_all | solution.py:30
